TPU v7x, 32 devices: a whole 2x2x4 slice. The times are simulated.
32 devices in a mesh: rep: 2 (over core), fs: 8 (over z, y), tp: 2 (over x).
Axes of the slice: x: 2, y: 2, z: 4, core: 2. Of those that a mesh axis runs over, the one named last changes fastest.
Arguments:
- residual: bfloat16 [2048, 4096], P('tp', ('rep', 'fs')), may hold values from -6 to 6
- mixer_gain: float32 [2048], replicated, may hold values from 0.1 to 1.9
- value_weight: float32 [2048, 512], P('fs', 'tp'), may hold values from -0.125 to 0.125
- value_scale: float32 [512], P('tp'), may hold values from 0.2 to 8, as said below
- input_gate_weight: float32 [2048, 512], P('fs', 'tp'), may hold values from -0.125 to 0.125
- input_gate_scale: float32 [512], P('tp'), may hold values from 0.5 to 2
- output_gate_weight: float32 [2048, 512], P('fs', 'tp'), may hold values from -0.125 to 0.125
- output_gate_scale: float32 [512], P('tp'), may hold values from 0.5 to 2
- conv_taps: float32 [3, 512], P(None, 'tp'), may hold values from -3 to 3
- conv_gain: float32 [512], P('tp'), may hold values from 0.1 to 1.9
- mixer_out_weight: float32 [512, 2048], P('tp', 'fs'), may hold values from -0.25 to 0.25
- mixer_out_scale: float32 [2048], P('fs'), may hold values from 0.5 to 2
- channel_gain: float32 [2048], replicated, may hold values from 0.1 to 1.9
- gate_weight: float32 [2048, 5632], P('fs', 'tp'), may hold values from -0.125 to 0.125
- gate_scale: float32 [5632], P('tp'), may hold values from 0.5 to 2
- up_weight: float32 [2048, 5632], P('fs', 'tp'), may hold values from -0.125 to 0.125
- up_scale: float32 [5632], P('tp'), may hold values from 0.5 to 2
- down_weight: float32 [5632, 2048], P('tp', 'fs'), may hold values from -0.078125 to 0.078125
- down_scale: float32 [2048], P('fs'), may hold values from 0.5 to 2
Outputs:
- layer_out: bfloat16 [2048, 4096], P('tp', ('rep', 'fs'))
Inputs may be any that keep to these rules, and one draw needn't show every extreme that they name: `value_scale`: positive column scales.
All inputs are finite; a program needn't handle non-finite values.
Results may differ from a plain program's by a relative error of at most 0.018.
Values may be sent and summed in bfloat16 or wider, within the bound.
No kernel may reach another device: no remote copies, remote signals or barrier semaphores. Data moves between devices by JAX's collectives and lax.ppermute only.
A program may use at most 128 MiB of HBM per device.

v0:
```python
import jax
import jax.numpy as jnp
from jax import lax
from jax.sharding import PartitionSpec as P

LEN = 128


epsilon = 1e-06


def normalize(values, gain):
    floats = values.astype(jnp.float32)
    mean = jnp.mean(floats * floats, axis=0, keepdims=True)
    return (floats * lax.rsqrt(mean + epsilon) * gain[:, None]).astype(jnp.bfloat16)


def contract(weight, rows):
    return lax.dot_general(
        weight, rows, (((0,), (0,)), ((), ())), preferred_element_type=jnp.float32
    )


def causal_conv(values, taps, length):
    total = values.shape[1]
    position = jnp.arange(total, dtype=jnp.int32) % length
    shifted_one = jnp.pad(values, ((0, 0), (1, 0)))[:, :total]
    shifted_two = jnp.pad(values, ((0, 0), (2, 0)))[:, :total]
    shifted_one = jnp.where(position[None, :] >= 1, shifted_one, 0.0)
    shifted_two = jnp.where(position[None, :] >= 2, shifted_two, 0.0)
    return (
        taps[2][:, None] * values + taps[1][:, None] * shifted_one + taps[0][:, None] * shifted_two
    )


def local(
    residual,
    mixer_gain,
    value_weight,
    value_scale,
    input_gate_weight,
    input_gate_scale,
    output_gate_weight,
    output_gate_scale,
    conv_taps,
    conv_gain,
    mixer_out_weight,
    mixer_out_scale,
    channel_gain,
    gate_weight,
    gate_scale,
    up_weight,
    up_scale,
    down_weight,
    down_scale,
):
    own_rows = residual.shape[0]
    tokens = residual.shape[1]
    groups = lax.axis_size("tp")
    channels = value_weight.shape[1] * groups
    whole = lax.all_gather(residual, "tp", axis=0, tiled=True)
    normed = normalize(whole, mixer_gain)
    value = contract(
        lax.all_gather(value_weight.astype(jnp.bfloat16), "fs", axis=0, tiled=True), normed
    )
    in_gate = contract(
        lax.all_gather(input_gate_weight.astype(jnp.bfloat16), "fs", axis=0, tiled=True), normed
    )
    out_gate = contract(
        lax.all_gather(output_gate_weight.astype(jnp.bfloat16), "fs", axis=0, tiled=True), normed
    )
    value = value * value_scale[:, None]
    in_gate = in_gate * input_gate_scale[:, None]
    out_gate = out_gate * output_gate_scale[:, None]
    mixed = out_gate * causal_conv(in_gate * value, conv_taps, LEN)
    squares = lax.psum(jnp.sum(mixed * mixed, axis=0), "tp")
    conv_normed = (
        mixed * lax.rsqrt(squares / channels + epsilon)[None, :] * conv_gain[:, None]
    ).astype(jnp.bfloat16)
    out_full = lax.all_gather(mixer_out_weight.astype(jnp.bfloat16), "fs", axis=1, tiled=True)
    out_scale, down_scale_full = (
        lax.all_gather(mixer_out_scale, "fs", axis=0, tiled=True),
        lax.all_gather(down_scale, "fs", axis=0, tiled=True),
    )
    conv_all = lax.all_gather(conv_normed, "tp", axis=0, tiled=True)
    out_own = lax.all_to_all(out_full, "tp", split_axis=1, concat_axis=0, tiled=True)
    block_width = conv_normed.shape[0]
    weight_blocks = out_own.reshape(groups, block_width, own_rows)
    row_blocks = conv_all.reshape(groups, block_width, tokens)
    parts = lax.dot_general(
        weight_blocks, row_blocks, (((1,), (1,)), ((0,), (0,))), preferred_element_type=jnp.float32
    )
    own_scale = lax.dynamic_slice_in_dim(out_scale, lax.axis_index("tp") * own_rows, own_rows, 0)
    rounded = (parts * own_scale[None, :, None]).astype(jnp.bfloat16)
    total = jnp.sum(rounded.astype(jnp.float32), axis=0)
    after_own = (residual.astype(jnp.float32) + total).astype(jnp.bfloat16)
    after_whole = lax.all_gather(after_own, "tp", axis=0, tiled=True)
    normed_two = normalize(after_whole, channel_gain)
    gate_full, up_full = (
        lax.all_gather(gate_weight.astype(jnp.bfloat16), "fs", axis=0, tiled=True),
        lax.all_gather(up_weight.astype(jnp.bfloat16), "fs", axis=0, tiled=True),
    )
    gate = contract(gate_full, normed_two)
    upper = contract(up_full, normed_two)
    hidden = (jax.nn.silu(gate * gate_scale[:, None]) * (upper * up_scale[:, None])).astype(
        jnp.bfloat16
    )
    down_full = lax.all_gather(down_weight.astype(jnp.bfloat16), "fs", axis=1, tiled=True)
    total_two = lax.psum_scatter(
        (contract(down_full, hidden) * down_scale_full[:, None]).astype(jnp.bfloat16),
        "tp",
        scatter_dimension=0,
        tiled=True,
    ).astype(jnp.float32)
    return (after_own.astype(jnp.float32) + total_two).astype(jnp.bfloat16)


def solution(mesh):
    placed = (
        P("tp", ("rep", "fs")),
        P(),
        P("fs", "tp"),
        P("tp"),
        P("fs", "tp"),
        P("tp"),
        P("fs", "tp"),
        P("tp"),
        P(None, "tp"),
        P("tp"),
        P("tp", "fs"),
        P("fs"),
        P(),
        P("fs", "tp"),
        P("tp"),
        P("fs", "tp"),
        P("tp"),
        P("tp", "fs"),
        P("fs"),
    )
    return jax.shard_map(
        local, mesh=mesh, in_specs=placed, out_specs=P("tp", ("rep", "fs")), check_vma=False
    )
```

profile of v0, /device:TPU:0, one launch (start us, length us, event | category | flops | bytes accessed | tf_op | source)
XLA Modules:
  0.0 769.4 jit_solution(15757913677722648637)
XLA Ops:
  6.5 0.0 all-gather.12.cloned.1.call-start
  6.6 0.7 all-gather.12.cloned.1.call-update
  7.3 0.0 all-gather.20.cloned.1.call-start
  7.3 1.7 copy.35
  9.0 0.0 all-gather.20.cloned.1.call-update
  9.1 0.0 all-gather.16.cloned.1.call-start
  9.1 1.6 convert_element_type.76
  10.7 0.0 all-gather.16.cloned.1.call-update
  10.8 0.0 all-gather.18.cloned.1.call-start
  10.8 1.6 convert_element_type.77
  12.4 0.0 all-gather.18.cloned.1.call-update
  12.5 0.0 all-gather.14.cloned.1.call-start
  12.5 0.7 convert_element_type.75
  13.2 0.0 all-gather.14.cloned.1.call-update
  13.2 0.2 copy.32
  13.4 22.3 %all-gather = f32[8,1,256]{2,1,0:T(1,128)S(1)} all-gather(f32[1,1,256]{2,1,0:T(1,128)S(1)} %bitcast.47), channel_id=1, replica_groups=mesh['rep'=2,'fs'=8,'tp'=2] {'fs'}, dimensions={0}, use_global_device_ids=true | all-gather | bytes 9216 | tf_op jit(solution)/shard_map/all_gather | solution.py:82
  35.8 0.0 copy-done.6
  35.8 0.0 all-gather.12.cloned.1.call-done
  35.8 1.5 fusion.6
  37.4 38.0 %all-gather.20.cloned.1.call-done = bf16[256,2048]{0,1:T(8,128)(2,1)} async-done(((bf16[256,256]{0,1:T(8,128)(2,1)}), bf16[256,2048]{0,1:T(8,128)(2,1)}) %all-gather.20.cloned.1.call-update) | async-done | bytes 1048592 | tf_op jit(solution)/shard_map/all_gather | solution.py:80
  75.4 2.4 copy.36
  77.7 3.6 all-to-all-start
  81.3 0.0 copy-start.15
  81.3 0.0 all-gather.22.cloned.1.call-start
  81.4 35.1 %all-gather.16.cloned.1.call-done = bf16[2048,256]{1,0:T(8,128)(2,1)} async-done(((bf16[256,256]{1,0:T(8,128)(2,1)}), bf16[2048,256]{1,0:T(8,128)(2,1)}) %all-gather.16.cloned.1.call-update) | async-done | bytes 1048592 | tf_op jit(solution)/shard_map/all_gather | solution.py:67
  116.5 0.0 copy-done.3
  116.5 2.0 convolution_multiply_fusion.4
  118.6 0.0 copy-start.16
  118.6 38.9 %all-gather.18.cloned.1.call-done = bf16[2048,256]{1,0:T(8,128)(2,1)} async-done(((bf16[256,256]{1,0:T(8,128)(2,1)}), bf16[2048,256]{1,0:T(8,128)(2,1)}) %all-gather.18.cloned.1.call-update) | async-done | bytes 1048592 | tf_op jit(solution)/shard_map/all_gather | solution.py:64
  157.5 2.0 fusion.13
  159.6 39.0 %all-gather.14.cloned.1.call-done = bf16[2048,256]{1,0:T(8,128)(2,1)} async-done(((bf16[256,256]{1,0:T(8,128)(2,1)}), bf16[2048,256]{1,0:T(8,128)(2,1)}) %all-gather.14.cloned.1.call-update) | async-done | bytes 1048592 | tf_op jit(solution)/shard_map/all_gather | solution.py:70
  198.5 0.0 copy-done.16
  198.5 2.1 multiply_reduce_fusion
  200.7 4.9 psum.7
  205.6 0.1 multiply_convert_fusion.1
  205.7 5.6 all_gather.40
  211.4 0.0 all-to-all-done
  211.4 0.5 convert_reduce_fusion
  211.9 1.0 fusion.16
  212.8 0.0 all-gather.22.cloned.1.call-update
  212.8 0.0 copy-start.1
  212.9 0.0 all-gather.24.cloned.1.call-start
  212.9 3.2 convert_element_type.86
  216.1 0.0 all-gather.24.cloned.1.call-update
  216.1 0.0 all-gather.26.cloned.1.call-start
  216.2 1.2 convert_element_type.87
  217.4 0.0 all-gather.26.cloned.1.call-update
  217.4 0.0 copy-start.9
  217.5 0.0 all-gather.28.cloned.1.call-start
  217.5 3.3 convert_element_type.89
  220.8 0.0 all-gather.28.cloned.1.call-update
  220.8 0.0 reduce-scatter.2.cloned.1.call-start
  220.9 18.3 %all-gather.1 = f32[8,1,256]{2,1,0:T(1,128)S(1)} all-gather(f32[1,1,256]{2,1,0:T(1,128)S(1)} %bitcast.48), channel_id=1, replica_groups=mesh['rep'=2,'fs'=8,'tp'=2] {'fs'}, dimensions={0}, use_global_device_ids=true | all-gather | bytes 9216 | tf_op jit(solution)/shard_map/all_gather | solution.py:83
  239.2 1.5 fusion.9
  240.7 0.0 copy-start.11
  240.7 157.8 %all-gather.24.cloned.1.call-done = bf16[2048,2816]{1,0:T(8,128)(2,1)} async-done(((bf16[256,2816]{1,0:T(8,128)(2,1)}), bf16[2048,2816]{1,0:T(8,128)(2,1)}) %all-gather.24.cloned.1.call-update) | async-done | bytes 11534352 | tf_op jit(solution)/shard_map/all_gather | solution.py:100
  398.5 9.4 %fusion = f32[2816,256]{0,1:T(8,128)} fusion(bf16[2048,2816]{1,0:T(8,128)(2,1)} %all-gather.24.cloned.1.call-done, f32[2816]{0:T(1024)S(1)} %copy-done.10, bf16[2048,256]{0,1:T(8,128)(2,1)} %all-gather.22.cloned.1.call-done, f32[2048]{0:T(1024)S(1)} %copy-done.13, f32[256]{0:T(256)S(1)} %add_rsqrt_fusion), kind=kOutput, calls=%fused_computation.2 | convolution fusion | flops 2955608064 | bytes 15486976 | tf_op jit(solution)/shard_map/dot_general | solution.py:19
  408.0 154.3 %all-gather.26.cloned.1.call-done = bf16[2048,2816]{1,0:T(8,128)(2,1)} async-done(((bf16[256,2816]{1,0:T(8,128)(2,1)}), bf16[2048,2816]{1,0:T(8,128)(2,1)}) %all-gather.26.cloned.1.call-update) | async-done | bytes 11534352 | tf_op jit(solution)/shard_map/all_gather | solution.py:101
  562.3 163.6 %all-gather.28.cloned.1.call-done = bf16[2816,2048]{1,0:T(8,128)(2,1)} async-done(((bf16[2816,256]{1,0:T(8,128)(2,1)}), bf16[2816,2048]{1,0:T(8,128)(2,1)}) %all-gather.28.cloned.1.call-update) | async-done | bytes 11534352 | tf_op jit(solution)/shard_map/all_gather | solution.py:108
  725.8 15.7 %fusion.5 = bf16[2048,256]{0,1:T(8,128)(2,1)} fusion(bf16[2816,2048]{1,0:T(8,128)(2,1)} %all-gather.28.cloned.1.call-done, f32[2048]{0:T(1024)S(1)} %bitcast.46, bf16[2048,2816]{1,0:T(8,128)(2,1)} %all-gather.26.cloned.1.call-done, f32[2816,256]{0,1:T(8,128)} %fusion, f32[2816]{0:T(1024)S(1)} %copy-done.11, bf16[2048,256]{0,1:T(8,128)(2,1)S(1)} %copy-done.4, ...), kind=kOutput, calls=%fused_computation.12 | convolution fusion | flops 5913772032 | bytes 28078080 | tf_op jit(solution)/shard_map/dot_general | solution.py:19
  741.6 0.0 reduce-scatter.2.cloned.1.call-update
  741.6 18.7 %reduce-scatter.2.cloned.1.call-done = bf16[1024,256]{0,1:T(8,128)(2,1)} async-done(((bf16[2048,256]{0,1:T(8,128)(2,1)}), bf16[1024,256]{0,1:T(8,128)(2,1)}) %reduce-scatter.2.cloned.1.call-update) | async-done | bytes 524304 | tf_op jit(solution)/shard_map/reduce_scatter | solution.py:109
  760.3 1.2 add_convert_fusion
  761.6 1.0 copy.38
  (33 shorter events, 0.1 us)
Async XLA Ops:
  6.5 6.7 copy-start.2
  6.5 6.0 copy-start.5
  6.5 6.9 copy-start.8
  6.5 29.2 %copy-start.6 = (f32[3,256]{1,0:T(4,128)S(1)}, f32[3,256]{1,0:T(4,128)}, u32[]{:S(2)}) copy-start(f32[3,256]{1,0:T(4,128)} %param.27) | copy-start | bytes 9220
  6.5 29.3 %all-gather.12.cloned.1.call-start = ((), (), s32[]{:S(2)}) async-start(), calls=%async_computation.2 | async-start | bytes 1572864 | tf_op jit(solution)/shard_map/all_gather | solution.py:61
  7.3 68.1 %all-gather.20.cloned.1.call-start = ((), (), s32[]{:S(2)}) async-start(), calls=%async_computation.6 | async-start | bytes 1179648 | tf_op jit(solution)/shard_map/all_gather | solution.py:80
  9.1 107.4 %all-gather.16.cloned.1.call-start = ((), (), s32[]{:S(2)}) async-start(), calls=%async_computation.4 | async-start | bytes 1179648 | tf_op jit(solution)/shard_map/all_gather | solution.py:67
  10.8 146.8 %all-gather.18.cloned.1.call-start = ((), (), s32[]{:S(2)}) async-start(), calls=%async_computation.5 | async-start | bytes 1179648 | tf_op jit(solution)/shard_map/all_gather | solution.py:64
  12.5 186.1 %all-gather.14.cloned.1.call-start = ((), (), s32[]{:S(2)}) async-start(), calls=%async_computation.3 | async-start | bytes 1179648 | tf_op jit(solution)/shard_map/all_gather | solution.py:70
  75.4 41.2 %copy-start.3 = (bf16[2048,256]{1,0:T(8,128)(2,1)S(1)}, bf16[2048,256]{1,0:T(8,128)(2,1)}, u32[]{:S(2)}) copy-start(bf16[2048,256]{1,0:T(8,128)(2,1)} %all-gather.12.cloned.1.call-done) | copy-start | bytes 3145732
  75.4 41.2 %copy-start.12 = (f32[2048]{0:T(1024)S(1)}, f32[2048]{0:T(1024)}, u32[]{:S(2)}) copy-start(f32[2048]{0:T(1024)} %param.20) | copy-start | bytes 24580
  75.4 41.2 %copy-start.14 = (f32[256]{0:T(256)S(1)}, f32[256]{0:T(256)}, u32[]{:S(2)}) copy-start(f32[256]{0:T(256)} %param.24) | copy-start | bytes 3076
  77.7 133.6 %all-to-all-start = ((bf16[256,2,1024]{2,0,1:T(8,128)(2,1)}), bf16[256,2,1024]{2,0,1:T(8,128)(2,1)S(1)}, u32[]{:S(2)}, u32[]{:S(2)}) async-start(bf16[256,2,1024]{2,0,1:T(8,128)(2,1)} %copy.36), calls=%async_computation | async-start | bytes 2097152 | tf_op jit(solution)/shard_map/all_to_all | solution.py:86
  81.3 76.2 %copy-start.15 = (f32[256]{0:T(256)S(1)}, f32[256]{0:T(256)}, u32[]{:S(2)}) copy-start(f32[256]{0:T(256)} %param.22) | copy-start | bytes 3076
  81.3 157.8 %all-gather.22.cloned.1.call-start = ((), (), s32[]{:S(2)}) async-start(), calls=%async_computation.7 | async-start | bytes 1572864 | tf_op jit(solution)/shard_map/all_gather | solution.py:97
  118.6 80.0 %copy-start.16 = (f32[256]{0:T(256)S(1)}, f32[256]{0:T(256)}, u32[]{:S(2)}) copy-start(f32[256]{0:T(256)} %param.26) | copy-start | bytes 3076
  198.5 7.1 copy-start.7
  212.8 3.3 copy-start.1
  212.9 185.7 %all-gather.24.cloned.1.call-start = ((), (), s32[]{:S(2)}) async-start(), calls=%async_computation.8 | async-start | bytes 12976128 | tf_op jit(solution)/shard_map/all_gather | solution.py:100
  216.1 346.1 %all-gather.26.cloned.1.call-start = ((), (), s32[]{:S(2)}) async-start(), calls=%async_computation.9 | async-start | bytes 12976128 | tf_op jit(solution)/shard_map/all_gather | solution.py:101
  217.4 3.4 copy-start.9
  217.5 508.4 %all-gather.28.cloned.1.call-start = ((), (), s32[]{:S(2)}) async-start(), calls=%async_computation.10 | async-start | bytes 12976128 | tf_op jit(solution)/shard_map/all_gather | solution.py:108
  220.8 177.8 %copy-start.10 = (f32[2816]{0:T(1024)S(1)}, f32[2816]{0:T(1024)}, u32[]{:S(2)}) copy-start(f32[2816]{0:T(1024)} %param.33) | copy-start | bytes 33796
  220.8 177.8 %copy-start.13 = (f32[2048]{0:T(1024)S(1)}, f32[2048]{0:T(1024)}, u32[]{:S(2)}) copy-start(f32[2048]{0:T(1024)} %param.31) | copy-start | bytes 24580
  220.8 539.5 %reduce-scatter.2.cloned.1.call-start = ((), (), s32[]{:S(2)}) async-start(), calls=%async_computation.11 | async-start | bytes 1572864 | tf_op jit(solution)/shard_map/reduce_scatter | solution.py:109
  240.7 485.1 %copy-start.4 = (bf16[2048,256]{0,1:T(8,128)(2,1)S(1)}, bf16[2048,256]{0,1:T(8,128)(2,1)}, u32[]{:S(2)}) copy-start(bf16[2048,256]{0,1:T(8,128)(2,1)} %all-gather.22.cloned.1.call-done) | copy-start | bytes 3145732
  240.7 485.1 %copy-start.11 = (f32[2816]{0:T(1024)S(1)}, f32[2816]{0:T(1024)}, u32[]{:S(2)}) copy-start(f32[2816]{0:T(1024)} %param.35) | copy-start | bytes 33796
  725.8 34.5 %copy-start = (bf16[1024,256]{0,1:T(8,128)(2,1)S(1)}, bf16[1024,256]{0,1:T(8,128)(2,1)}, u32[]{:S(2)}) copy-start(bf16[1024,256]{0,1:T(8,128)(2,1)} %fusion.16) | copy-start | bytes 1572868
Sparse Core Ops, SparseCore 0:
  8.9 23.9 all-gather.11
  35.0 40.2 all-gather.19
  77.5 38.9 all-gather.15
  118.5 38.9 all-gather.17
  159.5 38.9 all-gather.13
  213.0 19.9 all-gather.21
  235.2 163.2 all-gather.23
  400.7 161.4 all-gather.25
  564.3 161.4 all-gather.27
  741.7 18.5 reduce-scatter.1
where the time goes:
time: 770 us; the launch traced here: 769 us
  waiting for transfers between devices  646 us (84%)
  blocking collectives  51.2 us (7%)
  matrix products  31.9 us (4%)
  other arithmetic  17 us (2%)
  between operations  13.7 us (2%)
    all_gather x1, waiting for transfers between devices, local(): lax.all_gather(down_weight.astype(jnp.bfloat16), 'fs', axis=1, tiled=True)  164 us
    all_gather x1, waiting for transfers between devices, local(): lax.all_gather(gate_weight.astype(jnp.bfloat16), 'fs', axis=0, tiled=True)  158 us
    all_gather x1, waiting for transfers between devices, local(): lax.all_gather(up_weight.astype(jnp.bfloat16), 'fs', axis=0, tiled=True)  154 us
    all_gather x1, waiting for transfers between devices, local(): lax.all_gather(output_gate_weight.astype(jnp.bfloat16), 'fs', axis=0, til...  39 us
    all_gather x1, waiting for transfers between devices, local(): lax.all_gather(value_weight.astype(jnp.bfloat16), 'fs', axis=0, tiled=True)  38.9 us
    all_gather x1, waiting for transfers between devices, local(): lax.all_gather(mixer_out_weight.astype(jnp.bfloat16), 'fs', axis=1, tiled...  38 us
    all_gather x1, waiting for transfers between devices, local(): lax.all_gather(input_gate_weight.astype(jnp.bfloat16), 'fs', axis=0, tile...  35.1 us
    dot_general x5, matrix products, contract(): lax.dot_general(weight, rows, (((0,), (0,)), ((), ())), preferred_element...  31.4 us
  transfers between devices with their start and end apart: 11, of which 8 were waited for; matrix products, arithmetic and copies ran while one was open for 5% of the time, Pallas kernels for 0%

commit v1 on v0

--- a/solution.py
+++ b/solution.py
@@ -1,6 +1,9 @@
 import jax
 import jax.numpy as jnp
 from jax import lax
+from jax.experimental import pallas as pl
+from jax.experimental.pallas import tpu as pltpu
+from jax.sharding import Mesh
 from jax.sharding import PartitionSpec as P
 
 LEN = 128
@@ -33,7 +36,7 @@
     )
 
 
-def local(
+def gathered(
     residual,
     mixer_gain,
     value_weight,
@@ -115,28 +118,448 @@
     return (after_own.astype(jnp.float32) + total_two).astype(jnp.bfloat16)
 
 
+def flip(array, *axes):
+    count = 2 ** len(axes)
+    return lax.ppermute(array, axes, [(i, count - 1 - i) for i in range(count)])
+
+
+def feature_block(spot_ref, piece, dy):
+    zh, zl, y = spot_ref[1], spot_ref[2], spot_ref[3]
+    return ((zh ^ (piece >> 1)) * 2 + (zl ^ (piece & 1))) * 2 + (y ^ dy)
+
+
+def lay_out(spot_ref, index, piece, full_ref):
+    width = piece.shape[1]
+    start = feature_block(spot_ref, index & 3, index >> 2) * width
+    full_ref[:, pl.ds(pl.multiple_of(start, width), width)] = piece
+
+
+def tile_of(spot_ref, index):
+    return (spot_ref[2] ^ (index >> 1)) * 2 + (spot_ref[0] ^ (index & 1))
+
+
+def channels_of(spot_ref, index):
+    return (spot_ref[0] ^ (index & 1)) * 2 + (spot_ref[2] ^ (index >> 1))
+
+
+def own_row(array, row):
+    rows = lax.broadcasted_iota(jnp.int32, array.shape, 0)
+    return jnp.sum(jnp.where(rows == row, array, 0.0), axis=0, keepdims=True)
+
+
+def turn(spot_ref, weight_ref, scale_ref, gain, turned_ref):
+    lanes = scale_ref.shape[1]
+    scales = scale_ref[...]
+    count = weight_ref.shape[1] // lanes
+    for index in range(count):
+        place = slice(index * lanes, (index + 1) * lanes)
+        scaled = weight_ref[:, place] * own_row(scales, spot_ref[0] * count + index)
+        turned_ref[place, :] = (scaled.T * gain).astype(jnp.bfloat16)
+
+
+def own_gain(spot_ref, gain_ref):
+    block, gains = feature_block(spot_ref, 0, 0), gain_ref[...]
+    return jnp.concatenate([own_row(gains, 2 * block), own_row(gains, 2 * block + 1)], axis=1)
+
+
+def small_kernel(spot_ref, *refs):
+    weights, scales, gain_ref = refs[:3], refs[3:6], refs[6]
+    out_ref, conv_gain_ref, out_scale_ref, mine_ref, other_ref, turned_ref = refs[7:]
+    rep, zl = spot_ref[0], spot_ref[2]
+    lanes = weights[0].shape[1]
+    channels = lanes // 2
+    gain = own_gain(spot_ref, gain_ref)
+    for index in range(3):
+        turn(spot_ref, weights[index], scales[index], gain, turned_ref)
+        for target, dl, place in ((mine_ref, 0, 0), (other_ref, 1, lanes)):
+            start = pl.multiple_of((zl ^ dl) * channels, channels)
+            place = place + index * channels
+            target[place : place + channels, :] = turned_ref[pl.ds(start, channels), :]
+    scale = own_row(out_scale_ref[...], rep)
+    for index in range(2):
+        place = slice(index * lanes, (index + 1) * lanes)
+        turned = (out_ref[place, :] * scale).T * own_row(conv_gain_ref[...], index)
+        rows = turned.astype(jnp.bfloat16)
+        mine_ref[3 * channels :, place] = rows
+        other_ref[:lanes, place] = rows
+
+
+def pair_kernel(spot_ref, *refs):
+    weights, scales, gain_ref, targets, turned_ref = refs[:2], refs[2:4], refs[4], refs[5:9], refs[9]
+    gain = own_gain(spot_ref, gain_ref)
+    for index in range(2):
+        turn(spot_ref, weights[index], scales[index], gain, turned_ref)
+        units = targets[0].shape[0]
+        for dl in range(2):
+            start = pl.multiple_of((spot_ref[2] ^ dl) * units, 16)
+            targets[2 * index + dl][...] = turned_ref[pl.ds(start, units), :]
+
+
+def last_kernel(spot_ref, weight_ref, scale_ref, *targets):
+    units, width = targets[0].shape
+    for chunk in range(2):
+        scale = own_row(scale_ref[...], chunk)
+        for dl in range(2):
+            start = pl.multiple_of((spot_ref[2] ^ dl) * units, 16)
+            rows = weight_ref[pl.ds(start, units), chunk * width : (chunk + 1) * width]
+            targets[2 * chunk + dl][...] = (rows * scale).astype(jnp.bfloat16)
+
+
+def mix_kernel(spot_ref, *refs):
+    rows, own_ref, twin_ref = refs[:8], refs[8], refs[9]
+    taps_ref, mixed_ref, whole_ref, full_ref = refs[10:]
+    half, tokens = rows[0].shape
+    channels = mixed_ref.shape[0]
+    for index in range(4):
+        lay_out(spot_ref, index, own_ref[index], full_ref)
+        lay_out(spot_ref, index + 4, twin_ref[index], full_ref)
+    position = lax.broadcasted_iota(jnp.int32, (channels, tokens), 1) % LEN
+    for tile in range(4):
+        total = jnp.zeros((3 * channels, tokens), jnp.float32)
+        squares = jnp.zeros((1, tokens), jnp.float32)
+        spot = pl.multiple_of(tile_of(spot_ref, tile) * tokens, tokens)
+        for dx in range(2):
+            block = rows[dx * 4 + tile][...]
+            start = pl.multiple_of((spot_ref[4] ^ dx) * half, half)
+            whole_ref[pl.ds(start, half), pl.ds(spot, tokens)] = block
+            total = total + jnp.dot(
+                full_ref[:, pl.ds(start, half)], block, preferred_element_type=jnp.float32
+            )
+            floats = block.astype(jnp.float32)
+            squares = squares + jnp.sum(floats * floats, axis=0, keepdims=True)
+        total = total * lax.rsqrt(squares / (2 * half) + epsilon)
+        u = total[:channels] * total[channels : 2 * channels]
+        one = jnp.where(position >= 1, pltpu.roll(u, 1, 1), 0.0)
+        two = jnp.where(position >= 2, pltpu.roll(u, 2, 1), 0.0)
+        conv = taps_ref[:, 2:3] * u + taps_ref[:, 1:2] * one + taps_ref[:, 0:1] * two
+        mixed_ref[:, pl.ds(spot, tokens)] = (total[2 * channels :] * conv).astype(jnp.bfloat16)
+
+
+def after_kernel(spot_ref, *refs):
+    mixed, own_ref, other_ref, twin_ref = refs[:2], *refs[2:5]
+    whole_ref, after_ref, kept_ref, full_ref, weight_ref = refs[5:]
+    channels, tokens = mixed[0].shape[1:]
+    width = weight_ref.shape[0] // 16
+
+    @pl.when(pl.program_id(0) == 0)
+    def _():
+        for piece in range(4):
+            for dy in range(2):
+                block = feature_block(spot_ref, piece, dy)
+                for dr in range(2):
+                    start = pl.multiple_of((block * 2 + (spot_ref[0] ^ dr)) * width, width)
+                    for dx in range(2):
+                        part = (own_ref, other_ref)[dx][dy, piece]
+                        if dr:
+                            part = twin_ref[dx, dy, piece]
+                        place = slice(dx * 2 * width, (dx + 1) * 2 * width)
+                        weight_ref[pl.ds(start, width), place] = part
+
+    squares = jnp.zeros((1, tokens), jnp.float32)
+    for dr in range(2):
+        for index in range(4):
+            block = mixed[dr][index]
+            spot = channels_of(spot_ref, (index & 1) * 2 + dr)
+            spot = ((index >> 1) * 4 + spot) * channels
+            full_ref[pl.ds(pl.multiple_of(spot, channels), channels), :] = block
+            floats = block.astype(jnp.float32)
+            squares = squares + jnp.sum(floats * floats, axis=0, keepdims=True)
+    scale = lax.rsqrt(squares / (8 * channels) + epsilon)
+    part = jnp.dot(weight_ref[...], full_ref[...], preferred_element_type=jnp.float32)
+    total = whole_ref[...].astype(jnp.float32) + part * scale
+    after_ref[...] = total.astype(jnp.bfloat16)
+
+    @pl.when(pl.program_id(0) == tile_of(spot_ref, 0))
+    def _():
+        half = kept_ref.shape[0]
+        start = pl.multiple_of(spot_ref[4] * half, half)
+        kept_ref[...] = after_ref[pl.ds(start, half), :]
+
+
+def norm_scale(rows):
+    floats = rows.astype(jnp.float32)
+    squares = jnp.sum(floats * floats, axis=0, keepdims=True)
+    return lax.rsqrt(squares / rows.shape[0] + epsilon)
+
+
+def gate_kernel(spot_ref, *refs):
+    pieces, after_ref, active_ref, gate_ref = refs[:8], *refs[8:]
+
+    @pl.when(pl.program_id(0) == 0)
+    def _():
+        for index in range(8):
+            lay_out(spot_ref, index, pieces[index][...], gate_ref)
+
+    rows = after_ref[...]
+    gate = jnp.dot(gate_ref[...], rows, preferred_element_type=jnp.float32) * norm_scale(rows)
+    active_ref[...] = gate / (1.0 + jnp.exp(-gate))
+
+
+def hidden_kernel(spot_ref, *refs):
+    pieces, after_ref, active_ref, hidden_ref, up_ref = refs[:8], *refs[8:]
+
+    @pl.when(pl.program_id(0) == 0)
+    def _():
+        for index in range(8):
+            lay_out(spot_ref, index, pieces[index][...], up_ref)
+
+    rows = after_ref[...]
+    upper = jnp.dot(up_ref[...], rows, preferred_element_type=jnp.float32) * norm_scale(rows)
+    hidden_ref[...] = (active_ref[...] * upper).astype(jnp.bfloat16)
+
+
+def down_kernel(spot_ref, *refs):
+    pieces, hidden_ref, outs, full_ref = refs[:8], refs[8], refs[9:11], refs[11]
+    half, tokens = outs[0].shape[1:]
+    for index in range(8):
+        lay_out(spot_ref, index, pieces[index][...], full_ref)
+    for dr in (1, 0):
+        for dl in range(2):
+            spot = pl.multiple_of(tile_of(spot_ref, dl * 2 + dr) * tokens, tokens)
+            hidden = hidden_ref[:, pl.ds(spot, tokens)]
+            for dx in range(2):
+                start = pl.multiple_of((spot_ref[4] ^ dx) * half, half)
+                part = lax.dot_general(
+                    full_ref[:, pl.ds(start, half)],
+                    hidden,
+                    (((0,), (0,)), ((), ())),
+                    preferred_element_type=jnp.float32,
+                )
+                outs[dr][dx * 2 + dl] = part.astype(jnp.bfloat16)
+
+
+def shaped(*shape):
+    return jax.ShapeDtypeStruct(shape, jnp.bfloat16)
+
+
+def whole_blocks(count):
+    return [pl.BlockSpec(memory_space=pltpu.VMEM)] * count
+
+
+def exchanged(
+    residual,
+    mixer_gain,
+    value_weight,
+    value_scale,
+    input_gate_weight,
+    input_gate_scale,
+    output_gate_weight,
+    output_gate_scale,
+    conv_taps,
+    conv_gain,
+    mixer_out_weight,
+    mixer_out_scale,
+    channel_gain,
+    gate_weight,
+    gate_scale,
+    up_weight,
+    up_scale,
+    down_weight,
+    down_scale,
+):
+    axes = ("rep", "zh", "zl", "y", "tp")
+    spots = jnp.stack([lax.axis_index(axis) for axis in axes]).astype(jnp.int32)
+    half, tokens = residual.shape
+    depth = gate_weight.shape[0]
+    lanes = depth // 2
+    features = 2 * half
+    channels = value_weight.shape[1] // 4
+    units = gate_weight.shape[1] // 4
+    scalars = pl.BlockSpec(memory_space=pltpu.SMEM)
+    tile = lambda shape: pl.BlockSpec(shape, lambda i: (0,) * (len(shape) - 1) + (i,))
+    fixed = lambda shape: pl.BlockSpec(shape, lambda i: (0,) * len(shape))
+
+    def by_lane(array):
+        return array.reshape(-1, lanes)
+
+    def prepare(kernel, operands, half_columns, half_rows, outs, scratch):
+        def block(operand):
+            if any(operand is weight for weight in half_columns):
+                shape = (operand.shape[0], operand.shape[1] // 2)
+                return pl.BlockSpec(shape, lambda i, spot_ref: (0, spot_ref[0]))
+            if any(operand is weight for weight in half_rows):
+                shape = (operand.shape[0] // 2, operand.shape[1])
+                return pl.BlockSpec(shape, lambda i, spot_ref: (spot_ref[0], 0))
+            return pl.BlockSpec(operand.shape, lambda i, spot_ref: (0, 0))
+
+        return pl.pallas_call(
+            kernel,
+            out_shape=tuple(shaped(*shape) for shape in outs),
+            grid_spec=pltpu.PrefetchScalarGridSpec(
+                num_scalar_prefetch=1,
+                grid=(1,),
+                in_specs=[block(operand) for operand in operands],
+                out_specs=tuple(pl.BlockSpec(shape, lambda i, spot_ref: (0, 0)) for shape in outs),
+                scratch_shapes=scratch,
+            ),
+        )(spots, *operands)
+
+    def run(kernel, operands, in_specs, outs, out_specs, scratch, grid=(4,)):
+        return pl.pallas_call(
+            kernel,
+            grid=grid,
+            out_shape=outs,
+            in_specs=[scalars] + in_specs,
+            out_specs=out_specs,
+            scratch_shapes=scratch,
+        )(spots, *operands)
+
+    def over_z(mine, other):
+        return [mine, flip(other, "zl"), flip(mine, "zh"), flip(other, "zh", "zl")]
+
+    def over_y(pieces):
+        return pieces + [flip(piece, "y") for piece in pieces]
+
+    rows_zl = flip(residual, "zl")
+    rows_tp = flip(residual, "tp")
+    rows_both = flip(rows_zl, "tp")
+    rows = []
+    for block in (residual, rows_zl, rows_tp, rows_both):
+        rows = rows + [block, flip(block, "rep")]
+
+    small = (value_weight, input_gate_weight, output_gate_weight)
+    mine, other = prepare(
+        small_kernel,
+        small
+        + (by_lane(value_scale), by_lane(input_gate_scale), by_lane(output_gate_scale))
+        + (by_lane(mixer_gain), mixer_out_weight, by_lane(conv_gain), by_lane(mixer_out_scale)),
+        small + (mixer_out_weight,),
+        (),
+        [(3 * channels + lanes, depth)] * 2,
+        [pltpu.VMEM((lanes, depth), jnp.bfloat16)],
+    )
+    small_pieces = over_z(mine, other)
+
+    pair = (gate_weight, up_weight)
+    pairs = prepare(
+        pair_kernel,
+        pair + (by_lane(gate_scale), by_lane(up_scale), by_lane(channel_gain)),
+        pair,
+        (),
+        [(units, depth)] * 4,
+        [pltpu.VMEM((2 * units, depth), jnp.bfloat16)],
+    )
+    gates = over_y(over_z(pairs[0], pairs[1]))
+    ups = over_y(over_z(pairs[2], pairs[3]))
+    downs = prepare(
+        last_kernel,
+        (down_weight, by_lane(down_scale)),
+        (),
+        (down_weight,),
+        [(units, lanes)] * 4,
+        [],
+    )
+    lasts = over_y(over_z(downs[0], downs[1]))
+    lasts = lasts + over_y(over_z(downs[2], downs[3]))
+    small_pieces, _ = lax.optimization_barrier((small_pieces, downs[0]))
+
+    places = [lanes * (piece & 1) for piece in range(4)]
+    projections = jnp.stack(
+        [block[place : place + 3 * channels] for block, place in zip(small_pieces, places)]
+    )
+    other_projections = flip(projections, "y")
+    places = [3 * channels * (1 - (piece & 1)) for piece in range(4)]
+    own_out = jnp.stack([block[place : place + lanes] for block, place in zip(small_pieces, places)])
+    same_out = flip(own_out, "y")
+    place = (lax.axis_index("rep") * 2 + lax.axis_index("zl")) * channels
+    own_taps = lax.dynamic_slice_in_dim(conv_taps, place, channels, 1).T
+    mixed, whole = run(
+        mix_kernel,
+        rows[:4] + rows[4:] + [projections, other_projections, own_taps],
+        whole_blocks(11),
+        (shaped(channels, 4 * tokens), shaped(features, 4 * tokens)),
+        tuple(whole_blocks(2)),
+        [pltpu.VMEM((3 * channels, features), jnp.bfloat16)],
+        grid=(),
+    )
+    same_out, mixed = lax.optimization_barrier((same_out, mixed))
+    out_blocks = jnp.stack([own_out, same_out])
+    out_other = flip(out_blocks, "tp")
+    out_twin = flip(jnp.stack([out_blocks, out_other]), "rep")
+    mixes = jnp.stack([mixed, flip(mixed, "zl"), flip(mixed, "tp"), flip(mixed, "zl", "tp")])
+    twin_mixes = flip(mixes, "rep")
+    after, after_own = run(
+        after_kernel,
+        [mixes, twin_mixes, out_blocks, out_other, out_twin, whole],
+        [tile((4, channels, tokens))] * 2
+        + [fixed(block.shape) for block in (out_blocks, out_other, out_twin)]
+        + [tile((features, tokens))],
+        (shaped(features, 4 * tokens), shaped(half, tokens)),
+        (tile((features, tokens)), fixed((half, tokens))),
+        [
+            pltpu.VMEM((8 * channels, tokens), jnp.bfloat16),
+            pltpu.VMEM((features, 8 * channels), jnp.bfloat16),
+        ],
+    )
+
+    blocks = [fixed((units, depth))] * 8 + [tile((features, tokens))]
+    scratch = [pltpu.VMEM((units, features), jnp.bfloat16)]
+    active = run(
+        gate_kernel,
+        gates + [after],
+        blocks,
+        jax.ShapeDtypeStruct((units, 4 * tokens), jnp.float32),
+        tile((units, tokens)),
+        scratch,
+    )
+    hidden = run(
+        hidden_kernel,
+        ups + [after, active],
+        blocks + [tile((units, tokens))],
+        shaped(units, 4 * tokens),
+        tile((units, tokens)),
+        scratch,
+    )
+    totals = []
+    for chunk in range(2):
+        kept, sent = run(
+            down_kernel,
+            lasts[8 * chunk :][:8] + [hidden],
+            whole_blocks(9),
+            (shaped(4, half // 2, tokens),) * 2,
+            tuple(whole_blocks(2)),
+            [pltpu.VMEM((units, half), jnp.bfloat16)],
+            grid=(),
+        )
+        got = flip(sent, "rep")
+        sums = kept.astype(jnp.float32) + got.astype(jnp.float32)
+        own = after_own.reshape(-1, 2, lanes, tokens)[:, chunk].reshape(-1, tokens)
+        total = own.astype(jnp.float32) + sums[0]
+        for index, way in ((3, ("zl", "tp")), (2, ("tp",)), (1, ("zl",))):
+            part = flip(sums[index].astype(jnp.bfloat16), *way)
+            total = total + part.astype(jnp.float32)
+        totals.append(total.astype(jnp.bfloat16).reshape(-1, lanes, tokens))
+    return jnp.stack(totals, axis=1).reshape(half, tokens)
+
+
 def solution(mesh):
+    sizes = dict(mesh.shape)
+    if sizes == {"rep": 2, "fs": 8, "tp": 2}:
+        grid = Mesh(mesh.devices.reshape(2, 2, 2, 2, 2), ("rep", "zh", "zl", "y", "tp"))
+        fs, step = ("zh", "zl", "y"), exchanged
+    else:
+        grid, fs, step = mesh, ("fs",), gathered
+    own = P("tp", ("rep",) + fs)
     placed = (
-        P("tp", ("rep", "fs")),
+        own,
         P(),
-        P("fs", "tp"),
+        P(fs, "tp"),
         P("tp"),
-        P("fs", "tp"),
+        P(fs, "tp"),
         P("tp"),
-        P("fs", "tp"),
+        P(fs, "tp"),
         P("tp"),
         P(None, "tp"),
         P("tp"),
-        P("tp", "fs"),
-        P("fs"),
+        P("tp", fs),
+        P(fs),
         P(),
-        P("fs", "tp"),
+        P(fs, "tp"),
         P("tp"),
-        P("fs", "tp"),
+        P(fs, "tp"),
         P("tp"),
-        P("tp", "fs"),
-        P("fs"),
-    )
-    return jax.shard_map(
-        local, mesh=mesh, in_specs=placed, out_specs=P("tp", ("rep", "fs")), check_vma=False
-    )
+        P("tp", fs),
+        P(fs),
+    )
+    step = jax.shard_map(step, mesh=grid, in_specs=placed, out_specs=own, check_vma=False)
+    return step

time: 770 us -> 268 us (0.35)
  waiting for transfers between devices: 646 us -> 133 us
  starting transfers between devices: 3.98 us -> 77.1 us
  blocking collectives: 51.2 us -> 0 us
  Pallas kernels: 0 us -> 50.2 us
  matrix products: 31.9 us -> 0 us
  other arithmetic: 17 us -> 2.18 us
  between operations: 13.7 us -> 0.53 us
    all_gather x9 -> x0, waiting for transfers between devices: 627 us -> none  [the longest x1 164 us: local(): lax.all_gather(down_weight.astype(jnp.bfloat16), 'fs', axis=1, tiled=True)]
    ppermute x0 -> x54, waiting for transfers between devices: none -> 133 us  [flip(): return lax.ppermute(array, axes, [(i, count - 1 - i) for i in range(count)])]
    ppermute x0 -> x54, starting transfers between devices: none -> 77.1 us  [flip(): return lax.ppermute(array, axes, [(i, count - 1 - i) for i in range(count)])]
    pallas_call x0 -> x9, Pallas kernels: none -> 50.2 us  [the longest x6 40.2 us: run(): pl.pallas_call(kernel, grid=grid, out_shape=outs, in_specs=[scalars] + in...]
    all_gather x3 -> x0, blocking collectives: 46.3 us -> none  [the longest x1 22.3 us: local(): lax.all_gather(mixer_out_scale, 'fs', axis=0, tiled=True)]
    dot_general x6 -> x0, matrix products: 31.9 us -> none  [the longest x5 31.4 us: contract(): lax.dot_general(weight, rows, (((0,), (0,)), ((), ())), preferred_element...]
    reduce_scatter x1 -> x0, waiting for transfers between devices: 18.7 us -> none  [local(): lax.psum_scatter((contract(down_full, hidden) * down_scale_full[:, None])...]
    convert_element_type x9 -> x2, other arithmetic: 13.9 us -> 0.38 us  [exchanged(): totals.append(total.astype(jnp.bfloat16).reshape(-1, lanes, tokens))]
  transfers between devices with their start and end apart: 11 -> 54, of which waited for: 8 -> 24; matrix products, arithmetic and copies ran while one was open for 5% -> 2% of each run, Pallas kernels for 0% -> 17%
where the time goes in v1:
time: 268 us; the launch traced here: 267 us
  waiting for transfers between devices  133 us (50%)
  starting transfers between devices  77.1 us (29%)
  Pallas kernels  50.2 us (19%)
  local copies, waits for them, and re-layouts  4.72 us (2%)
    ppermute x54, waiting for transfers between devices, flip(): return lax.ppermute(array, axes, [(i, count - 1 - i) for i in range(count)])  133 us
    ppermute x54, starting transfers between devices, flip(): return lax.ppermute(array, axes, [(i, count - 1 - i) for i in range(count)])  77.1 us
    pallas_call x6, Pallas kernels, run(): pl.pallas_call(kernel, grid=grid, out_shape=outs, in_specs=[scalars] + in...  40.2 us
    pallas_call x3, Pallas kernels, prepare(): pl.pallas_call(kernel, out_shape=tuple((shaped(*shape) for shape in outs)...  9.98 us
  transfers between devices with their start and end apart: 54, of which 24 were waited for; matrix products, arithmetic and copies ran while one was open for 2% of the time, Pallas kernels for 17%

profile of v1, /device:TPU:0, one launch (start us, length us, event | category | flops | bytes accessed | tf_op | source)
XLA Modules:
  0.0 267.4 jit_solution(4595498412440586640)
XLA Ops:
  0.0 3.1 %collective-permute-start.5 = (bf16[1024,256]{1,0:T(8,128)(2,1)}, bf16[1024,256]{1,0:T(8,128)(2,1)S(1)}, u32[]{:S(2)}, u32[]{:S(2)}) collective-permute-start(bf16[1024,256]{1,0:T(8,128)(2,1)} %refs_0_.4), channel_id=1, source_target_pairs={{0,4},{4,0},{1,5},{5,1},{2,6},{6,2},{3,7},{7,3},{8,12},{12,8},{9,1... | collective-permute-start | bytes 1572872 | tf_op jit(solution)/shard_map/ppermute | solution.py:123
  3.7 2.7 %shard_map.181 = (bf16[320,256]{1,0:T(8,128)(2,1)}, bf16[320,256]{1,0:T(8,128)(2,1)}) custom-call(s32[5]{0:T(128)} %stack.89.spot_ref, f32[256,256]{1,0:T(8,128)} %refs_0_.3, f32[256,256]{1,0:T(8,128)} %refs_1_.2, f32[256,256]{1,0:T(8,128)} %refs_2_.1, f32[2,128]{1,0:T(2,128)} %bitcast.106, f32[2,128]{1,0:T(2,128)} %bitcast.107, f32[2,128]{1,0:T(2,128)} %bitcast.108, ...), custom_call_target="tpu_custom_call" | custom-call | tf_op jit(solution)/shard_map/pallas_call | solution.py:385
  6.4 3.0 %collective-permute-start.1 = (bf16[320,256]{1,0:T(8,128)(2,1)}, bf16[320,256]{1,0:T(8,128)(2,1)S(1)}, u32[]{:S(2)}, u32[]{:S(2)}) collective-permute-start(bf16[320,256]{1,0:T(8,128)(2,1)} %get-tuple-element.32), channel_id=1, source_target_pairs={{0,8},{8,0},{1,9},{9,1},{2,10},{10,2},{3,11},{11,3},{4,12},{12,4},... | collective-permute-start | bytes 491528 | tf_op jit(solution)/shard_map/ppermute | solution.py:123
  9.4 1.3 collective-permute-start.2
  10.8 1.5 collective-permute-start.7
  12.3 3.0 %shard_map.182 = (bf16[704,128]{1,0:T(8,128)(2,1)}, bf16[704,128]{1,0:T(8,128)(2,1)}, bf16[704,128]{1,0:T(8,128)(2,1)}, bf16[704,128]{1,0:T(8,128)(2,1)}) custom-call(s32[5]{0:T(128)} %stack.89.spot_ref, f32[2816,256]{1,0:T(8,128)} %weight_ref.1, f32[2,128]{1,0:T(2,128)} %bitcast.111), custom_call_target="tpu_custom_call" | custom-call | tf_op jit(solution)/shard_map/pallas_call | solution.py:385
  15.3 7.0 %collective-permute-done = bf16[320,256]{1,0:T(8,128)(2,1)S(1)} collective-permute-done((bf16[320,256]{1,0:T(8,128)(2,1)}, bf16[320,256]{1,0:T(8,128)(2,1)S(1)}, u32[]{:S(2)}, u32[]{:S(2)}) %collective-permute-start) | collective-permute-done | bytes 163872 | tf_op jit(solution)/shard_map/ppermute | solution.py:123
  22.7 5.2 %collective-permute-done.2 = bf16[320,256]{1,0:T(8,128)(2,1)S(1)} collective-permute-done((bf16[320,256]{1,0:T(8,128)(2,1)}, bf16[320,256]{1,0:T(8,128)(2,1)S(1)}, u32[]{:S(2)}, u32[]{:S(2)}) %collective-permute-start.2) | collective-permute-done | bytes 163872 | tf_op jit(solution)/shard_map/ppermute | solution.py:123
  28.6 1.5 collective-permute-start.9
  30.2 1.6 collective-permute-start.11
  31.8 0.9 slice_bitcast_fusion.12
  33.2 8.2 %collective-permute-done.9.refs_6_ = bf16[1024,256]{1,0:T(8,128)(2,1)S(1)} collective-permute-done((bf16[1024,256]{1,0:T(8,128)(2,1)S(1)}, bf16[1024,256]{1,0:T(8,128)(2,1)S(1)}, u32[]{:S(2)}, u32[]{:S(2)}) %collective-permute-start.9) | collective-permute-done | bytes 524320 | tf_op jit(solution)/shard_map/ppermute | solution.py:123
  41.4 0.9 fusion.13
  42.3 1.5 collective-permute-start.3
  43.9 0.7 copy.24
  44.7 5.8 %shard_map.183 = (bf16[64,1024]{1,0:T(8,128)(2,1)}, bf16[2048,1024]{1,0:T(8,128)(2,1)}) custom-call(s32[5]{0:T(128)} %stack.89.spot_ref, bf16[1024,256]{1,0:T(8,128)(2,1)} %refs_0_.4, bf16[1024,256]{1,0:T(8,128)(2,1)} %copy-done.12, bf16[1024,256]{1,0:T(8,128)(2,1)} %copy-done.10, bf16[1024,256]{1,0:T(8,128)(2,1)} %collective-permute-done.6.refs_3_, ...), custom_call_target="tpu_custom_call" | custom-call | tf_op jit(solution)/shard_map/pallas_call | solution.py:398
  51.2 1.6 collective-permute-start.16
  52.8 3.7 %collective-permute-start.18 = (bf16[704,128]{1,0:T(8,128)(2,1)S(1)}, bf16[704,128]{1,0:T(8,128)(2,1)S(1)}, u32[]{:S(2)}, u32[]{:S(2)}) collective-permute-start(bf16[704,128]{1,0:T(8,128)(2,1)S(1)} %copy-done.40), channel_id=1, source_target_pairs={{0,4},{4,0},{1,5},{5,1},{2,6},{6,2},{3,7},{7,3},{8,12},{12,8},{9,1... | collective-permute-start | bytes 540680 | tf_op jit(solution)/shard_map/ppermute | solution.py:123
  56.4 4.2 %shard_map.185 = (bf16[704,256]{1,0:T(8,128)(2,1)}, bf16[704,256]{1,0:T(8,128)(2,1)}, bf16[704,256]{1,0:T(8,128)(2,1)}, bf16[704,256]{1,0:T(8,128)(2,1)}) custom-call(s32[5]{0:T(128)} %stack.89.spot_ref, f32[256,2816]{1,0:T(8,128)} %refs_0_.5, f32[256,2816]{1,0:T(8,128)} %refs_1_.3, f32[22,128]{1,0:T(8,128)} %bitcast.102, f32[22,128]{1,0:T(8,128)} %bitcast.103, ...), custom_call_target="tpu_custom_call" | custom-call | tf_op jit(solution)/shard_map/pallas_call | solution.py:385
  60.8 1.2 collective-permute-start.32
  62.0 2.2 collective-permute-done.19.refs_2_
  64.2 6.6 %collective-permute-start.20 = (bf16[704,128]{1,0:T(8,128)(2,1)S(1)}, bf16[704,128]{1,0:T(8,128)(2,1)}, u32[]{:S(2)}, u32[]{:S(2)}) collective-permute-start(bf16[704,128]{1,0:T(8,128)(2,1)S(1)} %copy-done.40), channel_id=1, source_target_pairs={{0,12},{4,8},{8,4},{12,0},{1,13},{5,9},{9,5},{13,1},{2,14},{6,10},... | collective-permute-start | bytes 540680 | tf_op jit(solution)/shard_map/ppermute | solution.py:123
  70.9 13.6 %collective-permute-done.20.refs_3_ = bf16[704,128]{1,0:T(8,128)(2,1)} collective-permute-done((bf16[704,128]{1,0:T(8,128)(2,1)S(1)}, bf16[704,128]{1,0:T(8,128)(2,1)}, u32[]{:S(2)}, u32[]{:S(2)}) %collective-permute-start.20) | collective-permute-done | bytes 180256 | tf_op jit(solution)/shard_map/ppermute | solution.py:123
  84.4 1.5 collective-permute-start.35
  85.9 10.5 %collective-permute-start.26 = (bf16[704,256]{1,0:T(8,128)(2,1)}, bf16[704,256]{1,0:T(8,128)(2,1)S(1)}, u32[]{:S(2)}, u32[]{:S(2)}) collective-permute-start(bf16[704,256]{1,0:T(8,128)(2,1)} %get-tuple-element.42.refs_0_), channel_id=1, source_target_pairs={{0,8},{8,0},{1,9},{9,1},{2,10},{10,2},{3,11},{11,3},{4,12},{12,4},... | collective-permute-start | bytes 1081352 | tf_op jit(solution)/shard_map/ppermute | solution.py:123
  96.4 0.7 collective-permute-start.25
  97.1 2.4 collective-permute-start.27
  100.3 25.4 %collective-permute-done.26.refs_2_ = bf16[704,256]{1,0:T(8,128)(2,1)S(1)} collective-permute-done((bf16[704,256]{1,0:T(8,128)(2,1)}, bf16[704,256]{1,0:T(8,128)(2,1)S(1)}, u32[]{:S(2)}, u32[]{:S(2)}) %collective-permute-start.26) | collective-permute-done | bytes 360480 | tf_op jit(solution)/shard_map/ppermute | solution.py:123
  126.3 7.2 %collective-permute-start.14 = (bf16[64,1024]{1,0:T(8,128)(2,1)S(1)}, bf16[64,1024]{1,0:T(8,128)(2,1)S(1)}, u32[]{:S(2)}, u32[]{:S(2)}) collective-permute-start(bf16[64,1024]{1,0:T(8,128)(2,1)S(1)} %copy-done.39), channel_id=1, source_target_pairs={{0,5},{1,4},{4,1},{5,0},{2,7},{3,6},{6,3},{7,2},{8,13},{9,12},{12,... | collective-permute-start | bytes 393224 | tf_op jit(solution)/shard_map/ppermute | solution.py:123
  133.5 1.5 collective-permute-start.37
  135.5 1.2 collective-permute-done.14
  136.7 1.5 collective-permute-start.38
  138.4 6.4 %collective-permute-done.37.refs_6_ = bf16[704,256]{1,0:T(8,128)(2,1)S(1)} collective-permute-done((bf16[704,256]{1,0:T(8,128)(2,1)S(1)}, bf16[704,256]{1,0:T(8,128)(2,1)S(1)}, u32[]{:S(2)}, u32[]{:S(2)}) %collective-permute-start.37) | collective-permute-done | bytes 360480 | tf_op jit(solution)/shard_map/ppermute | solution.py:123
  144.8 1.5 collective-permute-start.30
  146.3 6.2 %collective-permute-done.36.refs_5_ = bf16[704,256]{1,0:T(8,128)(2,1)S(1)} collective-permute-done((bf16[704,256]{1,0:T(8,128)(2,1)S(1)}, bf16[704,256]{1,0:T(8,128)(2,1)S(1)}, u32[]{:S(2)}, u32[]{:S(2)}) %collective-permute-start.36) | collective-permute-done | bytes 360480 | tf_op jit(solution)/shard_map/ppermute | solution.py:123
  152.5 1.5 collective-permute-start.29
  154.0 6.2 %collective-permute-done.38.refs_7_ = bf16[704,256]{1,0:T(8,128)(2,1)S(1)} collective-permute-done((bf16[704,256]{1,0:T(8,128)(2,1)S(1)}, bf16[704,256]{1,0:T(8,128)(2,1)S(1)}, u32[]{:S(2)}, u32[]{:S(2)}) %collective-permute-start.38) | collective-permute-done | bytes 360480 | tf_op jit(solution)/shard_map/ppermute | solution.py:123
  160.2 1.5 collective-permute-start.31
  161.8 6.2 %collective-permute-done.30.refs_6_ = bf16[704,256]{1,0:T(8,128)(2,1)S(1)} collective-permute-done((bf16[704,256]{1,0:T(8,128)(2,1)S(1)}, bf16[704,256]{1,0:T(8,128)(2,1)S(1)}, u32[]{:S(2)}, u32[]{:S(2)}) %collective-permute-start.30) | collective-permute-done | bytes 360480 | tf_op jit(solution)/shard_map/ppermute | solution.py:123
  168.0 1.5 collective-permute-start.21
  169.5 6.2 %collective-permute-done.29.refs_5_ = bf16[704,256]{1,0:T(8,128)(2,1)S(1)} collective-permute-done((bf16[704,256]{1,0:T(8,128)(2,1)S(1)}, bf16[704,256]{1,0:T(8,128)(2,1)S(1)}, u32[]{:S(2)}, u32[]{:S(2)}) %collective-permute-start.29) | collective-permute-done | bytes 360480 | tf_op jit(solution)/shard_map/ppermute | solution.py:123
  175.7 1.5 collective-permute-start.23
  177.7 1.6 collective-permute-start.24
  179.4 7.8 %shard_map.184 = (bf16[2048,1024]{1,0:T(8,128)(2,1)}, bf16[1024,256]{1,0:T(8,128)(2,1)}) custom-call(s32[5]{0:T(128)} %stack.89.spot_ref, bf16[4,64,1024]{2,1,0:T(8,128)(2,1)} %copy-done.2, bf16[4,64,1024]{2,1,0:T(8,128)(2,1)} %copy-done.14, bf16[2,4,128,256]{3,2,1,0:T(8,128)(2,1)} %copy-done.1, bf16[2,4,128,256]{3,2,1,0:T(8,128)(2,1)} %copy-done.3, ...), custom_call_target="tpu_custom_call" | custom-call | tf_op jit(solution)/shard_map/pallas_call | solution.py:398
  187.2 7.9 %shard_map.186.refs_9_ = f32[704,1024]{1,0:T(8,128)} custom-call(s32[5]{0:T(128)} %stack.89.spot_ref, bf16[704,256]{1,0:T(8,128)(2,1)} %get-tuple-element.45.refs_0_, bf16[704,256]{1,0:T(8,128)(2,1)} %copy-done.17, bf16[704,256]{1,0:T(8,128)(2,1)} %copy-done.16, bf16[704,256]{1,0:T(8,128)(2,1)} %copy-done.18, bf16[704,256]{1,0:T(8,128)(2,1)} %copy-done.20, ...), custom_call_target="tpu_custom_call" | custom-call | tf_op jit(solution)/shard_map/pallas_call | solution.py:398
  195.1 8.1 %shard_map.187.refs_8_ = bf16[704,1024]{1,0:T(8,128)(2,1)} custom-call(s32[5]{0:T(128)} %stack.89.spot_ref, bf16[704,256]{1,0:T(8,128)(2,1)} %get-tuple-element.42.refs_0_, bf16[704,256]{1,0:T(8,128)(2,1)} %copy-done.21, bf16[704,256]{1,0:T(8,128)(2,1)} %copy-done.19, bf16[704,256]{1,0:T(8,128)(2,1)} %collective-permute-done.27.refs_3_, ...), custom_call_target="tpu_custom_call" | custom-call | tf_op jit(solution)/shard_map/pallas_call | solution.py:398
  203.2 5.4 %shard_map.188 = (bf16[4,512,256]{2,1,0:T(8,128)(2,1)}, bf16[4,512,256]{2,1,0:T(8,128)(2,1)}) custom-call(s32[5]{0:T(128)} %stack.89.spot_ref, bf16[704,128]{1,0:T(8,128)(2,1)} %get-tuple-element.31.refs_0_, bf16[704,128]{1,0:T(8,128)(2,1)} %copy-done.30, bf16[704,128]{1,0:T(8,128)(2,1)} %copy-done.29, bf16[704,128]{1,0:T(8,128)(2,1)} %collective-permute-done.20.refs_3_, ...), custom_call_target="tpu_custom_call" | custom-call | tf_op jit(solution)/shard_map/pallas_call | solution.py:398
  208.8 1.7 collective-permute-start.43
  210.5 2.6 collective-permute-start.45
  213.7 6.7 %collective-permute-done.44.refs_2_ = bf16[704,128]{1,0:T(8,128)(2,1)S(1)} collective-permute-done((bf16[704,128]{1,0:T(8,128)(2,1)S(1)}, bf16[704,128]{1,0:T(8,128)(2,1)S(1)}, u32[]{:S(2)}, u32[]{:S(2)}) %collective-permute-start.44) | collective-permute-done | bytes 180256 | tf_op jit(solution)/shard_map/ppermute | solution.py:123
  221.1 1.4 collective-permute-start.47
  222.5 1.4 collective-permute-done.45.refs_3_
  224.5 3.4 %collective-permute-done.48.refs_6_ = bf16[704,128]{1,0:T(8,128)(2,1)S(1)} collective-permute-done((bf16[704,128]{1,0:T(8,128)(2,1)S(1)}, bf16[704,128]{1,0:T(8,128)(2,1)S(1)}, u32[]{:S(2)}, u32[]{:S(2)}) %collective-permute-start.48) | collective-permute-done | bytes 180256 | tf_op jit(solution)/shard_map/ppermute | solution.py:123
  227.9 3.9 %collective-permute-done.47.refs_5_ = bf16[704,128]{1,0:T(8,128)(2,1)S(1)} collective-permute-done((bf16[704,128]{1,0:T(8,128)(2,1)S(1)}, bf16[704,128]{1,0:T(8,128)(2,1)S(1)}, u32[]{:S(2)}, u32[]{:S(2)}) %collective-permute-start.47) | collective-permute-done | bytes 180256 | tf_op jit(solution)/shard_map/ppermute | solution.py:123
  232.4 2.3 collective-permute-done.49.refs_7_
  234.7 5.3 %shard_map.189 = (bf16[4,512,256]{2,1,0:T(8,128)(2,1)}, bf16[4,512,256]{2,1,0:T(8,128)(2,1)}) custom-call(s32[5]{0:T(128)} %stack.89.spot_ref, bf16[704,128]{1,0:T(8,128)(2,1)} %get-tuple-element.49.refs_0_, bf16[704,128]{1,0:T(8,128)(2,1)} %copy-done.32, bf16[704,128]{1,0:T(8,128)(2,1)} %copy-done.31, bf16[704,128]{1,0:T(8,128)(2,1)} %copy-done.33, ...), custom_call_target="tpu_custom_call" | custom-call | tf_op jit(solution)/shard_map/pallas_call | solution.py:398
  240.7 1.4 collective-permute-start.41
  242.1 1.9 collective-permute-start.42
  244.6 1.4 collective-permute-start.52
  246.0 4.6 %collective-permute-done.40 = bf16[512,256]{1,0:T(8,128)(2,1)S(1)} collective-permute-done((bf16[512,256]{1,0:T(8,128)(2,1)S(1)}, bf16[512,256]{1,0:T(8,128)(2,1)S(1)}, u32[]{:S(2)}, u32[]{:S(2)}) %collective-permute-start.40) | collective-permute-done | bytes 262176 | tf_op jit(solution)/shard_map/ppermute | solution.py:123
  250.8 4.9 %collective-permute-done.41 = bf16[512,256]{1,0:T(8,128)(2,1)S(1)} collective-permute-done((bf16[512,256]{1,0:T(8,128)(2,1)S(1)}, bf16[512,256]{1,0:T(8,128)(2,1)S(1)}, u32[]{:S(2)}, u32[]{:S(2)}) %collective-permute-start.41) | collective-permute-done | bytes 262176 | tf_op jit(solution)/shard_map/ppermute | solution.py:123
  255.8 6.1 %collective-permute-done.51 = bf16[512,256]{1,0:T(8,128)(2,1)S(1)} collective-permute-done((bf16[512,256]{1,0:T(8,128)(2,1)S(1)}, bf16[512,256]{1,0:T(8,128)(2,1)S(1)}, u32[]{:S(2)}, u32[]{:S(2)}) %collective-permute-start.51) | collective-permute-done | bytes 262176 | tf_op jit(solution)/shard_map/ppermute | solution.py:123
  261.9 4.2 %collective-permute-done.52 = bf16[512,256]{1,0:T(8,128)(2,1)S(1)} collective-permute-done((bf16[512,256]{1,0:T(8,128)(2,1)S(1)}, bf16[512,256]{1,0:T(8,128)(2,1)S(1)}, u32[]{:S(2)}, u32[]{:S(2)}) %collective-permute-start.52) | collective-permute-done | bytes 262176 | tf_op jit(solution)/shard_map/ppermute | solution.py:123
  266.5 0.8 copy.23
  (156 shorter events, 10.6 us)
Async XLA Ops:
  0.0 28.6 %collective-permute-start.5 = (bf16[1024,256]{1,0:T(8,128)(2,1)}, bf16[1024,256]{1,0:T(8,128)(2,1)S(1)}, u32[]{:S(2)}, u32[]{:S(2)}) collective-permute-start(bf16[1024,256]{1,0:T(8,128)(2,1)} %refs_0_.4), channel_id=1, source_target_pairs={{0,4},{4,0},{1,5},{5,1},{2,6},{6,2},{3,7},{7,3},{8,12},{12,8},{9,1... | collective-permute-start | bytes 1572872 | tf_op jit(solution)/shard_map/ppermute | solution.py:123
  6.4 15.8 %collective-permute-start = (bf16[320,256]{1,0:T(8,128)(2,1)}, bf16[320,256]{1,0:T(8,128)(2,1)S(1)}, u32[]{:S(2)}, u32[]{:S(2)}) collective-permute-start(bf16[320,256]{1,0:T(8,128)(2,1)} %get-tuple-element.30), channel_id=1, source_target_pairs={{0,4},{4,0},{1,5},{5,1},{2,6},{6,2},{3,7},{7,3},{8,12},{12,8},{9,1... | collective-permute-start | bytes 491528 | tf_op jit(solution)/shard_map/ppermute | solution.py:123
  6.4 16.3 %collective-permute-start.1 = (bf16[320,256]{1,0:T(8,128)(2,1)}, bf16[320,256]{1,0:T(8,128)(2,1)S(1)}, u32[]{:S(2)}, u32[]{:S(2)}) collective-permute-start(bf16[320,256]{1,0:T(8,128)(2,1)} %get-tuple-element.32), channel_id=1, source_target_pairs={{0,8},{8,0},{1,9},{9,1},{2,10},{10,2},{3,11},{11,3},{4,12},{12,4},... | collective-permute-start | bytes 491528 | tf_op jit(solution)/shard_map/ppermute | solution.py:123
  9.4 18.5 %collective-permute-start.2 = (bf16[320,256]{1,0:T(8,128)(2,1)}, bf16[320,256]{1,0:T(8,128)(2,1)S(1)}, u32[]{:S(2)}, u32[]{:S(2)}) collective-permute-start(bf16[320,256]{1,0:T(8,128)(2,1)} %get-tuple-element.30), channel_id=1, source_target_pairs={{0,12},{4,8},{8,4},{12,0},{1,13},{5,9},{9,5},{13,1},{2,14},{6,10},... | collective-permute-start | bytes 491528 | tf_op jit(solution)/shard_map/ppermute | solution.py:123
  10.8 21.9 %collective-permute-start.7 = (bf16[1024,256]{1,0:T(8,128)(2,1)}, bf16[1024,256]{1,0:T(8,128)(2,1)S(1)}, u32[]{:S(2)}, u32[]{:S(2)}) collective-permute-start(bf16[1024,256]{1,0:T(8,128)(2,1)} %refs_0_.4), channel_id=1, source_target_pairs={{0,1},{1,0},{2,3},{3,2},{4,5},{5,4},{6,7},{7,6},{8,9},{9,8},{10,11... | collective-permute-start | bytes 1572872 | tf_op jit(solution)/shard_map/ppermute | solution.py:123
  22.2 20.0 %collective-permute-start.4 = (bf16[1024,256]{1,0:T(8,128)(2,1)S(1)}, bf16[1024,256]{1,0:T(8,128)(2,1)S(1)}, u32[]{:S(2)}, u32[]{:S(2)}) collective-permute-start(bf16[1024,256]{1,0:T(8,128)(2,1)S(1)} %copy-done.9), channel_id=1, source_target_pairs={{0,16},{16,0},{1,17},{17,1},{2,18},{18,2},{3,19},{19,3},{4,20},{20... | collective-permute-start | bytes 1572872 | tf_op jit(solution)/shard_map/ppermute | solution.py:123
  28.6 12.8 %collective-permute-start.9 = (bf16[1024,256]{1,0:T(8,128)(2,1)S(1)}, bf16[1024,256]{1,0:T(8,128)(2,1)S(1)}, u32[]{:S(2)}, u32[]{:S(2)}) collective-permute-start(bf16[1024,256]{1,0:T(8,128)(2,1)S(1)} %collective-permute-done.5.refs_2_), channel_id=1, source_target_pairs={{0,1},{1,0},{2,3},{3,2},{4,5},{5,4},{6,7},{7,6},{8,9},{9,8},{10,11... | collective-permute-start | bytes 1572872 | tf_op jit(solution)/shard_map/ppermute | solution.py:123
  30.2 14.4 %collective-permute-start.11 = (bf16[4,192,256]{2,1,0:T(8,128)(2,1)S(1)}, bf16[4,192,256]{2,1,0:T(8,128)(2,1)}, u32[]{:S(2)}, u32[]{:S(2)}) collective-permute-start(bf16[4,192,256]{2,1,0:T(8,128)(2,1)S(1)} %pad_maximum_fusion.4.refs_8_), channel_id=1, source_target_pairs={{0,2},{2,0},{1,3},{3,1},{4,6},{6,4},{5,7},{7,5},{8,10},{10,8},{9,1... | collective-permute-start | bytes 1179656 | tf_op jit(solution)/shard_map/ppermute | solution.py:123
  32.6 12.0 %collective-permute-start.6 = (bf16[1024,256]{1,0:T(8,128)(2,1)S(1)}, bf16[1024,256]{1,0:T(8,128)(2,1)}, u32[]{:S(2)}, u32[]{:S(2)}) collective-permute-start(bf16[1024,256]{1,0:T(8,128)(2,1)S(1)} %collective-permute-done.5.refs_2_), channel_id=1, source_target_pairs={{0,16},{16,0},{1,17},{17,1},{2,18},{18,2},{3,19},{19,3},{4,20},{20... | collective-permute-start | bytes 1572872 | tf_op jit(solution)/shard_map/ppermute | solution.py:123
  32.7 11.9 %collective-permute-start.8 = (bf16[1024,256]{1,0:T(8,128)(2,1)S(1)}, bf16[1024,256]{1,0:T(8,128)(2,1)}, u32[]{:S(2)}, u32[]{:S(2)}) collective-permute-start(bf16[1024,256]{1,0:T(8,128)(2,1)S(1)} %collective-permute-done.7.refs_4_), channel_id=1, source_target_pairs={{0,16},{16,0},{1,17},{17,1},{2,18},{18,2},{3,19},{19,3},{4,20},{20... | collective-permute-start | bytes 1572872 | tf_op jit(solution)/shard_map/ppermute | solution.py:123
  41.4 3.2 %collective-permute-start.10 = (bf16[1024,256]{1,0:T(8,128)(2,1)S(1)}, bf16[1024,256]{1,0:T(8,128)(2,1)}, u32[]{:S(2)}, u32[]{:S(2)}) collective-permute-start(bf16[1024,256]{1,0:T(8,128)(2,1)S(1)} %collective-permute-done.9.refs_6_), channel_id=1, source_target_pairs={{0,16},{16,0},{1,17},{17,1},{2,18},{18,2},{3,19},{19,3},{4,20},{20... | collective-permute-start | bytes 1572872 | tf_op jit(solution)/shard_map/ppermute | solution.py:123
  42.3 8.8 %collective-permute-start.3 = (bf16[4,128,256]{2,1,0:T(8,128)(2,1)}, bf16[4,128,256]{2,1,0:T(8,128)(2,1)S(1)}, u32[]{:S(2)}, u32[]{:S(2)}) collective-permute-start(bf16[4,128,256]{2,1,0:T(8,128)(2,1)} %get-tuple-element.68), channel_id=1, source_target_pairs={{0,2},{2,0},{1,3},{3,1},{4,6},{6,4},{5,7},{7,5},{8,10},{10,8},{9,1... | collective-permute-start | bytes 786440 | tf_op jit(solution)/shard_map/ppermute | solution.py:123
  51.2 45.9 %collective-permute-start.16 = (bf16[2,4,128,256]{3,2,1,0:T(8,128)(2,1)S(1)}, bf16[2,4,128,256]{3,2,1,0:T(8,128)(2,1)S(1)}, u32[]{:S(2)}, u32[]{:S(2)}) collective-permute-start(bf16[2,4,128,256]{3,2,1,0:T(8,128)(2,1)S(1)} %get-tuple-element.66.refs_2_), channel_id=1, source_target_pairs={{0,1},{1,0},{2,3},{3,2},{4,5},{5,4},{6,7},{7,6},{8,9},{9,8},{10,11... | collective-permute-start | bytes 1572872 | tf_op jit(solution)/shard_map/ppermute | solution.py:123
  52.8 11.5 %collective-permute-start.19 = (bf16[704,128]{1,0:T(8,128)(2,1)S(1)}, bf16[704,128]{1,0:T(8,128)(2,1)S(1)}, u32[]{:S(2)}, u32[]{:S(2)}) collective-permute-start(bf16[704,128]{1,0:T(8,128)(2,1)S(1)} %copy-done.28), channel_id=1, source_target_pairs={{0,8},{8,0},{1,9},{9,1},{2,10},{10,2},{3,11},{11,3},{4,12},{12,4},... | collective-permute-start | bytes 540680 | tf_op jit(solution)/shard_map/ppermute | solution.py:123
  52.8 18.0 %collective-permute-start.18 = (bf16[704,128]{1,0:T(8,128)(2,1)S(1)}, bf16[704,128]{1,0:T(8,128)(2,1)S(1)}, u32[]{:S(2)}, u32[]{:S(2)}) collective-permute-start(bf16[704,128]{1,0:T(8,128)(2,1)S(1)} %copy-done.40), channel_id=1, source_target_pairs={{0,4},{4,0},{1,5},{5,1},{2,6},{6,2},{3,7},{7,3},{8,12},{12,8},{9,1... | collective-permute-start | bytes 540680 | tf_op jit(solution)/shard_map/ppermute | solution.py:123
  60.7 65.0 %copy-start.39 = (bf16[64,1024]{1,0:T(8,128)(2,1)S(1)}, bf16[64,1024]{1,0:T(8,128)(2,1)}, u32[]{:S(2)}) copy-start(bf16[64,1024]{1,0:T(8,128)(2,1)} %get-tuple-element.37) | copy-start | bytes 393220
  60.7 25.3 %collective-permute-start.33 = (bf16[704,256]{1,0:T(8,128)(2,1)}, bf16[704,256]{1,0:T(8,128)(2,1)S(1)}, u32[]{:S(2)}, u32[]{:S(2)}) collective-permute-start(bf16[704,256]{1,0:T(8,128)(2,1)} %get-tuple-element.45.refs_0_), channel_id=1, source_target_pairs={{0,8},{8,0},{1,9},{9,1},{2,10},{10,2},{3,11},{11,3},{4,12},{12,4},... | collective-permute-start | bytes 1081352 | tf_op jit(solution)/shard_map/ppermute | solution.py:123
  60.8 35.6 %collective-permute-start.32 = (bf16[704,256]{1,0:T(8,128)(2,1)}, bf16[704,256]{1,0:T(8,128)(2,1)S(1)}, u32[]{:S(2)}, u32[]{:S(2)}) collective-permute-start(bf16[704,256]{1,0:T(8,128)(2,1)} %get-tuple-element.46), channel_id=1, source_target_pairs={{0,4},{4,0},{1,5},{5,1},{2,6},{6,2},{3,7},{7,3},{8,12},{12,8},{9,1... | collective-permute-start | bytes 1081352 | tf_op jit(solution)/shard_map/ppermute | solution.py:123
  64.2 74.0 %copy-start.29 = (bf16[704,128]{1,0:T(8,128)(2,1)}, bf16[704,128]{1,0:T(8,128)(2,1)S(1)}, u32[]{:S(2)}) copy-start(bf16[704,128]{1,0:T(8,128)(2,1)S(1)} %collective-permute-done.19.refs_2_) | copy-start | bytes 540676
  64.2 20.2 %collective-permute-start.20 = (bf16[704,128]{1,0:T(8,128)(2,1)S(1)}, bf16[704,128]{1,0:T(8,128)(2,1)}, u32[]{:S(2)}, u32[]{:S(2)}) collective-permute-start(bf16[704,128]{1,0:T(8,128)(2,1)S(1)} %copy-done.40), channel_id=1, source_target_pairs={{0,12},{4,8},{8,4},{12,0},{1,13},{5,9},{9,5},{13,1},{2,14},{6,10},... | collective-permute-start | bytes 540680 | tf_op jit(solution)/shard_map/ppermute | solution.py:123
  70.8 67.4 %copy-start.30 = (bf16[704,128]{1,0:T(8,128)(2,1)}, bf16[704,128]{1,0:T(8,128)(2,1)S(1)}, u32[]{:S(2)}) copy-start(bf16[704,128]{1,0:T(8,128)(2,1)S(1)} %collective-permute-done.18.refs_1_) | copy-start | bytes 540676
  70.8 28.8 %collective-permute-start.34 = (bf16[704,256]{1,0:T(8,128)(2,1)}, bf16[704,256]{1,0:T(8,128)(2,1)S(1)}, u32[]{:S(2)}, u32[]{:S(2)}) collective-permute-start(bf16[704,256]{1,0:T(8,128)(2,1)} %get-tuple-element.46), channel_id=1, source_target_pairs={{0,12},{4,8},{8,4},{12,0},{1,13},{5,9},{9,5},{13,1},{2,14},{6,10},... | collective-permute-start | bytes 1081352 | tf_op jit(solution)/shard_map/ppermute | solution.py:123
  84.4 15.2 %collective-permute-start.35 = (bf16[704,256]{1,0:T(8,128)(2,1)}, bf16[704,256]{1,0:T(8,128)(2,1)S(1)}, u32[]{:S(2)}, u32[]{:S(2)}) collective-permute-start(bf16[704,256]{1,0:T(8,128)(2,1)} %get-tuple-element.45.refs_0_), channel_id=1, source_target_pairs={{0,2},{2,0},{1,3},{3,1},{4,6},{6,4},{5,7},{7,5},{8,10},{10,8},{9,1... | collective-permute-start | bytes 1081352 | tf_op jit(solution)/shard_map/ppermute | solution.py:123
  85.9 101.3 %copy-start.16 = (bf16[704,256]{1,0:T(8,128)(2,1)}, bf16[704,256]{1,0:T(8,128)(2,1)S(1)}, u32[]{:S(2)}) copy-start(bf16[704,256]{1,0:T(8,128)(2,1)S(1)} %collective-permute-done.33.refs_2_) | copy-start | bytes 1081348
  85.9 39.8 %collective-permute-start.26 = (bf16[704,256]{1,0:T(8,128)(2,1)}, bf16[704,256]{1,0:T(8,128)(2,1)S(1)}, u32[]{:S(2)}, u32[]{:S(2)}) collective-permute-start(bf16[704,256]{1,0:T(8,128)(2,1)} %get-tuple-element.42.refs_0_), channel_id=1, source_target_pairs={{0,8},{8,0},{1,9},{9,1},{2,10},{10,2},{3,11},{11,3},{4,12},{12,4},... | collective-permute-start | bytes 1081352 | tf_op jit(solution)/shard_map/ppermute | solution.py:123
  96.4 81.3 %copy-start.17 = (bf16[704,256]{1,0:T(8,128)(2,1)}, bf16[704,256]{1,0:T(8,128)(2,1)S(1)}, u32[]{:S(2)}) copy-start(bf16[704,256]{1,0:T(8,128)(2,1)S(1)} %collective-permute-done.32.refs_1_) | copy-start | bytes 1081348
  96.4 29.3 %collective-permute-start.25 = (bf16[704,256]{1,0:T(8,128)(2,1)}, bf16[704,256]{1,0:T(8,128)(2,1)S(1)}, u32[]{:S(2)}, u32[]{:S(2)}) collective-permute-start(bf16[704,256]{1,0:T(8,128)(2,1)} %get-tuple-element.43), channel_id=1, source_target_pairs={{0,4},{4,0},{1,5},{5,1},{2,6},{6,2},{3,7},{7,3},{8,12},{12,8},{9,1... | collective-permute-start | bytes 1081352 | tf_op jit(solution)/shard_map/ppermute | solution.py:123
  97.1 82.3 %copy-start.3 = (bf16[2,4,128,256]{3,2,1,0:T(8,128)(2,1)}, bf16[2,4,128,256]{3,2,1,0:T(8,128)(2,1)S(1)}, u32[]{:S(2)}) copy-start(bf16[2,4,128,256]{3,2,1,0:T(8,128)(2,1)S(1)} %collective-permute-done.16.refs_3_) | copy-start | bytes 1572868
  97.1 29.2 %collective-permute-start.27 = (bf16[704,256]{1,0:T(8,128)(2,1)}, bf16[704,256]{1,0:T(8,128)(2,1)}, u32[]{:S(2)}, u32[]{:S(2)}) collective-permute-start(bf16[704,256]{1,0:T(8,128)(2,1)} %get-tuple-element.43), channel_id=1, source_target_pairs={{0,12},{4,8},{8,4},{12,0},{1,13},{5,9},{9,5},{13,1},{2,14},{6,10},... | collective-permute-start | bytes 1081352 | tf_op jit(solution)/shard_map/ppermute | solution.py:123
  99.6 79.7 %copy-start.18 = (bf16[704,256]{1,0:T(8,128)(2,1)}, bf16[704,256]{1,0:T(8,128)(2,1)S(1)}, u32[]{:S(2)}) copy-start(bf16[704,256]{1,0:T(8,128)(2,1)S(1)} %collective-permute-done.34.refs_3_) | copy-start | bytes 1081348
  99.6 78.1 %collective-permute-start.17 = (bf16[2,2,4,128,256]{4,3,2,1,0:T(8,128)(2,1)S(1)}, bf16[2,2,4,128,256]{4,3,2,1,0:T(8,128)(2,1)S(1)}, u32[]{:S(2)}, u32[]{:S(2)}) collective-permute-start(bf16[2,2,4,128,256]{4,3,2,1,0:T(8,128)(2,1)S(1)} %pad_maximum_fusion), channel_id=1, source_target_pairs={{0,16},{16,0},{1,17},{17,1},{2,18},{18,2},{3,19},{19,3},{4,20},{20... | collective-permute-start | bytes 3145736 | tf_op jit(solution)/shard_map/ppermute | solution.py:123
  99.7 79.6 %copy-start.20 = (bf16[704,256]{1,0:T(8,128)(2,1)}, bf16[704,256]{1,0:T(8,128)(2,1)S(1)}, u32[]{:S(2)}) copy-start(bf16[704,256]{1,0:T(8,128)(2,1)S(1)} %collective-permute-done.35.refs_4_) | copy-start | bytes 1081348
  99.7 38.6 %collective-permute-start.28 = (bf16[704,256]{1,0:T(8,128)(2,1)S(1)}, bf16[704,256]{1,0:T(8,128)(2,1)}, u32[]{:S(2)}, u32[]{:S(2)}) collective-permute-start(bf16[704,256]{1,0:T(8,128)(2,1)S(1)} %copy-done.15), channel_id=1, source_target_pairs={{0,2},{2,0},{1,3},{3,1},{4,6},{6,4},{5,7},{7,5},{8,10},{10,8},{9,1... | collective-permute-start | bytes 1081352 | tf_op jit(solution)/shard_map/ppermute | solution.py:123
  125.7 53.6 %copy-start.19 = (bf16[704,256]{1,0:T(8,128)(2,1)}, bf16[704,256]{1,0:T(8,128)(2,1)S(1)}, u32[]{:S(2)}) copy-start(bf16[704,256]{1,0:T(8,128)(2,1)S(1)} %collective-permute-done.26.refs_2_) | copy-start | bytes 1081348
  125.7 7.8 %collective-permute-start.12 = (bf16[64,1024]{1,0:T(8,128)(2,1)S(1)}, bf16[64,1024]{1,0:T(8,128)(2,1)S(1)}, u32[]{:S(2)}, u32[]{:S(2)}) collective-permute-start(bf16[64,1024]{1,0:T(8,128)(2,1)S(1)} %copy-done.39), channel_id=1, source_target_pairs={{0,4},{4,0},{1,5},{5,1},{2,6},{6,2},{3,7},{7,3},{8,12},{12,8},{9,1... | collective-permute-start | bytes 393224 | tf_op jit(solution)/shard_map/ppermute | solution.py:123
  125.7 53.6 %copy-start.21 = (bf16[704,256]{1,0:T(8,128)(2,1)}, bf16[704,256]{1,0:T(8,128)(2,1)S(1)}, u32[]{:S(2)}) copy-start(bf16[704,256]{1,0:T(8,128)(2,1)S(1)} %collective-permute-done.25.refs_1_) | copy-start | bytes 1081348
  125.7 9.3 %collective-permute-start.13 = (bf16[64,1024]{1,0:T(8,128)(2,1)S(1)}, bf16[64,1024]{1,0:T(8,128)(2,1)S(1)}, u32[]{:S(2)}, u32[]{:S(2)}) collective-permute-start(bf16[64,1024]{1,0:T(8,128)(2,1)S(1)} %copy-done.39), channel_id=1, source_target_pairs={{0,1},{1,0},{2,3},{3,2},{4,5},{5,4},{6,7},{7,6},{8,9},{9,8},{10,11... | collective-permute-start | bytes 393224 | tf_op jit(solution)/shard_map/ppermute | solution.py:123
  126.3 10.4 %collective-permute-start.14 = (bf16[64,1024]{1,0:T(8,128)(2,1)S(1)}, bf16[64,1024]{1,0:T(8,128)(2,1)S(1)}, u32[]{:S(2)}, u32[]{:S(2)}) collective-permute-start(bf16[64,1024]{1,0:T(8,128)(2,1)S(1)} %copy-done.39), channel_id=1, source_target_pairs={{0,5},{1,4},{4,1},{5,0},{2,7},{3,6},{6,3},{7,2},{8,13},{9,12},{12,... | collective-permute-start | bytes 393224 | tf_op jit(solution)/shard_map/ppermute | solution.py:123
  133.5 11.3 %collective-permute-start.37 = (bf16[704,256]{1,0:T(8,128)(2,1)S(1)}, bf16[704,256]{1,0:T(8,128)(2,1)S(1)}, u32[]{:S(2)}, u32[]{:S(2)}) collective-permute-start(bf16[704,256]{1,0:T(8,128)(2,1)S(1)} %collective-permute-done.33.refs_2_), channel_id=1, source_target_pairs={{0,2},{2,0},{1,3},{3,1},{4,6},{6,4},{5,7},{7,5},{8,10},{10,8},{9,1... | collective-permute-start | bytes 1081352 | tf_op jit(solution)/shard_map/ppermute | solution.py:123
  135.0 17.5 %collective-permute-start.36 = (bf16[704,256]{1,0:T(8,128)(2,1)S(1)}, bf16[704,256]{1,0:T(8,128)(2,1)S(1)}, u32[]{:S(2)}, u32[]{:S(2)}) collective-permute-start(bf16[704,256]{1,0:T(8,128)(2,1)S(1)} %collective-permute-done.32.refs_1_), channel_id=1, source_target_pairs={{0,2},{2,0},{1,3},{3,1},{4,6},{6,4},{5,7},{7,5},{8,10},{10,8},{9,1... | collective-permute-start | bytes 1081352 | tf_op jit(solution)/shard_map/ppermute | solution.py:123
  136.7 23.5 %collective-permute-start.38 = (bf16[704,256]{1,0:T(8,128)(2,1)S(1)}, bf16[704,256]{1,0:T(8,128)(2,1)S(1)}, u32[]{:S(2)}, u32[]{:S(2)}) collective-permute-start(bf16[704,256]{1,0:T(8,128)(2,1)S(1)} %collective-permute-done.34.refs_3_), channel_id=1, source_target_pairs={{0,2},{2,0},{1,3},{3,1},{4,6},{6,4},{5,7},{7,5},{8,10},{10,8},{9,1... | collective-permute-start | bytes 1081352 | tf_op jit(solution)/shard_map/ppermute | solution.py:123
  138.3 38.9 %collective-permute-start.15 = (bf16[4,64,1024]{2,1,0:T(8,128)(2,1)S(1)}, bf16[4,64,1024]{2,1,0:T(8,128)(2,1)S(1)}, u32[]{:S(2)}, u32[]{:S(2)}) collective-permute-start(bf16[4,64,1024]{2,1,0:T(8,128)(2,1)S(1)} %pad_maximum_fusion.1.refs_0_), channel_id=1, source_target_pairs={{0,16},{16,0},{1,17},{17,1},{2,18},{18,2},{3,19},{19,3},{4,20},{20... | collective-permute-start | bytes 1572872 | tf_op jit(solution)/shard_map/ppermute | solution.py:123
  144.8 23.2 %collective-permute-start.30 = (bf16[704,256]{1,0:T(8,128)(2,1)S(1)}, bf16[704,256]{1,0:T(8,128)(2,1)S(1)}, u32[]{:S(2)}, u32[]{:S(2)}) collective-permute-start(bf16[704,256]{1,0:T(8,128)(2,1)S(1)} %collective-permute-done.26.refs_2_), channel_id=1, source_target_pairs={{0,2},{2,0},{1,3},{3,1},{4,6},{6,4},{5,7},{7,5},{8,10},{10,8},{9,1... | collective-permute-start | bytes 1081352 | tf_op jit(solution)/shard_map/ppermute | solution.py:123
  152.5 23.2 %collective-permute-start.29 = (bf16[704,256]{1,0:T(8,128)(2,1)S(1)}, bf16[704,256]{1,0:T(8,128)(2,1)S(1)}, u32[]{:S(2)}, u32[]{:S(2)}) collective-permute-start(bf16[704,256]{1,0:T(8,128)(2,1)S(1)} %collective-permute-done.25.refs_1_), channel_id=1, source_target_pairs={{0,2},{2,0},{1,3},{3,1},{4,6},{6,4},{5,7},{7,5},{8,10},{10,8},{9,1... | collective-permute-start | bytes 1081352 | tf_op jit(solution)/shard_map/ppermute | solution.py:123
  160.2 34.9 %collective-permute-start.31 = (bf16[704,256]{1,0:T(8,128)(2,1)}, bf16[704,256]{1,0:T(8,128)(2,1)}, u32[]{:S(2)}, u32[]{:S(2)}) collective-permute-start(bf16[704,256]{1,0:T(8,128)(2,1)} %collective-permute-done.27.refs_3_), channel_id=1, source_target_pairs={{0,2},{2,0},{1,3},{3,1},{4,6},{6,4},{5,7},{7,5},{8,10},{10,8},{9,1... | collective-permute-start | bytes 1081352 | tf_op jit(solution)/shard_map/ppermute | solution.py:123
  168.0 35.2 %collective-permute-start.21 = (bf16[704,128]{1,0:T(8,128)(2,1)S(1)}, bf16[704,128]{1,0:T(8,128)(2,1)}, u32[]{:S(2)}, u32[]{:S(2)}) collective-permute-start(bf16[704,128]{1,0:T(8,128)(2,1)S(1)} %copy-done.28), channel_id=1, source_target_pairs={{0,2},{2,0},{1,3},{3,1},{4,6},{6,4},{5,7},{7,5},{8,10},{10,8},{9,1... | collective-permute-start | bytes 540680 | tf_op jit(solution)/shard_map/ppermute | solution.py:123
  175.7 27.5 %collective-permute-start.23 = (bf16[704,128]{1,0:T(8,128)(2,1)}, bf16[704,128]{1,0:T(8,128)(2,1)}, u32[]{:S(2)}, u32[]{:S(2)}) collective-permute-start(bf16[704,128]{1,0:T(8,128)(2,1)} %copy-done.29), channel_id=1, source_target_pairs={{0,2},{2,0},{1,3},{3,1},{4,6},{6,4},{5,7},{7,5},{8,10},{10,8},{9,1... | collective-permute-start | bytes 540680 | tf_op jit(solution)/shard_map/ppermute | solution.py:123
  177.2 26.0 %collective-permute-start.22 = (bf16[704,128]{1,0:T(8,128)(2,1)}, bf16[704,128]{1,0:T(8,128)(2,1)}, u32[]{:S(2)}, u32[]{:S(2)}) collective-permute-start(bf16[704,128]{1,0:T(8,128)(2,1)} %copy-done.30), channel_id=1, source_target_pairs={{0,2},{2,0},{1,3},{3,1},{4,6},{6,4},{5,7},{7,5},{8,10},{10,8},{9,1... | collective-permute-start | bytes 540680 | tf_op jit(solution)/shard_map/ppermute | solution.py:123
  177.7 25.5 %collective-permute-start.24 = (bf16[704,128]{1,0:T(8,128)(2,1)}, bf16[704,128]{1,0:T(8,128)(2,1)}, u32[]{:S(2)}, u32[]{:S(2)}) collective-permute-start(bf16[704,128]{1,0:T(8,128)(2,1)} %collective-permute-done.20.refs_3_), channel_id=1, source_target_pairs={{0,2},{2,0},{1,3},{3,1},{4,6},{6,4},{5,7},{7,5},{8,10},{10,8},{9,1... | collective-permute-start | bytes 540680 | tf_op jit(solution)/shard_map/ppermute | solution.py:123
  208.6 31.5 %collective-permute-start.39 = (bf16[4,512,256]{2,1,0:T(8,128)(2,1)}, bf16[4,512,256]{2,1,0:T(8,128)(2,1)S(1)}, u32[]{:S(2)}, u32[]{:S(2)}) collective-permute-start(bf16[4,512,256]{2,1,0:T(8,128)(2,1)} %get-tuple-element.48), channel_id=1, source_target_pairs={{0,16},{16,0},{1,17},{17,1},{2,18},{18,2},{3,19},{19,3},{4,20},{20... | collective-permute-start | bytes 3145736 | tf_op jit(solution)/shard_map/ppermute | solution.py:123
  208.7 11.8 %collective-permute-start.44 = (bf16[704,128]{1,0:T(8,128)(2,1)S(1)}, bf16[704,128]{1,0:T(8,128)(2,1)S(1)}, u32[]{:S(2)}, u32[]{:S(2)}) collective-permute-start(bf16[704,128]{1,0:T(8,128)(2,1)S(1)} %copy-done.27), channel_id=1, source_target_pairs={{0,8},{8,0},{1,9},{9,1},{2,10},{10,2},{3,11},{11,3},{4,12},{12,4},... | collective-permute-start | bytes 540680 | tf_op jit(solution)/shard_map/ppermute | solution.py:123
  208.8 12.3 %collective-permute-start.43 = (bf16[704,128]{1,0:T(8,128)(2,1)}, bf16[704,128]{1,0:T(8,128)(2,1)S(1)}, u32[]{:S(2)}, u32[]{:S(2)}) collective-permute-start(bf16[704,128]{1,0:T(8,128)(2,1)} %get-tuple-element.50), channel_id=1, source_target_pairs={{0,4},{4,0},{1,5},{5,1},{2,6},{6,2},{3,7},{7,3},{8,12},{12,8},{9,1... | collective-permute-start | bytes 540680 | tf_op jit(solution)/shard_map/ppermute | solution.py:123
  210.5 13.4 %collective-permute-start.45 = (bf16[704,128]{1,0:T(8,128)(2,1)}, bf16[704,128]{1,0:T(8,128)(2,1)S(1)}, u32[]{:S(2)}, u32[]{:S(2)}) collective-permute-start(bf16[704,128]{1,0:T(8,128)(2,1)} %get-tuple-element.50), channel_id=1, source_target_pairs={{0,12},{4,8},{8,4},{12,0},{1,13},{5,9},{9,5},{13,1},{2,14},{6,10},... | collective-permute-start | bytes 540680 | tf_op jit(solution)/shard_map/ppermute | solution.py:123
  213.1 11.3 %collective-permute-start.46 = (bf16[704,128]{1,0:T(8,128)(2,1)S(1)}, bf16[704,128]{1,0:T(8,128)(2,1)S(1)}, u32[]{:S(2)}, u32[]{:S(2)}) collective-permute-start(bf16[704,128]{1,0:T(8,128)(2,1)S(1)} %copy-done.27), channel_id=1, source_target_pairs={{0,2},{2,0},{1,3},{3,1},{4,6},{6,4},{5,7},{7,5},{8,10},{10,8},{9,1... | collective-permute-start | bytes 540680 | tf_op jit(solution)/shard_map/ppermute | solution.py:123
  220.4 7.4 %collective-permute-start.48 = (bf16[704,128]{1,0:T(8,128)(2,1)S(1)}, bf16[704,128]{1,0:T(8,128)(2,1)S(1)}, u32[]{:S(2)}, u32[]{:S(2)}) collective-permute-start(bf16[704,128]{1,0:T(8,128)(2,1)S(1)} %collective-permute-done.44.refs_2_), channel_id=1, source_target_pairs={{0,2},{2,0},{1,3},{3,1},{4,6},{6,4},{5,7},{7,5},{8,10},{10,8},{9,1... | collective-permute-start | bytes 540680 | tf_op jit(solution)/shard_map/ppermute | solution.py:123
  221.1 10.7 %collective-permute-start.47 = (bf16[704,128]{1,0:T(8,128)(2,1)S(1)}, bf16[704,128]{1,0:T(8,128)(2,1)S(1)}, u32[]{:S(2)}, u32[]{:S(2)}) collective-permute-start(bf16[704,128]{1,0:T(8,128)(2,1)S(1)} %collective-permute-done.43.refs_1_), channel_id=1, source_target_pairs={{0,2},{2,0},{1,3},{3,1},{4,6},{6,4},{5,7},{7,5},{8,10},{10,8},{9,1... | collective-permute-start | bytes 540680 | tf_op jit(solution)/shard_map/ppermute | solution.py:123
  223.9 10.8 %collective-permute-start.49 = (bf16[704,128]{1,0:T(8,128)(2,1)S(1)}, bf16[704,128]{1,0:T(8,128)(2,1)}, u32[]{:S(2)}, u32[]{:S(2)}) collective-permute-start(bf16[704,128]{1,0:T(8,128)(2,1)S(1)} %collective-permute-done.45.refs_3_), channel_id=1, source_target_pairs={{0,2},{2,0},{1,3},{3,1},{4,6},{6,4},{5,7},{7,5},{8,10},{10,8},{9,1... | collective-permute-start | bytes 540680 | tf_op jit(solution)/shard_map/ppermute | solution.py:123
  240.0 4.0 %collective-permute-start.50 = (bf16[4,512,256]{2,1,0:T(8,128)(2,1)}, bf16[4,512,256]{2,1,0:T(8,128)(2,1)S(1)}, u32[]{:S(2)}, u32[]{:S(2)}) collective-permute-start(bf16[4,512,256]{2,1,0:T(8,128)(2,1)} %get-tuple-element.52), channel_id=1, source_target_pairs={{0,16},{16,0},{1,17},{17,1},{2,18},{18,2},{3,19},{19,3},{4,20},{20... | collective-permute-start | bytes 3145736 | tf_op jit(solution)/shard_map/ppermute | solution.py:123
  240.5 10.2 %collective-permute-start.40 = (bf16[512,256]{1,0:T(8,128)(2,1)S(1)}, bf16[512,256]{1,0:T(8,128)(2,1)S(1)}, u32[]{:S(2)}, u32[]{:S(2)}) collective-permute-start(bf16[512,256]{1,0:T(8,128)(2,1)S(1)} %get-tuple-element.57), channel_id=1, source_target_pairs={{0,5},{1,4},{4,1},{5,0},{2,7},{3,6},{6,3},{7,2},{8,13},{9,12},{12,... | collective-permute-start | bytes 786440 | tf_op jit(solution)/shard_map/ppermute | solution.py:123
  240.7 14.9 %collective-permute-start.41 = (bf16[512,256]{1,0:T(8,128)(2,1)S(1)}, bf16[512,256]{1,0:T(8,128)(2,1)S(1)}, u32[]{:S(2)}, u32[]{:S(2)}) collective-permute-start(bf16[512,256]{1,0:T(8,128)(2,1)S(1)} %get-tuple-element.59), channel_id=1, source_target_pairs={{0,1},{1,0},{2,3},{3,2},{4,5},{5,4},{6,7},{7,6},{8,9},{9,8},{10,11... | collective-permute-start | bytes 786440 | tf_op jit(solution)/shard_map/ppermute | solution.py:123
  242.1 13.5 %collective-permute-start.42 = (bf16[512,256]{1,0:T(8,128)(2,1)S(1)}, bf16[512,256]{1,0:T(8,128)(2,1)S(1)}, u32[]{:S(2)}, u32[]{:S(2)}) collective-permute-start(bf16[512,256]{1,0:T(8,128)(2,1)S(1)} %get-tuple-element.58), channel_id=1, source_target_pairs={{0,4},{4,0},{1,5},{5,1},{2,6},{6,2},{3,7},{7,3},{8,12},{12,8},{9,1... | collective-permute-start | bytes 786440 | tf_op jit(solution)/shard_map/ppermute | solution.py:123
  244.4 17.6 %collective-permute-start.51 = (bf16[512,256]{1,0:T(8,128)(2,1)S(1)}, bf16[512,256]{1,0:T(8,128)(2,1)S(1)}, u32[]{:S(2)}, u32[]{:S(2)}) collective-permute-start(bf16[512,256]{1,0:T(8,128)(2,1)S(1)} %get-tuple-element.60), channel_id=1, source_target_pairs={{0,5},{1,4},{4,1},{5,0},{2,7},{3,6},{6,3},{7,2},{8,13},{9,12},{12,... | collective-permute-start | bytes 786440 | tf_op jit(solution)/shard_map/ppermute | solution.py:123
  244.6 21.6 %collective-permute-start.52 = (bf16[512,256]{1,0:T(8,128)(2,1)S(1)}, bf16[512,256]{1,0:T(8,128)(2,1)S(1)}, u32[]{:S(2)}, u32[]{:S(2)}) collective-permute-start(bf16[512,256]{1,0:T(8,128)(2,1)S(1)} %get-tuple-element.62), channel_id=1, source_target_pairs={{0,1},{1,0},{2,3},{3,2},{4,5},{5,4},{6,7},{7,6},{8,9},{9,8},{10,11... | collective-permute-start | bytes 786440 | tf_op jit(solution)/shard_map/ppermute | solution.py:123
  250.7 15.6 %collective-permute-start.53 = (bf16[512,256]{1,0:T(8,128)(2,1)S(1)}, bf16[512,256]{1,0:T(8,128)(2,1)S(1)}, u32[]{:S(2)}, u32[]{:S(2)}) collective-permute-start(bf16[512,256]{1,0:T(8,128)(2,1)S(1)} %get-tuple-element.61), channel_id=1, source_target_pairs={{0,4},{4,0},{1,5},{5,1},{2,6},{6,2},{3,7},{7,3},{8,12},{12,8},{9,1... | collective-permute-start | bytes 786440 | tf_op jit(solution)/shard_map/ppermute | solution.py:123
  (31 other events, 484.6 us)

commit v2 on v1

--- a/solution.py
+++ b/solution.py
@@ -292,7 +292,7 @@
 
     rows = after_ref[...]
     gate = jnp.dot(gate_ref[...], rows, preferred_element_type=jnp.float32) * norm_scale(rows)
-    active_ref[...] = gate / (1.0 + jnp.exp(-gate))
+    active_ref[...] = (gate / (1.0 + jnp.exp(-gate))).astype(jnp.bfloat16)
 
 
 def hidden_kernel(spot_ref, *refs):
@@ -305,7 +305,7 @@
 
     rows = after_ref[...]
     upper = jnp.dot(up_ref[...], rows, preferred_element_type=jnp.float32) * norm_scale(rows)
-    hidden_ref[...] = (active_ref[...] * upper).astype(jnp.bfloat16)
+    hidden_ref[...] = (active_ref[...].astype(jnp.float32) * upper).astype(jnp.bfloat16)
 
 
 def down_kernel(spot_ref, *refs):
@@ -498,7 +498,7 @@
         gate_kernel,
         gates + [after],
         blocks,
-        jax.ShapeDtypeStruct((units, 4 * tokens), jnp.float32),
+        shaped(units, 4 * tokens),
         tile((units, tokens)),
         scratch,
     )
@@ -522,11 +522,12 @@
             grid=(),
         )
         got = flip(sent, "rep")
-        sums = kept.astype(jnp.float32) + got.astype(jnp.float32)
         own = after_own.reshape(-1, 2, lanes, tokens)[:, chunk].reshape(-1, tokens)
-        total = own.astype(jnp.float32) + sums[0]
+        total = own.astype(jnp.float32) + kept[0].astype(jnp.float32) + got[0].astype(jnp.float32)
+        total = lax.optimization_barrier(total)
         for index, way in ((3, ("zl", "tp")), (2, ("tp",)), (1, ("zl",))):
-            part = flip(sums[index].astype(jnp.bfloat16), *way)
+            part = kept[index].astype(jnp.float32) + got[index].astype(jnp.float32)
+            part = flip(part.astype(jnp.bfloat16), *way)
             total = total + part.astype(jnp.float32)
         totals.append(total.astype(jnp.bfloat16).reshape(-1, lanes, tokens))
     return jnp.stack(totals, axis=1).reshape(half, tokens)

time: 268 us -> 267 us (level)
  no operation moved by 1% of the time
where the time goes in v2:
time: 267 us
  waiting for transfers between devices  132 us (49%)
  starting transfers between devices  77 us (29%)
  Pallas kernels  49.8 us (19%)
  local copies, waits for them, and re-layouts  4.66 us (2%)
    ppermute x54, waiting for transfers between devices, flip(): return lax.ppermute(array, axes, [(i, count - 1 - i) for i in range(count)])  132 us
    ppermute x54, starting transfers between devices, flip(): return lax.ppermute(array, axes, [(i, count - 1 - i) for i in range(count)])  77 us
    pallas_call x6, Pallas kernels, run(): pl.pallas_call(kernel, grid=grid, out_shape=outs, in_specs=[scalars] + in...  39.8 us
    pallas_call x3, Pallas kernels, prepare(): pl.pallas_call(kernel, out_shape=tuple((shaped(*shape) for shape in outs)...  10.1 us
  transfers between devices with their start and end apart: 54, of which 24 were waited for; matrix products, arithmetic and copies ran while one was open for 2% of the time, Pallas kernels for 17%

profile of v2, /device:TPU:0, one launch (start us, length us, event | category | flops | bytes accessed | tf_op | source)
XLA Modules:
  0.0 266.6 jit_solution(10789436075531508117)
XLA Ops:
  0.0 3.1 %collective-permute-start.5 = (bf16[1024,256]{1,0:T(8,128)(2,1)}, bf16[1024,256]{1,0:T(8,128)(2,1)S(1)}, u32[]{:S(2)}, u32[]{:S(2)}) collective-permute-start(bf16[1024,256]{1,0:T(8,128)(2,1)} %refs_0_.4), channel_id=1, source_target_pairs={{0,4},{4,0},{1,5},{5,1},{2,6},{6,2},{3,7},{7,3},{8,12},{12,8},{9,1... | collective-permute-start | bytes 1572872 | tf_op jit(solution)/shard_map/ppermute | solution.py:123
  3.7 2.7 %shard_map.181 = (bf16[320,256]{1,0:T(8,128)(2,1)}, bf16[320,256]{1,0:T(8,128)(2,1)}) custom-call(s32[5]{0:T(128)} %stack.89.spot_ref, f32[256,256]{1,0:T(8,128)} %refs_0_.3, f32[256,256]{1,0:T(8,128)} %refs_1_.2, f32[256,256]{1,0:T(8,128)} %refs_2_.1, f32[2,128]{1,0:T(2,128)} %bitcast.98, f32[2,128]{1,0:T(2,128)} %bitcast.99, f32[2,128]{1,0:T(2,128)} %bitcast.100, ...), custom_call_target="tpu_custom_call" | custom-call | tf_op jit(solution)/shard_map/pallas_call | solution.py:385
  6.5 3.0 %collective-permute-start.1 = (bf16[320,256]{1,0:T(8,128)(2,1)}, bf16[320,256]{1,0:T(8,128)(2,1)S(1)}, u32[]{:S(2)}, u32[]{:S(2)}) collective-permute-start(bf16[320,256]{1,0:T(8,128)(2,1)} %get-tuple-element.32), channel_id=1, source_target_pairs={{0,8},{8,0},{1,9},{9,1},{2,10},{10,2},{3,11},{11,3},{4,12},{12,4},... | collective-permute-start | bytes 491528 | tf_op jit(solution)/shard_map/ppermute | solution.py:123
  9.5 1.3 collective-permute-start.2
  10.8 1.5 collective-permute-start.7
  12.3 3.0 %shard_map.182 = (bf16[704,128]{1,0:T(8,128)(2,1)}, bf16[704,128]{1,0:T(8,128)(2,1)}, bf16[704,128]{1,0:T(8,128)(2,1)}, bf16[704,128]{1,0:T(8,128)(2,1)}) custom-call(s32[5]{0:T(128)} %stack.89.spot_ref, f32[2816,256]{1,0:T(8,128)} %weight_ref.1, f32[2,128]{1,0:T(2,128)} %bitcast.103), custom_call_target="tpu_custom_call" | custom-call | tf_op jit(solution)/shard_map/pallas_call | solution.py:385
  15.3 6.9 %collective-permute-done = bf16[320,256]{1,0:T(8,128)(2,1)S(1)} collective-permute-done((bf16[320,256]{1,0:T(8,128)(2,1)}, bf16[320,256]{1,0:T(8,128)(2,1)S(1)}, u32[]{:S(2)}, u32[]{:S(2)}) %collective-permute-start) | collective-permute-done | bytes 163872 | tf_op jit(solution)/shard_map/ppermute | solution.py:123
  22.7 5.2 %collective-permute-done.2 = bf16[320,256]{1,0:T(8,128)(2,1)S(1)} collective-permute-done((bf16[320,256]{1,0:T(8,128)(2,1)}, bf16[320,256]{1,0:T(8,128)(2,1)S(1)}, u32[]{:S(2)}, u32[]{:S(2)}) %collective-permute-start.2) | collective-permute-done | bytes 163872 | tf_op jit(solution)/shard_map/ppermute | solution.py:123
  28.6 1.5 collective-permute-start.9
  30.2 1.6 collective-permute-start.11
  31.8 0.9 slice_bitcast_fusion.6
  33.2 8.2 %collective-permute-done.9.refs_6_ = bf16[1024,256]{1,0:T(8,128)(2,1)S(1)} collective-permute-done((bf16[1024,256]{1,0:T(8,128)(2,1)S(1)}, bf16[1024,256]{1,0:T(8,128)(2,1)S(1)}, u32[]{:S(2)}, u32[]{:S(2)}) %collective-permute-start.9) | collective-permute-done | bytes 524320 | tf_op jit(solution)/shard_map/ppermute | solution.py:123
  41.4 0.9 fusion.7
  42.3 1.5 collective-permute-start.3
  43.9 0.7 copy.24
  44.7 5.7 %shard_map.183 = (bf16[64,1024]{1,0:T(8,128)(2,1)}, bf16[2048,1024]{1,0:T(8,128)(2,1)}) custom-call(s32[5]{0:T(128)} %stack.89.spot_ref, bf16[1024,256]{1,0:T(8,128)(2,1)} %refs_0_.4, bf16[1024,256]{1,0:T(8,128)(2,1)} %copy-done.12, bf16[1024,256]{1,0:T(8,128)(2,1)} %copy-done.10, bf16[1024,256]{1,0:T(8,128)(2,1)} %collective-permute-done.6.refs_3_, ...), custom_call_target="tpu_custom_call" | custom-call | tf_op jit(solution)/shard_map/pallas_call | solution.py:398
  51.2 1.6 collective-permute-start.16
  52.7 3.7 %collective-permute-start.18 = (bf16[704,128]{1,0:T(8,128)(2,1)S(1)}, bf16[704,128]{1,0:T(8,128)(2,1)S(1)}, u32[]{:S(2)}, u32[]{:S(2)}) collective-permute-start(bf16[704,128]{1,0:T(8,128)(2,1)S(1)} %copy-done.39), channel_id=1, source_target_pairs={{0,4},{4,0},{1,5},{5,1},{2,6},{6,2},{3,7},{7,3},{8,12},{12,8},{9,1... | collective-permute-start | bytes 540680 | tf_op jit(solution)/shard_map/ppermute | solution.py:123
  56.4 4.4 %shard_map.185 = (bf16[704,256]{1,0:T(8,128)(2,1)}, bf16[704,256]{1,0:T(8,128)(2,1)}, bf16[704,256]{1,0:T(8,128)(2,1)}, bf16[704,256]{1,0:T(8,128)(2,1)}) custom-call(s32[5]{0:T(128)} %stack.89.spot_ref, f32[256,2816]{1,0:T(8,128)} %refs_0_.5, f32[256,2816]{1,0:T(8,128)} %refs_1_.3, f32[22,128]{1,0:T(8,128)} %bitcast.94, f32[22,128]{1,0:T(8,128)} %bitcast.95, ...), custom_call_target="tpu_custom_call" | custom-call | tf_op jit(solution)/shard_map/pallas_call | solution.py:385
  60.9 1.2 collective-permute-start.32
  62.1 2.0 collective-permute-done.19.refs_2_
  64.0 6.7 %collective-permute-start.20 = (bf16[704,128]{1,0:T(8,128)(2,1)S(1)}, bf16[704,128]{1,0:T(8,128)(2,1)}, u32[]{:S(2)}, u32[]{:S(2)}) collective-permute-start(bf16[704,128]{1,0:T(8,128)(2,1)S(1)} %copy-done.39), channel_id=1, source_target_pairs={{0,12},{4,8},{8,4},{12,0},{1,13},{5,9},{9,5},{13,1},{2,14},{6,10},... | collective-permute-start | bytes 540680 | tf_op jit(solution)/shard_map/ppermute | solution.py:123
  70.8 13.7 %collective-permute-done.20.refs_3_ = bf16[704,128]{1,0:T(8,128)(2,1)} collective-permute-done((bf16[704,128]{1,0:T(8,128)(2,1)S(1)}, bf16[704,128]{1,0:T(8,128)(2,1)}, u32[]{:S(2)}, u32[]{:S(2)}) %collective-permute-start.20) | collective-permute-done | bytes 180256 | tf_op jit(solution)/shard_map/ppermute | solution.py:123
  84.5 1.5 collective-permute-start.35
  86.0 10.4 %collective-permute-start.26 = (bf16[704,256]{1,0:T(8,128)(2,1)}, bf16[704,256]{1,0:T(8,128)(2,1)S(1)}, u32[]{:S(2)}, u32[]{:S(2)}) collective-permute-start(bf16[704,256]{1,0:T(8,128)(2,1)} %get-tuple-element.42.refs_0_), channel_id=1, source_target_pairs={{0,8},{8,0},{1,9},{9,1},{2,10},{10,2},{3,11},{11,3},{4,12},{12,4},... | collective-permute-start | bytes 1081352 | tf_op jit(solution)/shard_map/ppermute | solution.py:123
  96.4 0.7 collective-permute-start.25
  97.1 2.4 collective-permute-start.27
  100.2 25.5 %collective-permute-done.26.refs_2_ = bf16[704,256]{1,0:T(8,128)(2,1)S(1)} collective-permute-done((bf16[704,256]{1,0:T(8,128)(2,1)}, bf16[704,256]{1,0:T(8,128)(2,1)S(1)}, u32[]{:S(2)}, u32[]{:S(2)}) %collective-permute-start.26) | collective-permute-done | bytes 360480 | tf_op jit(solution)/shard_map/ppermute | solution.py:123
  126.3 7.2 %collective-permute-start.14 = (bf16[64,1024]{1,0:T(8,128)(2,1)S(1)}, bf16[64,1024]{1,0:T(8,128)(2,1)S(1)}, u32[]{:S(2)}, u32[]{:S(2)}) collective-permute-start(bf16[64,1024]{1,0:T(8,128)(2,1)S(1)} %copy-done.38), channel_id=1, source_target_pairs={{0,5},{1,4},{4,1},{5,0},{2,7},{3,6},{6,3},{7,2},{8,13},{9,12},{12,... | collective-permute-start | bytes 393224 | tf_op jit(solution)/shard_map/ppermute | solution.py:123
  133.5 1.5 collective-permute-start.37
  135.5 1.2 collective-permute-done.14
  136.7 1.5 collective-permute-start.38
  138.4 6.4 %collective-permute-done.37.refs_6_ = bf16[704,256]{1,0:T(8,128)(2,1)S(1)} collective-permute-done((bf16[704,256]{1,0:T(8,128)(2,1)S(1)}, bf16[704,256]{1,0:T(8,128)(2,1)S(1)}, u32[]{:S(2)}, u32[]{:S(2)}) %collective-permute-start.37) | collective-permute-done | bytes 360480 | tf_op jit(solution)/shard_map/ppermute | solution.py:123
  144.7 1.5 collective-permute-start.30
  146.3 6.2 %collective-permute-done.36.refs_5_ = bf16[704,256]{1,0:T(8,128)(2,1)S(1)} collective-permute-done((bf16[704,256]{1,0:T(8,128)(2,1)S(1)}, bf16[704,256]{1,0:T(8,128)(2,1)S(1)}, u32[]{:S(2)}, u32[]{:S(2)}) %collective-permute-start.36) | collective-permute-done | bytes 360480 | tf_op jit(solution)/shard_map/ppermute | solution.py:123
  152.5 1.5 collective-permute-start.29
  154.0 6.2 %collective-permute-done.38.refs_7_ = bf16[704,256]{1,0:T(8,128)(2,1)S(1)} collective-permute-done((bf16[704,256]{1,0:T(8,128)(2,1)S(1)}, bf16[704,256]{1,0:T(8,128)(2,1)S(1)}, u32[]{:S(2)}, u32[]{:S(2)}) %collective-permute-start.38) | collective-permute-done | bytes 360480 | tf_op jit(solution)/shard_map/ppermute | solution.py:123
  160.2 1.5 collective-permute-start.31
  161.7 6.2 %collective-permute-done.30.refs_6_ = bf16[704,256]{1,0:T(8,128)(2,1)S(1)} collective-permute-done((bf16[704,256]{1,0:T(8,128)(2,1)S(1)}, bf16[704,256]{1,0:T(8,128)(2,1)S(1)}, u32[]{:S(2)}, u32[]{:S(2)}) %collective-permute-start.30) | collective-permute-done | bytes 360480 | tf_op jit(solution)/shard_map/ppermute | solution.py:123
  167.9 1.5 collective-permute-start.21
  169.4 6.2 %collective-permute-done.29.refs_5_ = bf16[704,256]{1,0:T(8,128)(2,1)S(1)} collective-permute-done((bf16[704,256]{1,0:T(8,128)(2,1)S(1)}, bf16[704,256]{1,0:T(8,128)(2,1)S(1)}, u32[]{:S(2)}, u32[]{:S(2)}) %collective-permute-start.29) | collective-permute-done | bytes 360480 | tf_op jit(solution)/shard_map/ppermute | solution.py:123
  175.6 1.5 collective-permute-start.23
  177.7 1.6 collective-permute-start.24
  179.4 7.8 %shard_map.184 = (bf16[2048,1024]{1,0:T(8,128)(2,1)}, bf16[1024,256]{1,0:T(8,128)(2,1)}) custom-call(s32[5]{0:T(128)} %stack.89.spot_ref, bf16[4,64,1024]{2,1,0:T(8,128)(2,1)} %copy-done.2, bf16[4,64,1024]{2,1,0:T(8,128)(2,1)} %copy-done.14, bf16[2,4,128,256]{3,2,1,0:T(8,128)(2,1)} %copy-done.1, bf16[2,4,128,256]{3,2,1,0:T(8,128)(2,1)} %copy-done.3, ...), custom_call_target="tpu_custom_call" | custom-call | tf_op jit(solution)/shard_map/pallas_call | solution.py:398
  187.2 7.6 %shard_map.186.refs_9_ = bf16[704,1024]{1,0:T(8,128)(2,1)} custom-call(s32[5]{0:T(128)} %stack.89.spot_ref, bf16[704,256]{1,0:T(8,128)(2,1)} %get-tuple-element.45.refs_0_, bf16[704,256]{1,0:T(8,128)(2,1)} %copy-done.16, bf16[704,256]{1,0:T(8,128)(2,1)} %copy-done.15, bf16[704,256]{1,0:T(8,128)(2,1)} %copy-done.17, bf16[704,256]{1,0:T(8,128)(2,1)} %copy-done.19, ...), custom_call_target="tpu_custom_call" | custom-call | tf_op jit(solution)/shard_map/pallas_call | solution.py:398
  194.8 7.8 %shard_map.187.refs_8_ = bf16[704,1024]{1,0:T(8,128)(2,1)} custom-call(s32[5]{0:T(128)} %stack.89.spot_ref, bf16[704,256]{1,0:T(8,128)(2,1)} %get-tuple-element.42.refs_0_, bf16[704,256]{1,0:T(8,128)(2,1)} %copy-done.20, bf16[704,256]{1,0:T(8,128)(2,1)} %copy-done.18, bf16[704,256]{1,0:T(8,128)(2,1)} %collective-permute-done.27.refs_3_, ...), custom_call_target="tpu_custom_call" | custom-call | tf_op jit(solution)/shard_map/pallas_call | solution.py:398
  202.7 5.4 %shard_map.188 = (bf16[4,512,256]{2,1,0:T(8,128)(2,1)}, bf16[4,512,256]{2,1,0:T(8,128)(2,1)}) custom-call(s32[5]{0:T(128)} %stack.89.spot_ref, bf16[704,128]{1,0:T(8,128)(2,1)} %get-tuple-element.31.refs_0_, bf16[704,128]{1,0:T(8,128)(2,1)} %copy-done.29, bf16[704,128]{1,0:T(8,128)(2,1)} %copy-done.28, bf16[704,128]{1,0:T(8,128)(2,1)} %collective-permute-done.20.refs_3_, ...), custom_call_target="tpu_custom_call" | custom-call | tf_op jit(solution)/shard_map/pallas_call | solution.py:398
  208.2 1.7 collective-permute-start.43
  209.9 2.6 collective-permute-start.45
  213.2 6.7 %collective-permute-done.44.refs_2_ = bf16[704,128]{1,0:T(8,128)(2,1)S(1)} collective-permute-done((bf16[704,128]{1,0:T(8,128)(2,1)S(1)}, bf16[704,128]{1,0:T(8,128)(2,1)S(1)}, u32[]{:S(2)}, u32[]{:S(2)}) %collective-permute-start.44) | collective-permute-done | bytes 180256 | tf_op jit(solution)/shard_map/ppermute | solution.py:123
  220.5 1.4 collective-permute-start.47
  221.9 1.4 collective-permute-done.45.refs_3_
  223.9 3.4 %collective-permute-done.48.refs_6_ = bf16[704,128]{1,0:T(8,128)(2,1)S(1)} collective-permute-done((bf16[704,128]{1,0:T(8,128)(2,1)S(1)}, bf16[704,128]{1,0:T(8,128)(2,1)S(1)}, u32[]{:S(2)}, u32[]{:S(2)}) %collective-permute-start.48) | collective-permute-done | bytes 180256 | tf_op jit(solution)/shard_map/ppermute | solution.py:123
  227.3 3.9 %collective-permute-done.47.refs_5_ = bf16[704,128]{1,0:T(8,128)(2,1)S(1)} collective-permute-done((bf16[704,128]{1,0:T(8,128)(2,1)S(1)}, bf16[704,128]{1,0:T(8,128)(2,1)S(1)}, u32[]{:S(2)}, u32[]{:S(2)}) %collective-permute-start.47) | collective-permute-done | bytes 180256 | tf_op jit(solution)/shard_map/ppermute | solution.py:123
  231.8 2.3 collective-permute-done.49.refs_7_
  234.1 5.4 %shard_map.189 = (bf16[4,512,256]{2,1,0:T(8,128)(2,1)}, bf16[4,512,256]{2,1,0:T(8,128)(2,1)}) custom-call(s32[5]{0:T(128)} %stack.89.spot_ref, bf16[704,128]{1,0:T(8,128)(2,1)} %get-tuple-element.49.refs_0_, bf16[704,128]{1,0:T(8,128)(2,1)} %copy-done.31, bf16[704,128]{1,0:T(8,128)(2,1)} %copy-done.30, bf16[704,128]{1,0:T(8,128)(2,1)} %copy-done.32, ...), custom_call_target="tpu_custom_call" | custom-call | tf_op jit(solution)/shard_map/pallas_call | solution.py:398
  240.0 1.4 collective-permute-start.41
  241.4 1.9 collective-permute-start.42
  244.0 1.4 collective-permute-start.52
  245.4 4.5 %collective-permute-done.40 = bf16[512,256]{1,0:T(8,128)(2,1)S(1)} collective-permute-done((bf16[512,256]{1,0:T(8,128)(2,1)S(1)}, bf16[512,256]{1,0:T(8,128)(2,1)S(1)}, u32[]{:S(2)}, u32[]{:S(2)}) %collective-permute-start.40) | collective-permute-done | bytes 262176 | tf_op jit(solution)/shard_map/ppermute | solution.py:123
  250.1 4.9 %collective-permute-done.41 = bf16[512,256]{1,0:T(8,128)(2,1)S(1)} collective-permute-done((bf16[512,256]{1,0:T(8,128)(2,1)S(1)}, bf16[512,256]{1,0:T(8,128)(2,1)S(1)}, u32[]{:S(2)}, u32[]{:S(2)}) %collective-permute-start.41) | collective-permute-done | bytes 262176 | tf_op jit(solution)/shard_map/ppermute | solution.py:123
  255.1 6.2 %collective-permute-done.51 = bf16[512,256]{1,0:T(8,128)(2,1)S(1)} collective-permute-done((bf16[512,256]{1,0:T(8,128)(2,1)S(1)}, bf16[512,256]{1,0:T(8,128)(2,1)S(1)}, u32[]{:S(2)}, u32[]{:S(2)}) %collective-permute-start.51) | collective-permute-done | bytes 262176 | tf_op jit(solution)/shard_map/ppermute | solution.py:123
  261.2 4.2 %collective-permute-done.52 = bf16[512,256]{1,0:T(8,128)(2,1)S(1)} collective-permute-done((bf16[512,256]{1,0:T(8,128)(2,1)S(1)}, bf16[512,256]{1,0:T(8,128)(2,1)S(1)}, u32[]{:S(2)}, u32[]{:S(2)}) %collective-permute-start.52) | collective-permute-done | bytes 262176 | tf_op jit(solution)/shard_map/ppermute | solution.py:123
  265.7 0.8 copy.23
  (154 shorter events, 10.3 us)
Async XLA Ops:
  0.0 28.6 %collective-permute-start.5 = (bf16[1024,256]{1,0:T(8,128)(2,1)}, bf16[1024,256]{1,0:T(8,128)(2,1)S(1)}, u32[]{:S(2)}, u32[]{:S(2)}) collective-permute-start(bf16[1024,256]{1,0:T(8,128)(2,1)} %refs_0_.4), channel_id=1, source_target_pairs={{0,4},{4,0},{1,5},{5,1},{2,6},{6,2},{3,7},{7,3},{8,12},{12,8},{9,1... | collective-permute-start | bytes 1572872 | tf_op jit(solution)/shard_map/ppermute | solution.py:123
  6.4 15.8 %collective-permute-start = (bf16[320,256]{1,0:T(8,128)(2,1)}, bf16[320,256]{1,0:T(8,128)(2,1)S(1)}, u32[]{:S(2)}, u32[]{:S(2)}) collective-permute-start(bf16[320,256]{1,0:T(8,128)(2,1)} %get-tuple-element.30), channel_id=1, source_target_pairs={{0,4},{4,0},{1,5},{5,1},{2,6},{6,2},{3,7},{7,3},{8,12},{12,8},{9,1... | collective-permute-start | bytes 491528 | tf_op jit(solution)/shard_map/ppermute | solution.py:123
  6.5 16.3 %collective-permute-start.1 = (bf16[320,256]{1,0:T(8,128)(2,1)}, bf16[320,256]{1,0:T(8,128)(2,1)S(1)}, u32[]{:S(2)}, u32[]{:S(2)}) collective-permute-start(bf16[320,256]{1,0:T(8,128)(2,1)} %get-tuple-element.32), channel_id=1, source_target_pairs={{0,8},{8,0},{1,9},{9,1},{2,10},{10,2},{3,11},{11,3},{4,12},{12,4},... | collective-permute-start | bytes 491528 | tf_op jit(solution)/shard_map/ppermute | solution.py:123
  9.5 18.4 %collective-permute-start.2 = (bf16[320,256]{1,0:T(8,128)(2,1)}, bf16[320,256]{1,0:T(8,128)(2,1)S(1)}, u32[]{:S(2)}, u32[]{:S(2)}) collective-permute-start(bf16[320,256]{1,0:T(8,128)(2,1)} %get-tuple-element.30), channel_id=1, source_target_pairs={{0,12},{4,8},{8,4},{12,0},{1,13},{5,9},{9,5},{13,1},{2,14},{6,10},... | collective-permute-start | bytes 491528 | tf_op jit(solution)/shard_map/ppermute | solution.py:123
  10.8 21.9 %collective-permute-start.7 = (bf16[1024,256]{1,0:T(8,128)(2,1)}, bf16[1024,256]{1,0:T(8,128)(2,1)S(1)}, u32[]{:S(2)}, u32[]{:S(2)}) collective-permute-start(bf16[1024,256]{1,0:T(8,128)(2,1)} %refs_0_.4), channel_id=1, source_target_pairs={{0,1},{1,0},{2,3},{3,2},{4,5},{5,4},{6,7},{7,6},{8,9},{9,8},{10,11... | collective-permute-start | bytes 1572872 | tf_op jit(solution)/shard_map/ppermute | solution.py:123
  22.2 20.0 %collective-permute-start.4 = (bf16[1024,256]{1,0:T(8,128)(2,1)S(1)}, bf16[1024,256]{1,0:T(8,128)(2,1)S(1)}, u32[]{:S(2)}, u32[]{:S(2)}) collective-permute-start(bf16[1024,256]{1,0:T(8,128)(2,1)S(1)} %copy-done.9), channel_id=1, source_target_pairs={{0,16},{16,0},{1,17},{17,1},{2,18},{18,2},{3,19},{19,3},{4,20},{20... | collective-permute-start | bytes 1572872 | tf_op jit(solution)/shard_map/ppermute | solution.py:123
  28.6 12.8 %collective-permute-start.9 = (bf16[1024,256]{1,0:T(8,128)(2,1)S(1)}, bf16[1024,256]{1,0:T(8,128)(2,1)S(1)}, u32[]{:S(2)}, u32[]{:S(2)}) collective-permute-start(bf16[1024,256]{1,0:T(8,128)(2,1)S(1)} %collective-permute-done.5.refs_2_), channel_id=1, source_target_pairs={{0,1},{1,0},{2,3},{3,2},{4,5},{5,4},{6,7},{7,6},{8,9},{9,8},{10,11... | collective-permute-start | bytes 1572872 | tf_op jit(solution)/shard_map/ppermute | solution.py:123
  30.2 14.4 %collective-permute-start.11 = (bf16[4,192,256]{2,1,0:T(8,128)(2,1)S(1)}, bf16[4,192,256]{2,1,0:T(8,128)(2,1)}, u32[]{:S(2)}, u32[]{:S(2)}) collective-permute-start(bf16[4,192,256]{2,1,0:T(8,128)(2,1)S(1)} %pad_maximum_fusion.4.refs_8_), channel_id=1, source_target_pairs={{0,2},{2,0},{1,3},{3,1},{4,6},{6,4},{5,7},{7,5},{8,10},{10,8},{9,1... | collective-permute-start | bytes 1179656 | tf_op jit(solution)/shard_map/ppermute | solution.py:123
  32.6 12.0 %collective-permute-start.6 = (bf16[1024,256]{1,0:T(8,128)(2,1)S(1)}, bf16[1024,256]{1,0:T(8,128)(2,1)}, u32[]{:S(2)}, u32[]{:S(2)}) collective-permute-start(bf16[1024,256]{1,0:T(8,128)(2,1)S(1)} %collective-permute-done.5.refs_2_), channel_id=1, source_target_pairs={{0,16},{16,0},{1,17},{17,1},{2,18},{18,2},{3,19},{19,3},{4,20},{20... | collective-permute-start | bytes 1572872 | tf_op jit(solution)/shard_map/ppermute | solution.py:123
  32.7 11.9 %collective-permute-start.8 = (bf16[1024,256]{1,0:T(8,128)(2,1)S(1)}, bf16[1024,256]{1,0:T(8,128)(2,1)}, u32[]{:S(2)}, u32[]{:S(2)}) collective-permute-start(bf16[1024,256]{1,0:T(8,128)(2,1)S(1)} %collective-permute-done.7.refs_4_), channel_id=1, source_target_pairs={{0,16},{16,0},{1,17},{17,1},{2,18},{18,2},{3,19},{19,3},{4,20},{20... | collective-permute-start | bytes 1572872 | tf_op jit(solution)/shard_map/ppermute | solution.py:123
  41.4 3.2 %collective-permute-start.10 = (bf16[1024,256]{1,0:T(8,128)(2,1)S(1)}, bf16[1024,256]{1,0:T(8,128)(2,1)}, u32[]{:S(2)}, u32[]{:S(2)}) collective-permute-start(bf16[1024,256]{1,0:T(8,128)(2,1)S(1)} %collective-permute-done.9.refs_6_), channel_id=1, source_target_pairs={{0,16},{16,0},{1,17},{17,1},{2,18},{18,2},{3,19},{19,3},{4,20},{20... | collective-permute-start | bytes 1572872 | tf_op jit(solution)/shard_map/ppermute | solution.py:123
  42.3 8.8 %collective-permute-start.3 = (bf16[4,128,256]{2,1,0:T(8,128)(2,1)}, bf16[4,128,256]{2,1,0:T(8,128)(2,1)S(1)}, u32[]{:S(2)}, u32[]{:S(2)}) collective-permute-start(bf16[4,128,256]{2,1,0:T(8,128)(2,1)} %get-tuple-element.64), channel_id=1, source_target_pairs={{0,2},{2,0},{1,3},{3,1},{4,6},{6,4},{5,7},{7,5},{8,10},{10,8},{9,1... | collective-permute-start | bytes 786440 | tf_op jit(solution)/shard_map/ppermute | solution.py:123
  51.2 45.9 %collective-permute-start.16 = (bf16[2,4,128,256]{3,2,1,0:T(8,128)(2,1)S(1)}, bf16[2,4,128,256]{3,2,1,0:T(8,128)(2,1)S(1)}, u32[]{:S(2)}, u32[]{:S(2)}) collective-permute-start(bf16[2,4,128,256]{3,2,1,0:T(8,128)(2,1)S(1)} %get-tuple-element.62.refs_2_), channel_id=1, source_target_pairs={{0,1},{1,0},{2,3},{3,2},{4,5},{5,4},{6,7},{7,6},{8,9},{9,8},{10,11... | collective-permute-start | bytes 1572872 | tf_op jit(solution)/shard_map/ppermute | solution.py:123
  52.7 11.3 %collective-permute-start.19 = (bf16[704,128]{1,0:T(8,128)(2,1)S(1)}, bf16[704,128]{1,0:T(8,128)(2,1)S(1)}, u32[]{:S(2)}, u32[]{:S(2)}) collective-permute-start(bf16[704,128]{1,0:T(8,128)(2,1)S(1)} %copy-done.27), channel_id=1, source_target_pairs={{0,8},{8,0},{1,9},{9,1},{2,10},{10,2},{3,11},{11,3},{4,12},{12,4},... | collective-permute-start | bytes 540680 | tf_op jit(solution)/shard_map/ppermute | solution.py:123
  52.7 17.9 %collective-permute-start.18 = (bf16[704,128]{1,0:T(8,128)(2,1)S(1)}, bf16[704,128]{1,0:T(8,128)(2,1)S(1)}, u32[]{:S(2)}, u32[]{:S(2)}) collective-permute-start(bf16[704,128]{1,0:T(8,128)(2,1)S(1)} %copy-done.39), channel_id=1, source_target_pairs={{0,4},{4,0},{1,5},{5,1},{2,6},{6,2},{3,7},{7,3},{8,12},{12,8},{9,1... | collective-permute-start | bytes 540680 | tf_op jit(solution)/shard_map/ppermute | solution.py:123
  56.4 69.2 %copy-start.38 = (bf16[64,1024]{1,0:T(8,128)(2,1)S(1)}, bf16[64,1024]{1,0:T(8,128)(2,1)}, u32[]{:S(2)}) copy-start(bf16[64,1024]{1,0:T(8,128)(2,1)} %get-tuple-element.37) | copy-start | bytes 393220
  60.8 25.2 %collective-permute-start.33 = (bf16[704,256]{1,0:T(8,128)(2,1)}, bf16[704,256]{1,0:T(8,128)(2,1)S(1)}, u32[]{:S(2)}, u32[]{:S(2)}) collective-permute-start(bf16[704,256]{1,0:T(8,128)(2,1)} %get-tuple-element.45.refs_0_), channel_id=1, source_target_pairs={{0,8},{8,0},{1,9},{9,1},{2,10},{10,2},{3,11},{11,3},{4,12},{12,4},... | collective-permute-start | bytes 1081352 | tf_op jit(solution)/shard_map/ppermute | solution.py:123
  60.9 35.5 %collective-permute-start.32 = (bf16[704,256]{1,0:T(8,128)(2,1)}, bf16[704,256]{1,0:T(8,128)(2,1)S(1)}, u32[]{:S(2)}, u32[]{:S(2)}) collective-permute-start(bf16[704,256]{1,0:T(8,128)(2,1)} %get-tuple-element.46), channel_id=1, source_target_pairs={{0,4},{4,0},{1,5},{5,1},{2,6},{6,2},{3,7},{7,3},{8,12},{12,8},{9,1... | collective-permute-start | bytes 1081352 | tf_op jit(solution)/shard_map/ppermute | solution.py:123
  64.0 74.2 %copy-start.28 = (bf16[704,128]{1,0:T(8,128)(2,1)}, bf16[704,128]{1,0:T(8,128)(2,1)S(1)}, u32[]{:S(2)}) copy-start(bf16[704,128]{1,0:T(8,128)(2,1)S(1)} %collective-permute-done.19.refs_2_) | copy-start | bytes 540676
  64.0 20.4 %collective-permute-start.20 = (bf16[704,128]{1,0:T(8,128)(2,1)S(1)}, bf16[704,128]{1,0:T(8,128)(2,1)}, u32[]{:S(2)}, u32[]{:S(2)}) collective-permute-start(bf16[704,128]{1,0:T(8,128)(2,1)S(1)} %copy-done.39), channel_id=1, source_target_pairs={{0,12},{4,8},{8,4},{12,0},{1,13},{5,9},{9,5},{13,1},{2,14},{6,10},... | collective-permute-start | bytes 540680 | tf_op jit(solution)/shard_map/ppermute | solution.py:123
  70.7 67.5 %copy-start.29 = (bf16[704,128]{1,0:T(8,128)(2,1)}, bf16[704,128]{1,0:T(8,128)(2,1)S(1)}, u32[]{:S(2)}) copy-start(bf16[704,128]{1,0:T(8,128)(2,1)S(1)} %collective-permute-done.18.refs_1_) | copy-start | bytes 540676
  70.7 28.8 %collective-permute-start.34 = (bf16[704,256]{1,0:T(8,128)(2,1)}, bf16[704,256]{1,0:T(8,128)(2,1)S(1)}, u32[]{:S(2)}, u32[]{:S(2)}) collective-permute-start(bf16[704,256]{1,0:T(8,128)(2,1)} %get-tuple-element.46), channel_id=1, source_target_pairs={{0,12},{4,8},{8,4},{12,0},{1,13},{5,9},{9,5},{13,1},{2,14},{6,10},... | collective-permute-start | bytes 1081352 | tf_op jit(solution)/shard_map/ppermute | solution.py:123
  84.5 15.2 %collective-permute-start.35 = (bf16[704,256]{1,0:T(8,128)(2,1)}, bf16[704,256]{1,0:T(8,128)(2,1)S(1)}, u32[]{:S(2)}, u32[]{:S(2)}) collective-permute-start(bf16[704,256]{1,0:T(8,128)(2,1)} %get-tuple-element.45.refs_0_), channel_id=1, source_target_pairs={{0,2},{2,0},{1,3},{3,1},{4,6},{6,4},{5,7},{7,5},{8,10},{10,8},{9,1... | collective-permute-start | bytes 1081352 | tf_op jit(solution)/shard_map/ppermute | solution.py:123
  86.0 101.2 %copy-start.15 = (bf16[704,256]{1,0:T(8,128)(2,1)}, bf16[704,256]{1,0:T(8,128)(2,1)S(1)}, u32[]{:S(2)}) copy-start(bf16[704,256]{1,0:T(8,128)(2,1)S(1)} %collective-permute-done.33.refs_2_) | copy-start | bytes 1081348
  86.0 39.7 %collective-permute-start.26 = (bf16[704,256]{1,0:T(8,128)(2,1)}, bf16[704,256]{1,0:T(8,128)(2,1)S(1)}, u32[]{:S(2)}, u32[]{:S(2)}) collective-permute-start(bf16[704,256]{1,0:T(8,128)(2,1)} %get-tuple-element.42.refs_0_), channel_id=1, source_target_pairs={{0,8},{8,0},{1,9},{9,1},{2,10},{10,2},{3,11},{11,3},{4,12},{12,4},... | collective-permute-start | bytes 1081352 | tf_op jit(solution)/shard_map/ppermute | solution.py:123
  96.4 90.8 %copy-start.16 = (bf16[704,256]{1,0:T(8,128)(2,1)}, bf16[704,256]{1,0:T(8,128)(2,1)S(1)}, u32[]{:S(2)}) copy-start(bf16[704,256]{1,0:T(8,128)(2,1)S(1)} %collective-permute-done.32.refs_1_) | copy-start | bytes 1081348
  96.4 29.3 %collective-permute-start.25 = (bf16[704,256]{1,0:T(8,128)(2,1)}, bf16[704,256]{1,0:T(8,128)(2,1)S(1)}, u32[]{:S(2)}, u32[]{:S(2)}) collective-permute-start(bf16[704,256]{1,0:T(8,128)(2,1)} %get-tuple-element.43), channel_id=1, source_target_pairs={{0,4},{4,0},{1,5},{5,1},{2,6},{6,2},{3,7},{7,3},{8,12},{12,8},{9,1... | collective-permute-start | bytes 1081352 | tf_op jit(solution)/shard_map/ppermute | solution.py:123
  97.1 82.3 %copy-start.3 = (bf16[2,4,128,256]{3,2,1,0:T(8,128)(2,1)}, bf16[2,4,128,256]{3,2,1,0:T(8,128)(2,1)S(1)}, u32[]{:S(2)}) copy-start(bf16[2,4,128,256]{3,2,1,0:T(8,128)(2,1)S(1)} %collective-permute-done.16.refs_3_) | copy-start | bytes 1572868
  97.1 29.2 %collective-permute-start.27 = (bf16[704,256]{1,0:T(8,128)(2,1)}, bf16[704,256]{1,0:T(8,128)(2,1)}, u32[]{:S(2)}, u32[]{:S(2)}) collective-permute-start(bf16[704,256]{1,0:T(8,128)(2,1)} %get-tuple-element.43), channel_id=1, source_target_pairs={{0,12},{4,8},{8,4},{12,0},{1,13},{5,9},{9,5},{13,1},{2,14},{6,10},... | collective-permute-start | bytes 1081352 | tf_op jit(solution)/shard_map/ppermute | solution.py:123
  99.5 78.2 %copy-start.17 = (bf16[704,256]{1,0:T(8,128)(2,1)}, bf16[704,256]{1,0:T(8,128)(2,1)S(1)}, u32[]{:S(2)}) copy-start(bf16[704,256]{1,0:T(8,128)(2,1)S(1)} %collective-permute-done.34.refs_3_) | copy-start | bytes 1081348
  99.5 78.1 %collective-permute-start.17 = (bf16[2,2,4,128,256]{4,3,2,1,0:T(8,128)(2,1)S(1)}, bf16[2,2,4,128,256]{4,3,2,1,0:T(8,128)(2,1)S(1)}, u32[]{:S(2)}, u32[]{:S(2)}) collective-permute-start(bf16[2,2,4,128,256]{4,3,2,1,0:T(8,128)(2,1)S(1)} %pad_maximum_fusion), channel_id=1, source_target_pairs={{0,16},{16,0},{1,17},{17,1},{2,18},{18,2},{3,19},{19,3},{4,20},{20... | collective-permute-start | bytes 3145736 | tf_op jit(solution)/shard_map/ppermute | solution.py:123
  99.6 79.6 %copy-start.19 = (bf16[704,256]{1,0:T(8,128)(2,1)}, bf16[704,256]{1,0:T(8,128)(2,1)S(1)}, u32[]{:S(2)}) copy-start(bf16[704,256]{1,0:T(8,128)(2,1)S(1)} %collective-permute-done.35.refs_4_) | copy-start | bytes 1081348
  99.6 38.6 %collective-permute-start.28 = (bf16[704,256]{1,0:T(8,128)(2,1)}, bf16[704,256]{1,0:T(8,128)(2,1)}, u32[]{:S(2)}, u32[]{:S(2)}) collective-permute-start(bf16[704,256]{1,0:T(8,128)(2,1)} %get-tuple-element.42.refs_0_), channel_id=1, source_target_pairs={{0,2},{2,0},{1,3},{3,1},{4,6},{6,4},{5,7},{7,5},{8,10},{10,8},{9,1... | collective-permute-start | bytes 1081352 | tf_op jit(solution)/shard_map/ppermute | solution.py:123
  125.7 53.6 %copy-start.18 = (bf16[704,256]{1,0:T(8,128)(2,1)}, bf16[704,256]{1,0:T(8,128)(2,1)S(1)}, u32[]{:S(2)}) copy-start(bf16[704,256]{1,0:T(8,128)(2,1)S(1)} %collective-permute-done.26.refs_2_) | copy-start | bytes 1081348
  125.7 7.8 %collective-permute-start.12 = (bf16[64,1024]{1,0:T(8,128)(2,1)S(1)}, bf16[64,1024]{1,0:T(8,128)(2,1)S(1)}, u32[]{:S(2)}, u32[]{:S(2)}) collective-permute-start(bf16[64,1024]{1,0:T(8,128)(2,1)S(1)} %copy-done.38), channel_id=1, source_target_pairs={{0,4},{4,0},{1,5},{5,1},{2,6},{6,2},{3,7},{7,3},{8,12},{12,8},{9,1... | collective-permute-start | bytes 393224 | tf_op jit(solution)/shard_map/ppermute | solution.py:123
  125.7 53.6 %copy-start.20 = (bf16[704,256]{1,0:T(8,128)(2,1)}, bf16[704,256]{1,0:T(8,128)(2,1)S(1)}, u32[]{:S(2)}) copy-start(bf16[704,256]{1,0:T(8,128)(2,1)S(1)} %collective-permute-done.25.refs_1_) | copy-start | bytes 1081348
  125.7 9.3 %collective-permute-start.13 = (bf16[64,1024]{1,0:T(8,128)(2,1)S(1)}, bf16[64,1024]{1,0:T(8,128)(2,1)S(1)}, u32[]{:S(2)}, u32[]{:S(2)}) collective-permute-start(bf16[64,1024]{1,0:T(8,128)(2,1)S(1)} %copy-done.38), channel_id=1, source_target_pairs={{0,1},{1,0},{2,3},{3,2},{4,5},{5,4},{6,7},{7,6},{8,9},{9,8},{10,11... | collective-permute-start | bytes 393224 | tf_op jit(solution)/shard_map/ppermute | solution.py:123
  126.3 10.4 %collective-permute-start.14 = (bf16[64,1024]{1,0:T(8,128)(2,1)S(1)}, bf16[64,1024]{1,0:T(8,128)(2,1)S(1)}, u32[]{:S(2)}, u32[]{:S(2)}) collective-permute-start(bf16[64,1024]{1,0:T(8,128)(2,1)S(1)} %copy-done.38), channel_id=1, source_target_pairs={{0,5},{1,4},{4,1},{5,0},{2,7},{3,6},{6,3},{7,2},{8,13},{9,12},{12,... | collective-permute-start | bytes 393224 | tf_op jit(solution)/shard_map/ppermute | solution.py:123
  133.5 11.3 %collective-permute-start.37 = (bf16[704,256]{1,0:T(8,128)(2,1)S(1)}, bf16[704,256]{1,0:T(8,128)(2,1)S(1)}, u32[]{:S(2)}, u32[]{:S(2)}) collective-permute-start(bf16[704,256]{1,0:T(8,128)(2,1)S(1)} %collective-permute-done.33.refs_2_), channel_id=1, source_target_pairs={{0,2},{2,0},{1,3},{3,1},{4,6},{6,4},{5,7},{7,5},{8,10},{10,8},{9,1... | collective-permute-start | bytes 1081352 | tf_op jit(solution)/shard_map/ppermute | solution.py:123
  135.0 17.5 %collective-permute-start.36 = (bf16[704,256]{1,0:T(8,128)(2,1)S(1)}, bf16[704,256]{1,0:T(8,128)(2,1)S(1)}, u32[]{:S(2)}, u32[]{:S(2)}) collective-permute-start(bf16[704,256]{1,0:T(8,128)(2,1)S(1)} %collective-permute-done.32.refs_1_), channel_id=1, source_target_pairs={{0,2},{2,0},{1,3},{3,1},{4,6},{6,4},{5,7},{7,5},{8,10},{10,8},{9,1... | collective-permute-start | bytes 1081352 | tf_op jit(solution)/shard_map/ppermute | solution.py:123
  136.7 23.5 %collective-permute-start.38 = (bf16[704,256]{1,0:T(8,128)(2,1)S(1)}, bf16[704,256]{1,0:T(8,128)(2,1)S(1)}, u32[]{:S(2)}, u32[]{:S(2)}) collective-permute-start(bf16[704,256]{1,0:T(8,128)(2,1)S(1)} %collective-permute-done.34.refs_3_), channel_id=1, source_target_pairs={{0,2},{2,0},{1,3},{3,1},{4,6},{6,4},{5,7},{7,5},{8,10},{10,8},{9,1... | collective-permute-start | bytes 1081352 | tf_op jit(solution)/shard_map/ppermute | solution.py:123
  138.3 38.9 %collective-permute-start.15 = (bf16[4,64,1024]{2,1,0:T(8,128)(2,1)S(1)}, bf16[4,64,1024]{2,1,0:T(8,128)(2,1)S(1)}, u32[]{:S(2)}, u32[]{:S(2)}) collective-permute-start(bf16[4,64,1024]{2,1,0:T(8,128)(2,1)S(1)} %pad_maximum_fusion.1.refs_0_), channel_id=1, source_target_pairs={{0,16},{16,0},{1,17},{17,1},{2,18},{18,2},{3,19},{19,3},{4,20},{20... | collective-permute-start | bytes 1572872 | tf_op jit(solution)/shard_map/ppermute | solution.py:123
  144.7 23.2 %collective-permute-start.30 = (bf16[704,256]{1,0:T(8,128)(2,1)S(1)}, bf16[704,256]{1,0:T(8,128)(2,1)S(1)}, u32[]{:S(2)}, u32[]{:S(2)}) collective-permute-start(bf16[704,256]{1,0:T(8,128)(2,1)S(1)} %collective-permute-done.26.refs_2_), channel_id=1, source_target_pairs={{0,2},{2,0},{1,3},{3,1},{4,6},{6,4},{5,7},{7,5},{8,10},{10,8},{9,1... | collective-permute-start | bytes 1081352 | tf_op jit(solution)/shard_map/ppermute | solution.py:123
  152.5 23.2 %collective-permute-start.29 = (bf16[704,256]{1,0:T(8,128)(2,1)S(1)}, bf16[704,256]{1,0:T(8,128)(2,1)S(1)}, u32[]{:S(2)}, u32[]{:S(2)}) collective-permute-start(bf16[704,256]{1,0:T(8,128)(2,1)S(1)} %collective-permute-done.25.refs_1_), channel_id=1, source_target_pairs={{0,2},{2,0},{1,3},{3,1},{4,6},{6,4},{5,7},{7,5},{8,10},{10,8},{9,1... | collective-permute-start | bytes 1081352 | tf_op jit(solution)/shard_map/ppermute | solution.py:123
  160.2 34.7 %collective-permute-start.31 = (bf16[704,256]{1,0:T(8,128)(2,1)}, bf16[704,256]{1,0:T(8,128)(2,1)}, u32[]{:S(2)}, u32[]{:S(2)}) collective-permute-start(bf16[704,256]{1,0:T(8,128)(2,1)} %collective-permute-done.27.refs_3_), channel_id=1, source_target_pairs={{0,2},{2,0},{1,3},{3,1},{4,6},{6,4},{5,7},{7,5},{8,10},{10,8},{9,1... | collective-permute-start | bytes 1081352 | tf_op jit(solution)/shard_map/ppermute | solution.py:123
  167.9 34.8 %collective-permute-start.21 = (bf16[704,128]{1,0:T(8,128)(2,1)S(1)}, bf16[704,128]{1,0:T(8,128)(2,1)}, u32[]{:S(2)}, u32[]{:S(2)}) collective-permute-start(bf16[704,128]{1,0:T(8,128)(2,1)S(1)} %copy-done.27), channel_id=1, source_target_pairs={{0,2},{2,0},{1,3},{3,1},{4,6},{6,4},{5,7},{7,5},{8,10},{10,8},{9,1... | collective-permute-start | bytes 540680 | tf_op jit(solution)/shard_map/ppermute | solution.py:123
  175.6 27.1 %collective-permute-start.23 = (bf16[704,128]{1,0:T(8,128)(2,1)}, bf16[704,128]{1,0:T(8,128)(2,1)}, u32[]{:S(2)}, u32[]{:S(2)}) collective-permute-start(bf16[704,128]{1,0:T(8,128)(2,1)} %copy-done.28), channel_id=1, source_target_pairs={{0,2},{2,0},{1,3},{3,1},{4,6},{6,4},{5,7},{7,5},{8,10},{10,8},{9,1... | collective-permute-start | bytes 540680 | tf_op jit(solution)/shard_map/ppermute | solution.py:123
  177.2 25.5 %collective-permute-start.22 = (bf16[704,128]{1,0:T(8,128)(2,1)}, bf16[704,128]{1,0:T(8,128)(2,1)}, u32[]{:S(2)}, u32[]{:S(2)}) collective-permute-start(bf16[704,128]{1,0:T(8,128)(2,1)} %copy-done.29), channel_id=1, source_target_pairs={{0,2},{2,0},{1,3},{3,1},{4,6},{6,4},{5,7},{7,5},{8,10},{10,8},{9,1... | collective-permute-start | bytes 540680 | tf_op jit(solution)/shard_map/ppermute | solution.py:123
  177.7 25.0 %collective-permute-start.24 = (bf16[704,128]{1,0:T(8,128)(2,1)}, bf16[704,128]{1,0:T(8,128)(2,1)}, u32[]{:S(2)}, u32[]{:S(2)}) collective-permute-start(bf16[704,128]{1,0:T(8,128)(2,1)} %collective-permute-done.20.refs_3_), channel_id=1, source_target_pairs={{0,2},{2,0},{1,3},{3,1},{4,6},{6,4},{5,7},{7,5},{8,10},{10,8},{9,1... | collective-permute-start | bytes 540680 | tf_op jit(solution)/shard_map/ppermute | solution.py:123
  208.1 31.4 %collective-permute-start.39 = (bf16[4,512,256]{2,1,0:T(8,128)(2,1)}, bf16[4,512,256]{2,1,0:T(8,128)(2,1)S(1)}, u32[]{:S(2)}, u32[]{:S(2)}) collective-permute-start(bf16[4,512,256]{2,1,0:T(8,128)(2,1)} %get-tuple-element.48), channel_id=1, source_target_pairs={{0,16},{16,0},{1,17},{17,1},{2,18},{18,2},{3,19},{19,3},{4,20},{20... | collective-permute-start | bytes 3145736 | tf_op jit(solution)/shard_map/ppermute | solution.py:123
  208.1 11.8 %collective-permute-start.44 = (bf16[704,128]{1,0:T(8,128)(2,1)S(1)}, bf16[704,128]{1,0:T(8,128)(2,1)S(1)}, u32[]{:S(2)}, u32[]{:S(2)}) collective-permute-start(bf16[704,128]{1,0:T(8,128)(2,1)S(1)} %copy-done.26), channel_id=1, source_target_pairs={{0,8},{8,0},{1,9},{9,1},{2,10},{10,2},{3,11},{11,3},{4,12},{12,4},... | collective-permute-start | bytes 540680 | tf_op jit(solution)/shard_map/ppermute | solution.py:123
  208.2 12.3 %collective-permute-start.43 = (bf16[704,128]{1,0:T(8,128)(2,1)}, bf16[704,128]{1,0:T(8,128)(2,1)S(1)}, u32[]{:S(2)}, u32[]{:S(2)}) collective-permute-start(bf16[704,128]{1,0:T(8,128)(2,1)} %get-tuple-element.50), channel_id=1, source_target_pairs={{0,4},{4,0},{1,5},{5,1},{2,6},{6,2},{3,7},{7,3},{8,12},{12,8},{9,1... | collective-permute-start | bytes 540680 | tf_op jit(solution)/shard_map/ppermute | solution.py:123
  209.9 13.4 %collective-permute-start.45 = (bf16[704,128]{1,0:T(8,128)(2,1)}, bf16[704,128]{1,0:T(8,128)(2,1)S(1)}, u32[]{:S(2)}, u32[]{:S(2)}) collective-permute-start(bf16[704,128]{1,0:T(8,128)(2,1)} %get-tuple-element.50), channel_id=1, source_target_pairs={{0,12},{4,8},{8,4},{12,0},{1,13},{5,9},{9,5},{13,1},{2,14},{6,10},... | collective-permute-start | bytes 540680 | tf_op jit(solution)/shard_map/ppermute | solution.py:123
  212.6 11.4 %collective-permute-start.46 = (bf16[704,128]{1,0:T(8,128)(2,1)S(1)}, bf16[704,128]{1,0:T(8,128)(2,1)S(1)}, u32[]{:S(2)}, u32[]{:S(2)}) collective-permute-start(bf16[704,128]{1,0:T(8,128)(2,1)S(1)} %copy-done.26), channel_id=1, source_target_pairs={{0,2},{2,0},{1,3},{3,1},{4,6},{6,4},{5,7},{7,5},{8,10},{10,8},{9,1... | collective-permute-start | bytes 540680 | tf_op jit(solution)/shard_map/ppermute | solution.py:123
  219.9 7.4 %collective-permute-start.48 = (bf16[704,128]{1,0:T(8,128)(2,1)S(1)}, bf16[704,128]{1,0:T(8,128)(2,1)S(1)}, u32[]{:S(2)}, u32[]{:S(2)}) collective-permute-start(bf16[704,128]{1,0:T(8,128)(2,1)S(1)} %collective-permute-done.44.refs_2_), channel_id=1, source_target_pairs={{0,2},{2,0},{1,3},{3,1},{4,6},{6,4},{5,7},{7,5},{8,10},{10,8},{9,1... | collective-permute-start | bytes 540680 | tf_op jit(solution)/shard_map/ppermute | solution.py:123
  220.5 10.7 %collective-permute-start.47 = (bf16[704,128]{1,0:T(8,128)(2,1)S(1)}, bf16[704,128]{1,0:T(8,128)(2,1)S(1)}, u32[]{:S(2)}, u32[]{:S(2)}) collective-permute-start(bf16[704,128]{1,0:T(8,128)(2,1)S(1)} %collective-permute-done.43.refs_1_), channel_id=1, source_target_pairs={{0,2},{2,0},{1,3},{3,1},{4,6},{6,4},{5,7},{7,5},{8,10},{10,8},{9,1... | collective-permute-start | bytes 540680 | tf_op jit(solution)/shard_map/ppermute | solution.py:123
  223.3 10.8 %collective-permute-start.49 = (bf16[704,128]{1,0:T(8,128)(2,1)S(1)}, bf16[704,128]{1,0:T(8,128)(2,1)}, u32[]{:S(2)}, u32[]{:S(2)}) collective-permute-start(bf16[704,128]{1,0:T(8,128)(2,1)S(1)} %collective-permute-done.45.refs_3_), channel_id=1, source_target_pairs={{0,2},{2,0},{1,3},{3,1},{4,6},{6,4},{5,7},{7,5},{8,10},{10,8},{9,1... | collective-permute-start | bytes 540680 | tf_op jit(solution)/shard_map/ppermute | solution.py:123
  239.5 4.0 %collective-permute-start.50 = (bf16[4,512,256]{2,1,0:T(8,128)(2,1)}, bf16[4,512,256]{2,1,0:T(8,128)(2,1)S(1)}, u32[]{:S(2)}, u32[]{:S(2)}) collective-permute-start(bf16[4,512,256]{2,1,0:T(8,128)(2,1)} %get-tuple-element.52), channel_id=1, source_target_pairs={{0,16},{16,0},{1,17},{17,1},{2,18},{18,2},{3,19},{19,3},{4,20},{20... | collective-permute-start | bytes 3145736 | tf_op jit(solution)/shard_map/ppermute | solution.py:123
  239.8 10.2 %collective-permute-start.40 = (bf16[512,256]{1,0:T(8,128)(2,1)S(1)}, bf16[512,256]{1,0:T(8,128)(2,1)S(1)}, u32[]{:S(2)}, u32[]{:S(2)}) collective-permute-start(bf16[512,256]{1,0:T(8,128)(2,1)S(1)} %get-tuple-element.53), channel_id=1, source_target_pairs={{0,5},{1,4},{4,1},{5,0},{2,7},{3,6},{6,3},{7,2},{8,13},{9,12},{12,... | collective-permute-start | bytes 786440 | tf_op jit(solution)/shard_map/ppermute | solution.py:123
  240.0 15.0 %collective-permute-start.41 = (bf16[512,256]{1,0:T(8,128)(2,1)S(1)}, bf16[512,256]{1,0:T(8,128)(2,1)S(1)}, u32[]{:S(2)}, u32[]{:S(2)}) collective-permute-start(bf16[512,256]{1,0:T(8,128)(2,1)S(1)} %get-tuple-element.55), channel_id=1, source_target_pairs={{0,1},{1,0},{2,3},{3,2},{4,5},{5,4},{6,7},{7,6},{8,9},{9,8},{10,11... | collective-permute-start | bytes 786440 | tf_op jit(solution)/shard_map/ppermute | solution.py:123
  241.4 13.5 %collective-permute-start.42 = (bf16[512,256]{1,0:T(8,128)(2,1)S(1)}, bf16[512,256]{1,0:T(8,128)(2,1)S(1)}, u32[]{:S(2)}, u32[]{:S(2)}) collective-permute-start(bf16[512,256]{1,0:T(8,128)(2,1)S(1)} %get-tuple-element.54), channel_id=1, source_target_pairs={{0,4},{4,0},{1,5},{5,1},{2,6},{6,2},{3,7},{7,3},{8,12},{12,8},{9,1... | collective-permute-start | bytes 786440 | tf_op jit(solution)/shard_map/ppermute | solution.py:123
  243.8 17.5 %collective-permute-start.51 = (bf16[512,256]{1,0:T(8,128)(2,1)S(1)}, bf16[512,256]{1,0:T(8,128)(2,1)S(1)}, u32[]{:S(2)}, u32[]{:S(2)}) collective-permute-start(bf16[512,256]{1,0:T(8,128)(2,1)S(1)} %get-tuple-element.56), channel_id=1, source_target_pairs={{0,5},{1,4},{4,1},{5,0},{2,7},{3,6},{6,3},{7,2},{8,13},{9,12},{12,... | collective-permute-start | bytes 786440 | tf_op jit(solution)/shard_map/ppermute | solution.py:123
  244.0 21.5 %collective-permute-start.52 = (bf16[512,256]{1,0:T(8,128)(2,1)S(1)}, bf16[512,256]{1,0:T(8,128)(2,1)S(1)}, u32[]{:S(2)}, u32[]{:S(2)}) collective-permute-start(bf16[512,256]{1,0:T(8,128)(2,1)S(1)} %get-tuple-element.58), channel_id=1, source_target_pairs={{0,1},{1,0},{2,3},{3,2},{4,5},{5,4},{6,7},{7,6},{8,9},{9,8},{10,11... | collective-permute-start | bytes 786440 | tf_op jit(solution)/shard_map/ppermute | solution.py:123
  250.0 15.6 %collective-permute-start.53 = (bf16[512,256]{1,0:T(8,128)(2,1)S(1)}, bf16[512,256]{1,0:T(8,128)(2,1)S(1)}, u32[]{:S(2)}, u32[]{:S(2)}) collective-permute-start(bf16[512,256]{1,0:T(8,128)(2,1)S(1)} %get-tuple-element.57), channel_id=1, source_target_pairs={{0,4},{4,0},{1,5},{5,1},{2,6},{6,2},{3,7},{7,3},{8,12},{12,8},{9,1... | collective-permute-start | bytes 786440 | tf_op jit(solution)/shard_map/ppermute | solution.py:123
  (30 other events, 435.6 us)

commit v3 on v2

--- a/solution.py
+++ b/solution.py
@@ -510,7 +510,7 @@
         tile((units, tokens)),
         scratch,
     )
-    totals = []
+    out = jnp.zeros((half // depth, 2, lanes, tokens), jnp.bfloat16)
     for chunk in range(2):
         kept, sent = run(
             down_kernel,
@@ -529,8 +529,9 @@
             part = kept[index].astype(jnp.float32) + got[index].astype(jnp.float32)
             part = flip(part.astype(jnp.bfloat16), *way)
             total = total + part.astype(jnp.float32)
-        totals.append(total.astype(jnp.bfloat16).reshape(-1, lanes, tokens))
-    return jnp.stack(totals, axis=1).reshape(half, tokens)
+        total = total.astype(jnp.bfloat16).reshape(-1, 1, lanes, tokens)
+        out = lax.dynamic_update_slice_in_dim(out, total, chunk, 1)
+    return out.reshape(half, tokens)
 
 
 def solution(mesh):

time: 267 us -> 267 us (level)
  no operation moved by 1% of the time
where the time goes in v3:
time: 267 us
  waiting for transfers between devices  132 us (49%)
  starting transfers between devices  77 us (29%)
  Pallas kernels  49.8 us (19%)
  local copies, waits for them, and re-layouts  4.66 us (2%)
    ppermute x54, waiting for transfers between devices, flip(): return lax.ppermute(array, axes, [(i, count - 1 - i) for i in range(count)])  132 us
    ppermute x54, starting transfers between devices, flip(): return lax.ppermute(array, axes, [(i, count - 1 - i) for i in range(count)])  77 us
    pallas_call x6, Pallas kernels, run(): pl.pallas_call(kernel, grid=grid, out_shape=outs, in_specs=[scalars] + in...  39.8 us
    pallas_call x3, Pallas kernels, prepare(): pl.pallas_call(kernel, out_shape=tuple((shaped(*shape) for shape in outs)...  10.1 us
  transfers between devices with their start and end apart: 54, of which 24 were waited for; matrix products, arithmetic and copies ran while one was open for 2% of the time, Pallas kernels for 17%

profile of v3, /device:TPU:0, one launch (start us, length us, event | category | flops | bytes accessed | tf_op | source)
XLA Modules:
  0.0 266.6 jit_solution(10789436075531508117)
XLA Ops:
  0.0 3.1 %collective-permute-start.5 = (bf16[1024,256]{1,0:T(8,128)(2,1)}, bf16[1024,256]{1,0:T(8,128)(2,1)S(1)}, u32[]{:S(2)}, u32[]{:S(2)}) collective-permute-start(bf16[1024,256]{1,0:T(8,128)(2,1)} %refs_0_.4), channel_id=1, source_target_pairs={{0,4},{4,0},{1,5},{5,1},{2,6},{6,2},{3,7},{7,3},{8,12},{12,8},{9,1... | collective-permute-start | bytes 1572872 | tf_op jit(solution)/shard_map/ppermute | solution.py:123
  3.7 2.7 %shard_map.181 = (bf16[320,256]{1,0:T(8,128)(2,1)}, bf16[320,256]{1,0:T(8,128)(2,1)}) custom-call(s32[5]{0:T(128)} %stack.86.spot_ref, f32[256,256]{1,0:T(8,128)} %refs_0_.3, f32[256,256]{1,0:T(8,128)} %refs_1_.2, f32[256,256]{1,0:T(8,128)} %refs_2_.1, f32[2,128]{1,0:T(2,128)} %bitcast.98, f32[2,128]{1,0:T(2,128)} %bitcast.99, f32[2,128]{1,0:T(2,128)} %bitcast.100, ...), custom_call_target="tpu_custom_call" | custom-call | tf_op jit(solution)/shard_map/pallas_call | solution.py:385
  6.5 3.0 %collective-permute-start.1 = (bf16[320,256]{1,0:T(8,128)(2,1)}, bf16[320,256]{1,0:T(8,128)(2,1)S(1)}, u32[]{:S(2)}, u32[]{:S(2)}) collective-permute-start(bf16[320,256]{1,0:T(8,128)(2,1)} %get-tuple-element.32), channel_id=1, source_target_pairs={{0,8},{8,0},{1,9},{9,1},{2,10},{10,2},{3,11},{11,3},{4,12},{12,4},... | collective-permute-start | bytes 491528 | tf_op jit(solution)/shard_map/ppermute | solution.py:123
  9.5 1.3 collective-permute-start.2
  10.8 1.5 collective-permute-start.7
  12.3 3.0 %shard_map.182 = (bf16[704,128]{1,0:T(8,128)(2,1)}, bf16[704,128]{1,0:T(8,128)(2,1)}, bf16[704,128]{1,0:T(8,128)(2,1)}, bf16[704,128]{1,0:T(8,128)(2,1)}) custom-call(s32[5]{0:T(128)} %stack.86.spot_ref, f32[2816,256]{1,0:T(8,128)} %weight_ref.1, f32[2,128]{1,0:T(2,128)} %bitcast.103), custom_call_target="tpu_custom_call" | custom-call | tf_op jit(solution)/shard_map/pallas_call | solution.py:385
  15.3 6.9 %collective-permute-done = bf16[320,256]{1,0:T(8,128)(2,1)S(1)} collective-permute-done((bf16[320,256]{1,0:T(8,128)(2,1)}, bf16[320,256]{1,0:T(8,128)(2,1)S(1)}, u32[]{:S(2)}, u32[]{:S(2)}) %collective-permute-start) | collective-permute-done | bytes 163872 | tf_op jit(solution)/shard_map/ppermute | solution.py:123
  22.7 5.2 %collective-permute-done.2 = bf16[320,256]{1,0:T(8,128)(2,1)S(1)} collective-permute-done((bf16[320,256]{1,0:T(8,128)(2,1)}, bf16[320,256]{1,0:T(8,128)(2,1)S(1)}, u32[]{:S(2)}, u32[]{:S(2)}) %collective-permute-start.2) | collective-permute-done | bytes 163872 | tf_op jit(solution)/shard_map/ppermute | solution.py:123
  28.6 1.5 collective-permute-start.9
  30.2 1.6 collective-permute-start.11
  31.8 0.9 slice_bitcast_fusion.6
  33.2 8.2 %collective-permute-done.9.refs_6_ = bf16[1024,256]{1,0:T(8,128)(2,1)S(1)} collective-permute-done((bf16[1024,256]{1,0:T(8,128)(2,1)S(1)}, bf16[1024,256]{1,0:T(8,128)(2,1)S(1)}, u32[]{:S(2)}, u32[]{:S(2)}) %collective-permute-start.9) | collective-permute-done | bytes 524320 | tf_op jit(solution)/shard_map/ppermute | solution.py:123
  41.4 0.9 fusion.7
  42.3 1.5 collective-permute-start.3
  43.9 0.7 copy.24
  44.7 5.7 %shard_map.183 = (bf16[64,1024]{1,0:T(8,128)(2,1)}, bf16[2048,1024]{1,0:T(8,128)(2,1)}) custom-call(s32[5]{0:T(128)} %stack.86.spot_ref, bf16[1024,256]{1,0:T(8,128)(2,1)} %refs_0_.4, bf16[1024,256]{1,0:T(8,128)(2,1)} %copy-done.12, bf16[1024,256]{1,0:T(8,128)(2,1)} %copy-done.10, bf16[1024,256]{1,0:T(8,128)(2,1)} %collective-permute-done.6.refs_3_, ...), custom_call_target="tpu_custom_call" | custom-call | tf_op jit(solution)/shard_map/pallas_call | solution.py:398
  51.2 1.6 collective-permute-start.16
  52.7 3.7 %collective-permute-start.18 = (bf16[704,128]{1,0:T(8,128)(2,1)S(1)}, bf16[704,128]{1,0:T(8,128)(2,1)S(1)}, u32[]{:S(2)}, u32[]{:S(2)}) collective-permute-start(bf16[704,128]{1,0:T(8,128)(2,1)S(1)} %copy-done.39), channel_id=1, source_target_pairs={{0,4},{4,0},{1,5},{5,1},{2,6},{6,2},{3,7},{7,3},{8,12},{12,8},{9,1... | collective-permute-start | bytes 540680 | tf_op jit(solution)/shard_map/ppermute | solution.py:123
  56.4 4.4 %shard_map.185 = (bf16[704,256]{1,0:T(8,128)(2,1)}, bf16[704,256]{1,0:T(8,128)(2,1)}, bf16[704,256]{1,0:T(8,128)(2,1)}, bf16[704,256]{1,0:T(8,128)(2,1)}) custom-call(s32[5]{0:T(128)} %stack.86.spot_ref, f32[256,2816]{1,0:T(8,128)} %refs_0_.5, f32[256,2816]{1,0:T(8,128)} %refs_1_.3, f32[22,128]{1,0:T(8,128)} %bitcast.94, f32[22,128]{1,0:T(8,128)} %bitcast.95, ...), custom_call_target="tpu_custom_call" | custom-call | tf_op jit(solution)/shard_map/pallas_call | solution.py:385
  60.9 1.2 collective-permute-start.32
  62.1 2.0 collective-permute-done.19.refs_2_
  64.0 6.7 %collective-permute-start.20 = (bf16[704,128]{1,0:T(8,128)(2,1)S(1)}, bf16[704,128]{1,0:T(8,128)(2,1)}, u32[]{:S(2)}, u32[]{:S(2)}) collective-permute-start(bf16[704,128]{1,0:T(8,128)(2,1)S(1)} %copy-done.39), channel_id=1, source_target_pairs={{0,12},{4,8},{8,4},{12,0},{1,13},{5,9},{9,5},{13,1},{2,14},{6,10},... | collective-permute-start | bytes 540680 | tf_op jit(solution)/shard_map/ppermute | solution.py:123
  70.8 13.7 %collective-permute-done.20.refs_3_ = bf16[704,128]{1,0:T(8,128)(2,1)} collective-permute-done((bf16[704,128]{1,0:T(8,128)(2,1)S(1)}, bf16[704,128]{1,0:T(8,128)(2,1)}, u32[]{:S(2)}, u32[]{:S(2)}) %collective-permute-start.20) | collective-permute-done | bytes 180256 | tf_op jit(solution)/shard_map/ppermute | solution.py:123
  84.5 1.5 collective-permute-start.35
  86.0 10.4 %collective-permute-start.26 = (bf16[704,256]{1,0:T(8,128)(2,1)}, bf16[704,256]{1,0:T(8,128)(2,1)S(1)}, u32[]{:S(2)}, u32[]{:S(2)}) collective-permute-start(bf16[704,256]{1,0:T(8,128)(2,1)} %get-tuple-element.42.refs_0_), channel_id=1, source_target_pairs={{0,8},{8,0},{1,9},{9,1},{2,10},{10,2},{3,11},{11,3},{4,12},{12,4},... | collective-permute-start | bytes 1081352 | tf_op jit(solution)/shard_map/ppermute | solution.py:123
  96.4 0.7 collective-permute-start.25
  97.1 2.4 collective-permute-start.27
  100.2 25.5 %collective-permute-done.26.refs_2_ = bf16[704,256]{1,0:T(8,128)(2,1)S(1)} collective-permute-done((bf16[704,256]{1,0:T(8,128)(2,1)}, bf16[704,256]{1,0:T(8,128)(2,1)S(1)}, u32[]{:S(2)}, u32[]{:S(2)}) %collective-permute-start.26) | collective-permute-done | bytes 360480 | tf_op jit(solution)/shard_map/ppermute | solution.py:123
  126.3 7.2 %collective-permute-start.14 = (bf16[64,1024]{1,0:T(8,128)(2,1)S(1)}, bf16[64,1024]{1,0:T(8,128)(2,1)S(1)}, u32[]{:S(2)}, u32[]{:S(2)}) collective-permute-start(bf16[64,1024]{1,0:T(8,128)(2,1)S(1)} %copy-done.38), channel_id=1, source_target_pairs={{0,5},{1,4},{4,1},{5,0},{2,7},{3,6},{6,3},{7,2},{8,13},{9,12},{12,... | collective-permute-start | bytes 393224 | tf_op jit(solution)/shard_map/ppermute | solution.py:123
  133.5 1.5 collective-permute-start.37
  135.5 1.2 collective-permute-done.14
  136.7 1.5 collective-permute-start.38
  138.4 6.4 %collective-permute-done.37.refs_6_ = bf16[704,256]{1,0:T(8,128)(2,1)S(1)} collective-permute-done((bf16[704,256]{1,0:T(8,128)(2,1)S(1)}, bf16[704,256]{1,0:T(8,128)(2,1)S(1)}, u32[]{:S(2)}, u32[]{:S(2)}) %collective-permute-start.37) | collective-permute-done | bytes 360480 | tf_op jit(solution)/shard_map/ppermute | solution.py:123
  144.7 1.5 collective-permute-start.30
  146.3 6.2 %collective-permute-done.36.refs_5_ = bf16[704,256]{1,0:T(8,128)(2,1)S(1)} collective-permute-done((bf16[704,256]{1,0:T(8,128)(2,1)S(1)}, bf16[704,256]{1,0:T(8,128)(2,1)S(1)}, u32[]{:S(2)}, u32[]{:S(2)}) %collective-permute-start.36) | collective-permute-done | bytes 360480 | tf_op jit(solution)/shard_map/ppermute | solution.py:123
  152.5 1.5 collective-permute-start.29
  154.0 6.2 %collective-permute-done.38.refs_7_ = bf16[704,256]{1,0:T(8,128)(2,1)S(1)} collective-permute-done((bf16[704,256]{1,0:T(8,128)(2,1)S(1)}, bf16[704,256]{1,0:T(8,128)(2,1)S(1)}, u32[]{:S(2)}, u32[]{:S(2)}) %collective-permute-start.38) | collective-permute-done | bytes 360480 | tf_op jit(solution)/shard_map/ppermute | solution.py:123
  160.2 1.5 collective-permute-start.31
  161.7 6.2 %collective-permute-done.30.refs_6_ = bf16[704,256]{1,0:T(8,128)(2,1)S(1)} collective-permute-done((bf16[704,256]{1,0:T(8,128)(2,1)S(1)}, bf16[704,256]{1,0:T(8,128)(2,1)S(1)}, u32[]{:S(2)}, u32[]{:S(2)}) %collective-permute-start.30) | collective-permute-done | bytes 360480 | tf_op jit(solution)/shard_map/ppermute | solution.py:123
  167.9 1.5 collective-permute-start.21
  169.4 6.2 %collective-permute-done.29.refs_5_ = bf16[704,256]{1,0:T(8,128)(2,1)S(1)} collective-permute-done((bf16[704,256]{1,0:T(8,128)(2,1)S(1)}, bf16[704,256]{1,0:T(8,128)(2,1)S(1)}, u32[]{:S(2)}, u32[]{:S(2)}) %collective-permute-start.29) | collective-permute-done | bytes 360480 | tf_op jit(solution)/shard_map/ppermute | solution.py:123
  175.6 1.5 collective-permute-start.23
  177.7 1.6 collective-permute-start.24
  179.4 7.8 %shard_map.184 = (bf16[2048,1024]{1,0:T(8,128)(2,1)}, bf16[1024,256]{1,0:T(8,128)(2,1)}) custom-call(s32[5]{0:T(128)} %stack.86.spot_ref, bf16[4,64,1024]{2,1,0:T(8,128)(2,1)} %copy-done.2, bf16[4,64,1024]{2,1,0:T(8,128)(2,1)} %copy-done.14, bf16[2,4,128,256]{3,2,1,0:T(8,128)(2,1)} %copy-done.1, bf16[2,4,128,256]{3,2,1,0:T(8,128)(2,1)} %copy-done.3, ...), custom_call_target="tpu_custom_call" | custom-call | tf_op jit(solution)/shard_map/pallas_call | solution.py:398
  187.2 7.6 %shard_map.186.refs_9_ = bf16[704,1024]{1,0:T(8,128)(2,1)} custom-call(s32[5]{0:T(128)} %stack.86.spot_ref, bf16[704,256]{1,0:T(8,128)(2,1)} %get-tuple-element.45.refs_0_, bf16[704,256]{1,0:T(8,128)(2,1)} %copy-done.16, bf16[704,256]{1,0:T(8,128)(2,1)} %copy-done.15, bf16[704,256]{1,0:T(8,128)(2,1)} %copy-done.17, bf16[704,256]{1,0:T(8,128)(2,1)} %copy-done.19, ...), custom_call_target="tpu_custom_call" | custom-call | tf_op jit(solution)/shard_map/pallas_call | solution.py:398
  194.8 7.8 %shard_map.187.refs_8_ = bf16[704,1024]{1,0:T(8,128)(2,1)} custom-call(s32[5]{0:T(128)} %stack.86.spot_ref, bf16[704,256]{1,0:T(8,128)(2,1)} %get-tuple-element.42.refs_0_, bf16[704,256]{1,0:T(8,128)(2,1)} %copy-done.20, bf16[704,256]{1,0:T(8,128)(2,1)} %copy-done.18, bf16[704,256]{1,0:T(8,128)(2,1)} %collective-permute-done.27.refs_3_, ...), custom_call_target="tpu_custom_call" | custom-call | tf_op jit(solution)/shard_map/pallas_call | solution.py:398
  202.7 5.4 %shard_map.188 = (bf16[4,512,256]{2,1,0:T(8,128)(2,1)}, bf16[4,512,256]{2,1,0:T(8,128)(2,1)}) custom-call(s32[5]{0:T(128)} %stack.86.spot_ref, bf16[704,128]{1,0:T(8,128)(2,1)} %get-tuple-element.31.refs_0_, bf16[704,128]{1,0:T(8,128)(2,1)} %copy-done.29, bf16[704,128]{1,0:T(8,128)(2,1)} %copy-done.28, bf16[704,128]{1,0:T(8,128)(2,1)} %collective-permute-done.20.refs_3_, ...), custom_call_target="tpu_custom_call" | custom-call | tf_op jit(solution)/shard_map/pallas_call | solution.py:398
  208.2 1.7 collective-permute-start.43
  209.9 2.6 collective-permute-start.45
  213.2 6.7 %collective-permute-done.44.refs_2_ = bf16[704,128]{1,0:T(8,128)(2,1)S(1)} collective-permute-done((bf16[704,128]{1,0:T(8,128)(2,1)S(1)}, bf16[704,128]{1,0:T(8,128)(2,1)S(1)}, u32[]{:S(2)}, u32[]{:S(2)}) %collective-permute-start.44) | collective-permute-done | bytes 180256 | tf_op jit(solution)/shard_map/ppermute | solution.py:123
  220.5 1.4 collective-permute-start.47
  221.9 1.4 collective-permute-done.45.refs_3_
  223.9 3.4 %collective-permute-done.48.refs_6_ = bf16[704,128]{1,0:T(8,128)(2,1)S(1)} collective-permute-done((bf16[704,128]{1,0:T(8,128)(2,1)S(1)}, bf16[704,128]{1,0:T(8,128)(2,1)S(1)}, u32[]{:S(2)}, u32[]{:S(2)}) %collective-permute-start.48) | collective-permute-done | bytes 180256 | tf_op jit(solution)/shard_map/ppermute | solution.py:123
  227.3 3.9 %collective-permute-done.47.refs_5_ = bf16[704,128]{1,0:T(8,128)(2,1)S(1)} collective-permute-done((bf16[704,128]{1,0:T(8,128)(2,1)S(1)}, bf16[704,128]{1,0:T(8,128)(2,1)S(1)}, u32[]{:S(2)}, u32[]{:S(2)}) %collective-permute-start.47) | collective-permute-done | bytes 180256 | tf_op jit(solution)/shard_map/ppermute | solution.py:123
  231.8 2.3 collective-permute-done.49.refs_7_
  234.1 5.4 %shard_map.189 = (bf16[4,512,256]{2,1,0:T(8,128)(2,1)}, bf16[4,512,256]{2,1,0:T(8,128)(2,1)}) custom-call(s32[5]{0:T(128)} %stack.86.spot_ref, bf16[704,128]{1,0:T(8,128)(2,1)} %get-tuple-element.49.refs_0_, bf16[704,128]{1,0:T(8,128)(2,1)} %copy-done.31, bf16[704,128]{1,0:T(8,128)(2,1)} %copy-done.30, bf16[704,128]{1,0:T(8,128)(2,1)} %copy-done.32, ...), custom_call_target="tpu_custom_call" | custom-call | tf_op jit(solution)/shard_map/pallas_call | solution.py:398
  240.0 1.4 collective-permute-start.41
  241.4 1.9 collective-permute-start.42
  244.0 1.4 collective-permute-start.52
  245.4 4.5 %collective-permute-done.40 = bf16[512,256]{1,0:T(8,128)(2,1)S(1)} collective-permute-done((bf16[512,256]{1,0:T(8,128)(2,1)S(1)}, bf16[512,256]{1,0:T(8,128)(2,1)S(1)}, u32[]{:S(2)}, u32[]{:S(2)}) %collective-permute-start.40) | collective-permute-done | bytes 262176 | tf_op jit(solution)/shard_map/ppermute | solution.py:123
  250.1 4.9 %collective-permute-done.41 = bf16[512,256]{1,0:T(8,128)(2,1)S(1)} collective-permute-done((bf16[512,256]{1,0:T(8,128)(2,1)S(1)}, bf16[512,256]{1,0:T(8,128)(2,1)S(1)}, u32[]{:S(2)}, u32[]{:S(2)}) %collective-permute-start.41) | collective-permute-done | bytes 262176 | tf_op jit(solution)/shard_map/ppermute | solution.py:123
  255.1 6.2 %collective-permute-done.51 = bf16[512,256]{1,0:T(8,128)(2,1)S(1)} collective-permute-done((bf16[512,256]{1,0:T(8,128)(2,1)S(1)}, bf16[512,256]{1,0:T(8,128)(2,1)S(1)}, u32[]{:S(2)}, u32[]{:S(2)}) %collective-permute-start.51) | collective-permute-done | bytes 262176 | tf_op jit(solution)/shard_map/ppermute | solution.py:123
  261.2 4.2 %collective-permute-done.52 = bf16[512,256]{1,0:T(8,128)(2,1)S(1)} collective-permute-done((bf16[512,256]{1,0:T(8,128)(2,1)S(1)}, bf16[512,256]{1,0:T(8,128)(2,1)S(1)}, u32[]{:S(2)}, u32[]{:S(2)}) %collective-permute-start.52) | collective-permute-done | bytes 262176 | tf_op jit(solution)/shard_map/ppermute | solution.py:123
  265.7 0.8 copy.23
  (154 shorter events, 10.3 us)
Async XLA Ops:
  0.0 28.6 %collective-permute-start.5 = (bf16[1024,256]{1,0:T(8,128)(2,1)}, bf16[1024,256]{1,0:T(8,128)(2,1)S(1)}, u32[]{:S(2)}, u32[]{:S(2)}) collective-permute-start(bf16[1024,256]{1,0:T(8,128)(2,1)} %refs_0_.4), channel_id=1, source_target_pairs={{0,4},{4,0},{1,5},{5,1},{2,6},{6,2},{3,7},{7,3},{8,12},{12,8},{9,1... | collective-permute-start | bytes 1572872 | tf_op jit(solution)/shard_map/ppermute | solution.py:123
  6.4 15.8 %collective-permute-start = (bf16[320,256]{1,0:T(8,128)(2,1)}, bf16[320,256]{1,0:T(8,128)(2,1)S(1)}, u32[]{:S(2)}, u32[]{:S(2)}) collective-permute-start(bf16[320,256]{1,0:T(8,128)(2,1)} %get-tuple-element.30), channel_id=1, source_target_pairs={{0,4},{4,0},{1,5},{5,1},{2,6},{6,2},{3,7},{7,3},{8,12},{12,8},{9,1... | collective-permute-start | bytes 491528 | tf_op jit(solution)/shard_map/ppermute | solution.py:123
  6.5 16.3 %collective-permute-start.1 = (bf16[320,256]{1,0:T(8,128)(2,1)}, bf16[320,256]{1,0:T(8,128)(2,1)S(1)}, u32[]{:S(2)}, u32[]{:S(2)}) collective-permute-start(bf16[320,256]{1,0:T(8,128)(2,1)} %get-tuple-element.32), channel_id=1, source_target_pairs={{0,8},{8,0},{1,9},{9,1},{2,10},{10,2},{3,11},{11,3},{4,12},{12,4},... | collective-permute-start | bytes 491528 | tf_op jit(solution)/shard_map/ppermute | solution.py:123
  9.5 18.4 %collective-permute-start.2 = (bf16[320,256]{1,0:T(8,128)(2,1)}, bf16[320,256]{1,0:T(8,128)(2,1)S(1)}, u32[]{:S(2)}, u32[]{:S(2)}) collective-permute-start(bf16[320,256]{1,0:T(8,128)(2,1)} %get-tuple-element.30), channel_id=1, source_target_pairs={{0,12},{4,8},{8,4},{12,0},{1,13},{5,9},{9,5},{13,1},{2,14},{6,10},... | collective-permute-start | bytes 491528 | tf_op jit(solution)/shard_map/ppermute | solution.py:123
  10.8 21.9 %collective-permute-start.7 = (bf16[1024,256]{1,0:T(8,128)(2,1)}, bf16[1024,256]{1,0:T(8,128)(2,1)S(1)}, u32[]{:S(2)}, u32[]{:S(2)}) collective-permute-start(bf16[1024,256]{1,0:T(8,128)(2,1)} %refs_0_.4), channel_id=1, source_target_pairs={{0,1},{1,0},{2,3},{3,2},{4,5},{5,4},{6,7},{7,6},{8,9},{9,8},{10,11... | collective-permute-start | bytes 1572872 | tf_op jit(solution)/shard_map/ppermute | solution.py:123
  22.2 20.0 %collective-permute-start.4 = (bf16[1024,256]{1,0:T(8,128)(2,1)S(1)}, bf16[1024,256]{1,0:T(8,128)(2,1)S(1)}, u32[]{:S(2)}, u32[]{:S(2)}) collective-permute-start(bf16[1024,256]{1,0:T(8,128)(2,1)S(1)} %copy-done.9), channel_id=1, source_target_pairs={{0,16},{16,0},{1,17},{17,1},{2,18},{18,2},{3,19},{19,3},{4,20},{20... | collective-permute-start | bytes 1572872 | tf_op jit(solution)/shard_map/ppermute | solution.py:123
  28.6 12.8 %collective-permute-start.9 = (bf16[1024,256]{1,0:T(8,128)(2,1)S(1)}, bf16[1024,256]{1,0:T(8,128)(2,1)S(1)}, u32[]{:S(2)}, u32[]{:S(2)}) collective-permute-start(bf16[1024,256]{1,0:T(8,128)(2,1)S(1)} %collective-permute-done.5.refs_2_), channel_id=1, source_target_pairs={{0,1},{1,0},{2,3},{3,2},{4,5},{5,4},{6,7},{7,6},{8,9},{9,8},{10,11... | collective-permute-start | bytes 1572872 | tf_op jit(solution)/shard_map/ppermute | solution.py:123
  30.2 14.4 %collective-permute-start.11 = (bf16[4,192,256]{2,1,0:T(8,128)(2,1)S(1)}, bf16[4,192,256]{2,1,0:T(8,128)(2,1)}, u32[]{:S(2)}, u32[]{:S(2)}) collective-permute-start(bf16[4,192,256]{2,1,0:T(8,128)(2,1)S(1)} %pad_maximum_fusion.4.refs_8_), channel_id=1, source_target_pairs={{0,2},{2,0},{1,3},{3,1},{4,6},{6,4},{5,7},{7,5},{8,10},{10,8},{9,1... | collective-permute-start | bytes 1179656 | tf_op jit(solution)/shard_map/ppermute | solution.py:123
  32.6 12.0 %collective-permute-start.6 = (bf16[1024,256]{1,0:T(8,128)(2,1)S(1)}, bf16[1024,256]{1,0:T(8,128)(2,1)}, u32[]{:S(2)}, u32[]{:S(2)}) collective-permute-start(bf16[1024,256]{1,0:T(8,128)(2,1)S(1)} %collective-permute-done.5.refs_2_), channel_id=1, source_target_pairs={{0,16},{16,0},{1,17},{17,1},{2,18},{18,2},{3,19},{19,3},{4,20},{20... | collective-permute-start | bytes 1572872 | tf_op jit(solution)/shard_map/ppermute | solution.py:123
  32.7 11.9 %collective-permute-start.8 = (bf16[1024,256]{1,0:T(8,128)(2,1)S(1)}, bf16[1024,256]{1,0:T(8,128)(2,1)}, u32[]{:S(2)}, u32[]{:S(2)}) collective-permute-start(bf16[1024,256]{1,0:T(8,128)(2,1)S(1)} %collective-permute-done.7.refs_4_), channel_id=1, source_target_pairs={{0,16},{16,0},{1,17},{17,1},{2,18},{18,2},{3,19},{19,3},{4,20},{20... | collective-permute-start | bytes 1572872 | tf_op jit(solution)/shard_map/ppermute | solution.py:123
  41.4 3.2 %collective-permute-start.10 = (bf16[1024,256]{1,0:T(8,128)(2,1)S(1)}, bf16[1024,256]{1,0:T(8,128)(2,1)}, u32[]{:S(2)}, u32[]{:S(2)}) collective-permute-start(bf16[1024,256]{1,0:T(8,128)(2,1)S(1)} %collective-permute-done.9.refs_6_), channel_id=1, source_target_pairs={{0,16},{16,0},{1,17},{17,1},{2,18},{18,2},{3,19},{19,3},{4,20},{20... | collective-permute-start | bytes 1572872 | tf_op jit(solution)/shard_map/ppermute | solution.py:123
  42.3 8.8 %collective-permute-start.3 = (bf16[4,128,256]{2,1,0:T(8,128)(2,1)}, bf16[4,128,256]{2,1,0:T(8,128)(2,1)S(1)}, u32[]{:S(2)}, u32[]{:S(2)}) collective-permute-start(bf16[4,128,256]{2,1,0:T(8,128)(2,1)} %get-tuple-element.64), channel_id=1, source_target_pairs={{0,2},{2,0},{1,3},{3,1},{4,6},{6,4},{5,7},{7,5},{8,10},{10,8},{9,1... | collective-permute-start | bytes 786440 | tf_op jit(solution)/shard_map/ppermute | solution.py:123
  51.2 45.9 %collective-permute-start.16 = (bf16[2,4,128,256]{3,2,1,0:T(8,128)(2,1)S(1)}, bf16[2,4,128,256]{3,2,1,0:T(8,128)(2,1)S(1)}, u32[]{:S(2)}, u32[]{:S(2)}) collective-permute-start(bf16[2,4,128,256]{3,2,1,0:T(8,128)(2,1)S(1)} %get-tuple-element.62.refs_2_), channel_id=1, source_target_pairs={{0,1},{1,0},{2,3},{3,2},{4,5},{5,4},{6,7},{7,6},{8,9},{9,8},{10,11... | collective-permute-start | bytes 1572872 | tf_op jit(solution)/shard_map/ppermute | solution.py:123
  52.7 11.3 %collective-permute-start.19 = (bf16[704,128]{1,0:T(8,128)(2,1)S(1)}, bf16[704,128]{1,0:T(8,128)(2,1)S(1)}, u32[]{:S(2)}, u32[]{:S(2)}) collective-permute-start(bf16[704,128]{1,0:T(8,128)(2,1)S(1)} %copy-done.27), channel_id=1, source_target_pairs={{0,8},{8,0},{1,9},{9,1},{2,10},{10,2},{3,11},{11,3},{4,12},{12,4},... | collective-permute-start | bytes 540680 | tf_op jit(solution)/shard_map/ppermute | solution.py:123
  52.7 17.9 %collective-permute-start.18 = (bf16[704,128]{1,0:T(8,128)(2,1)S(1)}, bf16[704,128]{1,0:T(8,128)(2,1)S(1)}, u32[]{:S(2)}, u32[]{:S(2)}) collective-permute-start(bf16[704,128]{1,0:T(8,128)(2,1)S(1)} %copy-done.39), channel_id=1, source_target_pairs={{0,4},{4,0},{1,5},{5,1},{2,6},{6,2},{3,7},{7,3},{8,12},{12,8},{9,1... | collective-permute-start | bytes 540680 | tf_op jit(solution)/shard_map/ppermute | solution.py:123
  56.4 69.2 %copy-start.38 = (bf16[64,1024]{1,0:T(8,128)(2,1)S(1)}, bf16[64,1024]{1,0:T(8,128)(2,1)}, u32[]{:S(2)}) copy-start(bf16[64,1024]{1,0:T(8,128)(2,1)} %get-tuple-element.37) | copy-start | bytes 393220
  60.8 25.2 %collective-permute-start.33 = (bf16[704,256]{1,0:T(8,128)(2,1)}, bf16[704,256]{1,0:T(8,128)(2,1)S(1)}, u32[]{:S(2)}, u32[]{:S(2)}) collective-permute-start(bf16[704,256]{1,0:T(8,128)(2,1)} %get-tuple-element.45.refs_0_), channel_id=1, source_target_pairs={{0,8},{8,0},{1,9},{9,1},{2,10},{10,2},{3,11},{11,3},{4,12},{12,4},... | collective-permute-start | bytes 1081352 | tf_op jit(solution)/shard_map/ppermute | solution.py:123
  60.9 35.5 %collective-permute-start.32 = (bf16[704,256]{1,0:T(8,128)(2,1)}, bf16[704,256]{1,0:T(8,128)(2,1)S(1)}, u32[]{:S(2)}, u32[]{:S(2)}) collective-permute-start(bf16[704,256]{1,0:T(8,128)(2,1)} %get-tuple-element.46), channel_id=1, source_target_pairs={{0,4},{4,0},{1,5},{5,1},{2,6},{6,2},{3,7},{7,3},{8,12},{12,8},{9,1... | collective-permute-start | bytes 1081352 | tf_op jit(solution)/shard_map/ppermute | solution.py:123
  64.0 74.2 %copy-start.28 = (bf16[704,128]{1,0:T(8,128)(2,1)}, bf16[704,128]{1,0:T(8,128)(2,1)S(1)}, u32[]{:S(2)}) copy-start(bf16[704,128]{1,0:T(8,128)(2,1)S(1)} %collective-permute-done.19.refs_2_) | copy-start | bytes 540676
  64.0 20.4 %collective-permute-start.20 = (bf16[704,128]{1,0:T(8,128)(2,1)S(1)}, bf16[704,128]{1,0:T(8,128)(2,1)}, u32[]{:S(2)}, u32[]{:S(2)}) collective-permute-start(bf16[704,128]{1,0:T(8,128)(2,1)S(1)} %copy-done.39), channel_id=1, source_target_pairs={{0,12},{4,8},{8,4},{12,0},{1,13},{5,9},{9,5},{13,1},{2,14},{6,10},... | collective-permute-start | bytes 540680 | tf_op jit(solution)/shard_map/ppermute | solution.py:123
  70.7 67.5 %copy-start.29 = (bf16[704,128]{1,0:T(8,128)(2,1)}, bf16[704,128]{1,0:T(8,128)(2,1)S(1)}, u32[]{:S(2)}) copy-start(bf16[704,128]{1,0:T(8,128)(2,1)S(1)} %collective-permute-done.18.refs_1_) | copy-start | bytes 540676
  70.7 28.8 %collective-permute-start.34 = (bf16[704,256]{1,0:T(8,128)(2,1)}, bf16[704,256]{1,0:T(8,128)(2,1)S(1)}, u32[]{:S(2)}, u32[]{:S(2)}) collective-permute-start(bf16[704,256]{1,0:T(8,128)(2,1)} %get-tuple-element.46), channel_id=1, source_target_pairs={{0,12},{4,8},{8,4},{12,0},{1,13},{5,9},{9,5},{13,1},{2,14},{6,10},... | collective-permute-start | bytes 1081352 | tf_op jit(solution)/shard_map/ppermute | solution.py:123
  84.5 15.2 %collective-permute-start.35 = (bf16[704,256]{1,0:T(8,128)(2,1)}, bf16[704,256]{1,0:T(8,128)(2,1)S(1)}, u32[]{:S(2)}, u32[]{:S(2)}) collective-permute-start(bf16[704,256]{1,0:T(8,128)(2,1)} %get-tuple-element.45.refs_0_), channel_id=1, source_target_pairs={{0,2},{2,0},{1,3},{3,1},{4,6},{6,4},{5,7},{7,5},{8,10},{10,8},{9,1... | collective-permute-start | bytes 1081352 | tf_op jit(solution)/shard_map/ppermute | solution.py:123
  86.0 101.2 %copy-start.15 = (bf16[704,256]{1,0:T(8,128)(2,1)}, bf16[704,256]{1,0:T(8,128)(2,1)S(1)}, u32[]{:S(2)}) copy-start(bf16[704,256]{1,0:T(8,128)(2,1)S(1)} %collective-permute-done.33.refs_2_) | copy-start | bytes 1081348
  86.0 39.7 %collective-permute-start.26 = (bf16[704,256]{1,0:T(8,128)(2,1)}, bf16[704,256]{1,0:T(8,128)(2,1)S(1)}, u32[]{:S(2)}, u32[]{:S(2)}) collective-permute-start(bf16[704,256]{1,0:T(8,128)(2,1)} %get-tuple-element.42.refs_0_), channel_id=1, source_target_pairs={{0,8},{8,0},{1,9},{9,1},{2,10},{10,2},{3,11},{11,3},{4,12},{12,4},... | collective-permute-start | bytes 1081352 | tf_op jit(solution)/shard_map/ppermute | solution.py:123
  96.4 90.8 %copy-start.16 = (bf16[704,256]{1,0:T(8,128)(2,1)}, bf16[704,256]{1,0:T(8,128)(2,1)S(1)}, u32[]{:S(2)}) copy-start(bf16[704,256]{1,0:T(8,128)(2,1)S(1)} %collective-permute-done.32.refs_1_) | copy-start | bytes 1081348
  96.4 29.3 %collective-permute-start.25 = (bf16[704,256]{1,0:T(8,128)(2,1)}, bf16[704,256]{1,0:T(8,128)(2,1)S(1)}, u32[]{:S(2)}, u32[]{:S(2)}) collective-permute-start(bf16[704,256]{1,0:T(8,128)(2,1)} %get-tuple-element.43), channel_id=1, source_target_pairs={{0,4},{4,0},{1,5},{5,1},{2,6},{6,2},{3,7},{7,3},{8,12},{12,8},{9,1... | collective-permute-start | bytes 1081352 | tf_op jit(solution)/shard_map/ppermute | solution.py:123
  97.1 82.3 %copy-start.3 = (bf16[2,4,128,256]{3,2,1,0:T(8,128)(2,1)}, bf16[2,4,128,256]{3,2,1,0:T(8,128)(2,1)S(1)}, u32[]{:S(2)}) copy-start(bf16[2,4,128,256]{3,2,1,0:T(8,128)(2,1)S(1)} %collective-permute-done.16.refs_3_) | copy-start | bytes 1572868
  97.1 29.2 %collective-permute-start.27 = (bf16[704,256]{1,0:T(8,128)(2,1)}, bf16[704,256]{1,0:T(8,128)(2,1)}, u32[]{:S(2)}, u32[]{:S(2)}) collective-permute-start(bf16[704,256]{1,0:T(8,128)(2,1)} %get-tuple-element.43), channel_id=1, source_target_pairs={{0,12},{4,8},{8,4},{12,0},{1,13},{5,9},{9,5},{13,1},{2,14},{6,10},... | collective-permute-start | bytes 1081352 | tf_op jit(solution)/shard_map/ppermute | solution.py:123
  99.5 78.2 %copy-start.17 = (bf16[704,256]{1,0:T(8,128)(2,1)}, bf16[704,256]{1,0:T(8,128)(2,1)S(1)}, u32[]{:S(2)}) copy-start(bf16[704,256]{1,0:T(8,128)(2,1)S(1)} %collective-permute-done.34.refs_3_) | copy-start | bytes 1081348
  99.5 78.1 %collective-permute-start.17 = (bf16[2,2,4,128,256]{4,3,2,1,0:T(8,128)(2,1)S(1)}, bf16[2,2,4,128,256]{4,3,2,1,0:T(8,128)(2,1)S(1)}, u32[]{:S(2)}, u32[]{:S(2)}) collective-permute-start(bf16[2,2,4,128,256]{4,3,2,1,0:T(8,128)(2,1)S(1)} %pad_maximum_fusion), channel_id=1, source_target_pairs={{0,16},{16,0},{1,17},{17,1},{2,18},{18,2},{3,19},{19,3},{4,20},{20... | collective-permute-start | bytes 3145736 | tf_op jit(solution)/shard_map/ppermute | solution.py:123
  99.6 79.6 %copy-start.19 = (bf16[704,256]{1,0:T(8,128)(2,1)}, bf16[704,256]{1,0:T(8,128)(2,1)S(1)}, u32[]{:S(2)}) copy-start(bf16[704,256]{1,0:T(8,128)(2,1)S(1)} %collective-permute-done.35.refs_4_) | copy-start | bytes 1081348
  99.6 38.6 %collective-permute-start.28 = (bf16[704,256]{1,0:T(8,128)(2,1)}, bf16[704,256]{1,0:T(8,128)(2,1)}, u32[]{:S(2)}, u32[]{:S(2)}) collective-permute-start(bf16[704,256]{1,0:T(8,128)(2,1)} %get-tuple-element.42.refs_0_), channel_id=1, source_target_pairs={{0,2},{2,0},{1,3},{3,1},{4,6},{6,4},{5,7},{7,5},{8,10},{10,8},{9,1... | collective-permute-start | bytes 1081352 | tf_op jit(solution)/shard_map/ppermute | solution.py:123
  125.7 53.6 %copy-start.18 = (bf16[704,256]{1,0:T(8,128)(2,1)}, bf16[704,256]{1,0:T(8,128)(2,1)S(1)}, u32[]{:S(2)}) copy-start(bf16[704,256]{1,0:T(8,128)(2,1)S(1)} %collective-permute-done.26.refs_2_) | copy-start | bytes 1081348
  125.7 7.8 %collective-permute-start.12 = (bf16[64,1024]{1,0:T(8,128)(2,1)S(1)}, bf16[64,1024]{1,0:T(8,128)(2,1)S(1)}, u32[]{:S(2)}, u32[]{:S(2)}) collective-permute-start(bf16[64,1024]{1,0:T(8,128)(2,1)S(1)} %copy-done.38), channel_id=1, source_target_pairs={{0,4},{4,0},{1,5},{5,1},{2,6},{6,2},{3,7},{7,3},{8,12},{12,8},{9,1... | collective-permute-start | bytes 393224 | tf_op jit(solution)/shard_map/ppermute | solution.py:123
  125.7 53.6 %copy-start.20 = (bf16[704,256]{1,0:T(8,128)(2,1)}, bf16[704,256]{1,0:T(8,128)(2,1)S(1)}, u32[]{:S(2)}) copy-start(bf16[704,256]{1,0:T(8,128)(2,1)S(1)} %collective-permute-done.25.refs_1_) | copy-start | bytes 1081348
  125.7 9.3 %collective-permute-start.13 = (bf16[64,1024]{1,0:T(8,128)(2,1)S(1)}, bf16[64,1024]{1,0:T(8,128)(2,1)S(1)}, u32[]{:S(2)}, u32[]{:S(2)}) collective-permute-start(bf16[64,1024]{1,0:T(8,128)(2,1)S(1)} %copy-done.38), channel_id=1, source_target_pairs={{0,1},{1,0},{2,3},{3,2},{4,5},{5,4},{6,7},{7,6},{8,9},{9,8},{10,11... | collective-permute-start | bytes 393224 | tf_op jit(solution)/shard_map/ppermute | solution.py:123
  126.3 10.4 %collective-permute-start.14 = (bf16[64,1024]{1,0:T(8,128)(2,1)S(1)}, bf16[64,1024]{1,0:T(8,128)(2,1)S(1)}, u32[]{:S(2)}, u32[]{:S(2)}) collective-permute-start(bf16[64,1024]{1,0:T(8,128)(2,1)S(1)} %copy-done.38), channel_id=1, source_target_pairs={{0,5},{1,4},{4,1},{5,0},{2,7},{3,6},{6,3},{7,2},{8,13},{9,12},{12,... | collective-permute-start | bytes 393224 | tf_op jit(solution)/shard_map/ppermute | solution.py:123
  133.5 11.3 %collective-permute-start.37 = (bf16[704,256]{1,0:T(8,128)(2,1)S(1)}, bf16[704,256]{1,0:T(8,128)(2,1)S(1)}, u32[]{:S(2)}, u32[]{:S(2)}) collective-permute-start(bf16[704,256]{1,0:T(8,128)(2,1)S(1)} %collective-permute-done.33.refs_2_), channel_id=1, source_target_pairs={{0,2},{2,0},{1,3},{3,1},{4,6},{6,4},{5,7},{7,5},{8,10},{10,8},{9,1... | collective-permute-start | bytes 1081352 | tf_op jit(solution)/shard_map/ppermute | solution.py:123
  135.0 17.5 %collective-permute-start.36 = (bf16[704,256]{1,0:T(8,128)(2,1)S(1)}, bf16[704,256]{1,0:T(8,128)(2,1)S(1)}, u32[]{:S(2)}, u32[]{:S(2)}) collective-permute-start(bf16[704,256]{1,0:T(8,128)(2,1)S(1)} %collective-permute-done.32.refs_1_), channel_id=1, source_target_pairs={{0,2},{2,0},{1,3},{3,1},{4,6},{6,4},{5,7},{7,5},{8,10},{10,8},{9,1... | collective-permute-start | bytes 1081352 | tf_op jit(solution)/shard_map/ppermute | solution.py:123
  136.7 23.5 %collective-permute-start.38 = (bf16[704,256]{1,0:T(8,128)(2,1)S(1)}, bf16[704,256]{1,0:T(8,128)(2,1)S(1)}, u32[]{:S(2)}, u32[]{:S(2)}) collective-permute-start(bf16[704,256]{1,0:T(8,128)(2,1)S(1)} %collective-permute-done.34.refs_3_), channel_id=1, source_target_pairs={{0,2},{2,0},{1,3},{3,1},{4,6},{6,4},{5,7},{7,5},{8,10},{10,8},{9,1... | collective-permute-start | bytes 1081352 | tf_op jit(solution)/shard_map/ppermute | solution.py:123
  138.3 38.9 %collective-permute-start.15 = (bf16[4,64,1024]{2,1,0:T(8,128)(2,1)S(1)}, bf16[4,64,1024]{2,1,0:T(8,128)(2,1)S(1)}, u32[]{:S(2)}, u32[]{:S(2)}) collective-permute-start(bf16[4,64,1024]{2,1,0:T(8,128)(2,1)S(1)} %pad_maximum_fusion.1.refs_0_), channel_id=1, source_target_pairs={{0,16},{16,0},{1,17},{17,1},{2,18},{18,2},{3,19},{19,3},{4,20},{20... | collective-permute-start | bytes 1572872 | tf_op jit(solution)/shard_map/ppermute | solution.py:123
  144.7 23.2 %collective-permute-start.30 = (bf16[704,256]{1,0:T(8,128)(2,1)S(1)}, bf16[704,256]{1,0:T(8,128)(2,1)S(1)}, u32[]{:S(2)}, u32[]{:S(2)}) collective-permute-start(bf16[704,256]{1,0:T(8,128)(2,1)S(1)} %collective-permute-done.26.refs_2_), channel_id=1, source_target_pairs={{0,2},{2,0},{1,3},{3,1},{4,6},{6,4},{5,7},{7,5},{8,10},{10,8},{9,1... | collective-permute-start | bytes 1081352 | tf_op jit(solution)/shard_map/ppermute | solution.py:123
  152.5 23.2 %collective-permute-start.29 = (bf16[704,256]{1,0:T(8,128)(2,1)S(1)}, bf16[704,256]{1,0:T(8,128)(2,1)S(1)}, u32[]{:S(2)}, u32[]{:S(2)}) collective-permute-start(bf16[704,256]{1,0:T(8,128)(2,1)S(1)} %collective-permute-done.25.refs_1_), channel_id=1, source_target_pairs={{0,2},{2,0},{1,3},{3,1},{4,6},{6,4},{5,7},{7,5},{8,10},{10,8},{9,1... | collective-permute-start | bytes 1081352 | tf_op jit(solution)/shard_map/ppermute | solution.py:123
  160.2 34.7 %collective-permute-start.31 = (bf16[704,256]{1,0:T(8,128)(2,1)}, bf16[704,256]{1,0:T(8,128)(2,1)}, u32[]{:S(2)}, u32[]{:S(2)}) collective-permute-start(bf16[704,256]{1,0:T(8,128)(2,1)} %collective-permute-done.27.refs_3_), channel_id=1, source_target_pairs={{0,2},{2,0},{1,3},{3,1},{4,6},{6,4},{5,7},{7,5},{8,10},{10,8},{9,1... | collective-permute-start | bytes 1081352 | tf_op jit(solution)/shard_map/ppermute | solution.py:123
  167.9 34.8 %collective-permute-start.21 = (bf16[704,128]{1,0:T(8,128)(2,1)S(1)}, bf16[704,128]{1,0:T(8,128)(2,1)}, u32[]{:S(2)}, u32[]{:S(2)}) collective-permute-start(bf16[704,128]{1,0:T(8,128)(2,1)S(1)} %copy-done.27), channel_id=1, source_target_pairs={{0,2},{2,0},{1,3},{3,1},{4,6},{6,4},{5,7},{7,5},{8,10},{10,8},{9,1... | collective-permute-start | bytes 540680 | tf_op jit(solution)/shard_map/ppermute | solution.py:123
  175.6 27.1 %collective-permute-start.23 = (bf16[704,128]{1,0:T(8,128)(2,1)}, bf16[704,128]{1,0:T(8,128)(2,1)}, u32[]{:S(2)}, u32[]{:S(2)}) collective-permute-start(bf16[704,128]{1,0:T(8,128)(2,1)} %copy-done.28), channel_id=1, source_target_pairs={{0,2},{2,0},{1,3},{3,1},{4,6},{6,4},{5,7},{7,5},{8,10},{10,8},{9,1... | collective-permute-start | bytes 540680 | tf_op jit(solution)/shard_map/ppermute | solution.py:123
  177.2 25.5 %collective-permute-start.22 = (bf16[704,128]{1,0:T(8,128)(2,1)}, bf16[704,128]{1,0:T(8,128)(2,1)}, u32[]{:S(2)}, u32[]{:S(2)}) collective-permute-start(bf16[704,128]{1,0:T(8,128)(2,1)} %copy-done.29), channel_id=1, source_target_pairs={{0,2},{2,0},{1,3},{3,1},{4,6},{6,4},{5,7},{7,5},{8,10},{10,8},{9,1... | collective-permute-start | bytes 540680 | tf_op jit(solution)/shard_map/ppermute | solution.py:123
  177.7 25.0 %collective-permute-start.24 = (bf16[704,128]{1,0:T(8,128)(2,1)}, bf16[704,128]{1,0:T(8,128)(2,1)}, u32[]{:S(2)}, u32[]{:S(2)}) collective-permute-start(bf16[704,128]{1,0:T(8,128)(2,1)} %collective-permute-done.20.refs_3_), channel_id=1, source_target_pairs={{0,2},{2,0},{1,3},{3,1},{4,6},{6,4},{5,7},{7,5},{8,10},{10,8},{9,1... | collective-permute-start | bytes 540680 | tf_op jit(solution)/shard_map/ppermute | solution.py:123
  208.1 31.4 %collective-permute-start.39 = (bf16[4,512,256]{2,1,0:T(8,128)(2,1)}, bf16[4,512,256]{2,1,0:T(8,128)(2,1)S(1)}, u32[]{:S(2)}, u32[]{:S(2)}) collective-permute-start(bf16[4,512,256]{2,1,0:T(8,128)(2,1)} %get-tuple-element.48), channel_id=1, source_target_pairs={{0,16},{16,0},{1,17},{17,1},{2,18},{18,2},{3,19},{19,3},{4,20},{20... | collective-permute-start | bytes 3145736 | tf_op jit(solution)/shard_map/ppermute | solution.py:123
  208.1 11.8 %collective-permute-start.44 = (bf16[704,128]{1,0:T(8,128)(2,1)S(1)}, bf16[704,128]{1,0:T(8,128)(2,1)S(1)}, u32[]{:S(2)}, u32[]{:S(2)}) collective-permute-start(bf16[704,128]{1,0:T(8,128)(2,1)S(1)} %copy-done.26), channel_id=1, source_target_pairs={{0,8},{8,0},{1,9},{9,1},{2,10},{10,2},{3,11},{11,3},{4,12},{12,4},... | collective-permute-start | bytes 540680 | tf_op jit(solution)/shard_map/ppermute | solution.py:123
  208.2 12.3 %collective-permute-start.43 = (bf16[704,128]{1,0:T(8,128)(2,1)}, bf16[704,128]{1,0:T(8,128)(2,1)S(1)}, u32[]{:S(2)}, u32[]{:S(2)}) collective-permute-start(bf16[704,128]{1,0:T(8,128)(2,1)} %get-tuple-element.50), channel_id=1, source_target_pairs={{0,4},{4,0},{1,5},{5,1},{2,6},{6,2},{3,7},{7,3},{8,12},{12,8},{9,1... | collective-permute-start | bytes 540680 | tf_op jit(solution)/shard_map/ppermute | solution.py:123
  209.9 13.4 %collective-permute-start.45 = (bf16[704,128]{1,0:T(8,128)(2,1)}, bf16[704,128]{1,0:T(8,128)(2,1)S(1)}, u32[]{:S(2)}, u32[]{:S(2)}) collective-permute-start(bf16[704,128]{1,0:T(8,128)(2,1)} %get-tuple-element.50), channel_id=1, source_target_pairs={{0,12},{4,8},{8,4},{12,0},{1,13},{5,9},{9,5},{13,1},{2,14},{6,10},... | collective-permute-start | bytes 540680 | tf_op jit(solution)/shard_map/ppermute | solution.py:123
  212.6 11.4 %collective-permute-start.46 = (bf16[704,128]{1,0:T(8,128)(2,1)S(1)}, bf16[704,128]{1,0:T(8,128)(2,1)S(1)}, u32[]{:S(2)}, u32[]{:S(2)}) collective-permute-start(bf16[704,128]{1,0:T(8,128)(2,1)S(1)} %copy-done.26), channel_id=1, source_target_pairs={{0,2},{2,0},{1,3},{3,1},{4,6},{6,4},{5,7},{7,5},{8,10},{10,8},{9,1... | collective-permute-start | bytes 540680 | tf_op jit(solution)/shard_map/ppermute | solution.py:123
  219.9 7.4 %collective-permute-start.48 = (bf16[704,128]{1,0:T(8,128)(2,1)S(1)}, bf16[704,128]{1,0:T(8,128)(2,1)S(1)}, u32[]{:S(2)}, u32[]{:S(2)}) collective-permute-start(bf16[704,128]{1,0:T(8,128)(2,1)S(1)} %collective-permute-done.44.refs_2_), channel_id=1, source_target_pairs={{0,2},{2,0},{1,3},{3,1},{4,6},{6,4},{5,7},{7,5},{8,10},{10,8},{9,1... | collective-permute-start | bytes 540680 | tf_op jit(solution)/shard_map/ppermute | solution.py:123
  220.5 10.7 %collective-permute-start.47 = (bf16[704,128]{1,0:T(8,128)(2,1)S(1)}, bf16[704,128]{1,0:T(8,128)(2,1)S(1)}, u32[]{:S(2)}, u32[]{:S(2)}) collective-permute-start(bf16[704,128]{1,0:T(8,128)(2,1)S(1)} %collective-permute-done.43.refs_1_), channel_id=1, source_target_pairs={{0,2},{2,0},{1,3},{3,1},{4,6},{6,4},{5,7},{7,5},{8,10},{10,8},{9,1... | collective-permute-start | bytes 540680 | tf_op jit(solution)/shard_map/ppermute | solution.py:123
  223.3 10.8 %collective-permute-start.49 = (bf16[704,128]{1,0:T(8,128)(2,1)S(1)}, bf16[704,128]{1,0:T(8,128)(2,1)}, u32[]{:S(2)}, u32[]{:S(2)}) collective-permute-start(bf16[704,128]{1,0:T(8,128)(2,1)S(1)} %collective-permute-done.45.refs_3_), channel_id=1, source_target_pairs={{0,2},{2,0},{1,3},{3,1},{4,6},{6,4},{5,7},{7,5},{8,10},{10,8},{9,1... | collective-permute-start | bytes 540680 | tf_op jit(solution)/shard_map/ppermute | solution.py:123
  239.5 4.0 %collective-permute-start.50 = (bf16[4,512,256]{2,1,0:T(8,128)(2,1)}, bf16[4,512,256]{2,1,0:T(8,128)(2,1)S(1)}, u32[]{:S(2)}, u32[]{:S(2)}) collective-permute-start(bf16[4,512,256]{2,1,0:T(8,128)(2,1)} %get-tuple-element.52), channel_id=1, source_target_pairs={{0,16},{16,0},{1,17},{17,1},{2,18},{18,2},{3,19},{19,3},{4,20},{20... | collective-permute-start | bytes 3145736 | tf_op jit(solution)/shard_map/ppermute | solution.py:123
  239.8 10.2 %collective-permute-start.40 = (bf16[512,256]{1,0:T(8,128)(2,1)S(1)}, bf16[512,256]{1,0:T(8,128)(2,1)S(1)}, u32[]{:S(2)}, u32[]{:S(2)}) collective-permute-start(bf16[512,256]{1,0:T(8,128)(2,1)S(1)} %get-tuple-element.53), channel_id=1, source_target_pairs={{0,5},{1,4},{4,1},{5,0},{2,7},{3,6},{6,3},{7,2},{8,13},{9,12},{12,... | collective-permute-start | bytes 786440 | tf_op jit(solution)/shard_map/ppermute | solution.py:123
  240.0 15.0 %collective-permute-start.41 = (bf16[512,256]{1,0:T(8,128)(2,1)S(1)}, bf16[512,256]{1,0:T(8,128)(2,1)S(1)}, u32[]{:S(2)}, u32[]{:S(2)}) collective-permute-start(bf16[512,256]{1,0:T(8,128)(2,1)S(1)} %get-tuple-element.55), channel_id=1, source_target_pairs={{0,1},{1,0},{2,3},{3,2},{4,5},{5,4},{6,7},{7,6},{8,9},{9,8},{10,11... | collective-permute-start | bytes 786440 | tf_op jit(solution)/shard_map/ppermute | solution.py:123
  241.4 13.5 %collective-permute-start.42 = (bf16[512,256]{1,0:T(8,128)(2,1)S(1)}, bf16[512,256]{1,0:T(8,128)(2,1)S(1)}, u32[]{:S(2)}, u32[]{:S(2)}) collective-permute-start(bf16[512,256]{1,0:T(8,128)(2,1)S(1)} %get-tuple-element.54), channel_id=1, source_target_pairs={{0,4},{4,0},{1,5},{5,1},{2,6},{6,2},{3,7},{7,3},{8,12},{12,8},{9,1... | collective-permute-start | bytes 786440 | tf_op jit(solution)/shard_map/ppermute | solution.py:123
  243.8 17.5 %collective-permute-start.51 = (bf16[512,256]{1,0:T(8,128)(2,1)S(1)}, bf16[512,256]{1,0:T(8,128)(2,1)S(1)}, u32[]{:S(2)}, u32[]{:S(2)}) collective-permute-start(bf16[512,256]{1,0:T(8,128)(2,1)S(1)} %get-tuple-element.56), channel_id=1, source_target_pairs={{0,5},{1,4},{4,1},{5,0},{2,7},{3,6},{6,3},{7,2},{8,13},{9,12},{12,... | collective-permute-start | bytes 786440 | tf_op jit(solution)/shard_map/ppermute | solution.py:123
  244.0 21.5 %collective-permute-start.52 = (bf16[512,256]{1,0:T(8,128)(2,1)S(1)}, bf16[512,256]{1,0:T(8,128)(2,1)S(1)}, u32[]{:S(2)}, u32[]{:S(2)}) collective-permute-start(bf16[512,256]{1,0:T(8,128)(2,1)S(1)} %get-tuple-element.58), channel_id=1, source_target_pairs={{0,1},{1,0},{2,3},{3,2},{4,5},{5,4},{6,7},{7,6},{8,9},{9,8},{10,11... | collective-permute-start | bytes 786440 | tf_op jit(solution)/shard_map/ppermute | solution.py:123
  250.0 15.6 %collective-permute-start.53 = (bf16[512,256]{1,0:T(8,128)(2,1)S(1)}, bf16[512,256]{1,0:T(8,128)(2,1)S(1)}, u32[]{:S(2)}, u32[]{:S(2)}) collective-permute-start(bf16[512,256]{1,0:T(8,128)(2,1)S(1)} %get-tuple-element.57), channel_id=1, source_target_pairs={{0,4},{4,0},{1,5},{5,1},{2,6},{6,2},{3,7},{7,3},{8,12},{12,8},{9,1... | collective-permute-start | bytes 786440 | tf_op jit(solution)/shard_map/ppermute | solution.py:123
  (30 other events, 435.6 us)
